TPU v7x, 32 devices: a whole 2x2x4 slice. The times are simulated.
32 devices in a mesh: dp: 4 (over y, x), kv: 4 (over z), tp: 2 (over core).
Axes of the slice: x: 2, y: 2, z: 4, core: 2. Of those that a mesh axis runs over, the one named last changes fastest.
Arguments:
- tokens: bfloat16 [16, 4096], P('dp', ('kv', 'tp')), may hold values from -24 to 24
- rec_state: float32 [16, 16, 128, 128], P(('dp', 'kv'), 'tp'), may hold values from -2 to 2
- norm_gain: float32 [4096], replicated, may hold values from 0.1 to 1.9
- w_query: bfloat16 [4096, 2048], P('kv', 'tp'), may hold values from -0.09375 to 0.09375
- w_forget: bfloat16 [4096, 2048], P('kv', 'tp'), may hold values from -0.09375 to 0.09375
- w_input: bfloat16 [4096, 2048], P('kv', 'tp'), may hold values from -0.09375 to 0.09375
- w_outgate: bfloat16 [4096, 2048], P('kv', 'tp'), may hold values from -0.09375 to 0.09375
- lower_bound: float32 [2048], P('tp'), may hold values from 0 to 0.9
- head_gain: float32 [2048], P('tp'), may hold values from 0.1 to 1.9
- w_heads_out: bfloat16 [2048, 4096], P(None, ('kv', 'tp')), may hold values from -0.125 to 0.125
- mixer_gain: float32 [4096], replicated, may hold values from 0.1 to 1.9
- w_gate: bfloat16 [4096, 11264], P(None, ('kv', 'tp')), may hold values from -0.09375 to 0.09375
- w_up: bfloat16 [4096, 11264], P(None, ('kv', 'tp')), may hold values from -0.09375 to 0.09375
- w_down: bfloat16 [11264, 4096], P(('kv', 'tp')), may hold values from -0.078125 to 0.078125
Outputs:
- result: bfloat16 [16, 4096], P('dp', ('kv', 'tp'))
- new_state: float32 [16, 16, 128, 128], P(('dp', 'kv'), 'tp')
All inputs are finite; a program needn't handle non-finite values.
Results may differ from a plain program's by a relative error of at most 0.012.
Values may be sent and summed in bfloat16 or wider, within the bound.
No kernel may reach another device: no remote copies, remote signals or barrier semaphores. Data moves between devices by JAX's collectives and lax.ppermute only.
A program may use at most 128 MiB of HBM per device.

v0:
```python
import jax
import jax.numpy as jnp
from jax import lax
from jax.sharding import PartitionSpec as P

HEAD_DIM = 128


epsilon = 1e-06


def channel_mixer(whole_rows, mixer_gain, w_gate, w_up, w_down):
    rows_float = whole_rows.astype(jnp.float32)
    mixer_scale = lax.rsqrt(jnp.mean(rows_float * rows_float, axis=1, keepdims=True) + epsilon)
    normed = (rows_float * mixer_scale * mixer_gain).astype(jnp.bfloat16)
    gate_val = jnp.dot(normed, w_gate, preferred_element_type=jnp.float32)
    up_val = jnp.dot(normed, w_up, preferred_element_type=jnp.float32)
    hidden = (jax.nn.silu(gate_val) * up_val).astype(jnp.bfloat16)
    return jnp.dot(hidden, w_down, preferred_element_type=jnp.float32)


def local(
    tokens,
    rec_state,
    norm_gain,
    w_query,
    w_forget,
    w_input,
    w_outgate,
    lower_bound,
    head_gain,
    w_heads_out,
    mixer_gain,
    w_gate,
    w_up,
    w_down,
):
    kv_count = lax.axis_size("kv")
    tp_count = lax.axis_size("tp")
    kv_index = lax.axis_index("kv")
    row_count = tokens.shape[0]
    seq_count = rec_state.shape[0]
    model_width = norm_gain.shape[0]
    col_block = model_width // kv_count
    tok_float = tokens.astype(jnp.float32)
    whole_rows = lax.all_gather(tokens, ("kv", "tp"), axis=1, tiled=True).astype(jnp.float32)
    squares = jnp.sum(whole_rows * whole_rows, axis=1)
    own_cols = lax.dynamic_slice_in_dim(whole_rows, kv_index * col_block, col_block, 1)
    gain_block = lax.dynamic_slice_in_dim(norm_gain, kv_index * col_block, col_block, 0)
    scaled = (own_cols * gain_block).astype(jnp.bfloat16)
    projected = lax.psum_scatter(
        jnp.stack(
            [
                jnp.dot(scaled, weight, preferred_element_type=jnp.float32)
                for weight in (w_query, w_forget, w_input, w_outgate)
            ],
            axis=1,
        ),
        "kv",
        scatter_dimension=0,
        tiled=True,
    )
    my_squares = lax.dynamic_slice_in_dim(squares, kv_index * seq_count, seq_count, 0)
    row_scale = lax.rsqrt(my_squares / model_width + epsilon)[:, None]
    query_pre = row_scale * projected[:, 0]
    forget_pre = row_scale * projected[:, 1]
    value_in = row_scale * projected[:, 2]
    gate_pre = row_scale * projected[:, 3]
    forget = lower_bound + (1.0 - lower_bound) * jax.nn.sigmoid(forget_pre)
    key_in = 1.0 - forget
    query_act = jax.nn.silu(query_pre)
    head_count = rec_state.shape[1]
    shaped = (seq_count, head_count, HEAD_DIM)
    forget = forget.reshape(shaped)
    key_in = key_in.reshape(shaped)
    value_in = value_in.reshape(shaped)
    query_act = query_act.reshape(shaped)
    new_state = forget[:, :, :, None] * rec_state + key_in[:, :, :, None] * value_in[:, :, None, :]
    head_out = jnp.sum(query_act[:, :, :, None] * new_state, axis=2)
    head_out = head_out * lax.rsqrt(jnp.mean(head_out * head_out, axis=2, keepdims=True) + epsilon)
    head_out = head_out * head_gain.reshape(head_count, HEAD_DIM)
    local_width = head_count * HEAD_DIM
    gated = (head_out.reshape(seq_count, local_width) * jax.nn.silu(gate_pre)).astype(jnp.bfloat16)
    every_head = lax.all_gather(gated[None], ("kv", "tp"), axis=0, tiled=True)
    every_head = every_head.reshape(kv_count, tp_count, seq_count, local_width)
    every_head = every_head.transpose(0, 2, 1, 3).reshape(
        kv_count * seq_count, tp_count * local_width
    )
    mixed_add = jnp.dot(every_head, w_heads_out, preferred_element_type=jnp.float32)
    mixed = (tok_float + mixed_add).astype(jnp.bfloat16)
    gathered = lax.all_gather(mixed, ("kv", "tp"), axis=1, tiled=True)
    terms = channel_mixer(gathered, mixer_gain, w_gate, w_up, w_down)
    out_block = model_width // (kv_count * tp_count)
    blocked = terms.reshape(row_count, kv_count, tp_count, out_block)
    chip_sum = lax.psum_scatter(blocked.astype(jnp.bfloat16), "tp", scatter_dimension=2, tiled=True)
    down_sum = (
        lax.psum_scatter(chip_sum, "kv", scatter_dimension=1, tiled=True)
        .astype(jnp.float32)
        .reshape(row_count, out_block)
    )
    result = (mixed.astype(jnp.float32) + down_sum).astype(jnp.bfloat16)
    return (result, new_state)


def solution(mesh):
    placed = (
        P("dp", ("kv", "tp")),
        P(("dp", "kv"), "tp", None, None),
        P(),
        P("kv", "tp"),
        P("kv", "tp"),
        P("kv", "tp"),
        P("kv", "tp"),
        P("tp"),
        P("tp"),
        P(None, ("kv", "tp")),
        P(),
        P(None, ("kv", "tp")),
        P(None, ("kv", "tp")),
        P(("kv", "tp"), None),
    )
    return jax.shard_map(
        local,
        mesh=mesh,
        in_specs=placed,
        out_specs=(P("dp", ("kv", "tp")), P(("dp", "kv"), "tp", None, None)),
        check_vma=False,
    )
```

profile of v0, /device:TPU:0, one launch (start us, length us, event | category | flops | bytes accessed | tf_op | source)
XLA Modules:
  0.0 140.6 jit_solution(1454577620565583170)
XLA Ops:
  7.2 0.0 copy-start
  7.2 0.0 all-reduce.5.cloned.1.call-start
  7.2 16.1 %all_gather.9 = bf16[4,4096]{1,0:T(4,128)(2,1)S(1)} all-gather(bf16[4,512]{1,0:T(4,128)(2,1)} %param.14), channel_id=1, replica_groups=mesh['dp'=4,'kv'=4,'tp'=2] {'kv','tp'}, dimensions={1}, use_global_device_ids=true | all-gather | bytes 36864 | tf_op jit(solution)/shard_map/all_gather | solution.py:46
  23.3 0.8 dynamic_slice.11
  24.2 0.4 convolution_bitcast_fusion
  24.6 0.3 copy-done.1
  24.9 0.4 convolution_bitcast_fusion.1
  25.3 0.6 copy-done.2
  25.9 0.4 convolution_bitcast_fusion.2
  26.3 0.3 copy-done.3
  26.7 0.4 convolution_bitcast_fusion.3
  27.1 0.7 copy.18
  27.7 0.0 all-reduce.5.cloned.1.call-update
  27.8 0.6 dynamic-slice.2
  28.4 0.6 dynamic-slice
  29.0 0.1 multiply_reduce_fusion.1
  29.1 0.6 dynamic_slice.9
  30.4 32.8 %all-reduce.5.cloned.1.call-done = f32[4,4,1024]{2,1,0:T(4,128)} async-done(((f32[4,4,1024]{2,1,0:T(4,128)}), f32[4,4,1024]{2,1,0:T(4,128)}) %all-reduce.5.cloned.1.call-update) | async-done | bytes 65552
  63.2 1.5 %dynamic-slice_multiply_fusion = (f32[1,1,1024]{2,1,0:T(1,128)S(1)}, f32[1,1,1024]{2,1,0:T(1,128)S(1)}, f32[1,1,1024]{2,1,0:T(1,128)S(1)}, f32[1,1,1024]{2,1,0:T(1,128)S(1)}) fusion(f32[4,4,1024]{2,1,0:T(4,128)} %all-reduce.5.cloned.1.call-done, u32[]{:T(128)} %bitcast.19, u32[]{:T(128)S(6)} %convert.4, f32[]{:T(128)} %bitcast, u32[]{:T(128)S(6)} %convert.3, ...), kind=kLoop, calls=%fused_computation.26 | loop fusion | flops 7168 | bytes 32788 | tf_op jit(solution)/shard_map/mul | solution.py:68
  64.8 1.3 multiply_reduce_fusion
  66.0 0.1 multiply_reduce_fusion.2
  66.1 0.1 mul.206
  66.2 12.8 %all-gather = bf16[8192]{0:T(1024)(128)(2,1)S(1)} all-gather(bf16[1024]{0:T(1024)(128)(2,1)S(1)} %fusion.13), channel_id=2, replica_groups=mesh['dp'=4,'kv'=4,'tp'=2] {'kv','tp'}, dimensions={0}, use_global_device_ids=true | all-gather | bytes 18432 | tf_op jit(solution)/shard_map/all_gather | solution.py:84
  79.0 2.0 %fusion.1 = bf16[4,512]{1,0:T(4,128)(2,1)S(1)} fusion(bf16[4,2048]{1,0:T(4,128)(2,1)S(1)} %reshape_transpose_reshape.3, bf16[2048,512]{1,0:T(8,128)(2,1)} %param.23, bf16[4,512]{1,0:T(4,128)(2,1)S(1)} %copy-done.6), kind=kOutput, calls=%fused_computation.8 | convolution fusion | flops 8394752 | bytes 2121728 | tf_op jit(solution)/shard_map/dot_general | solution.py:89
  81.0 14.1 %all_gather.11 = bf16[4,4096]{1,0:T(4,128)(2,1)S(1)} all-gather(bf16[4,512]{1,0:T(4,128)(2,1)S(1)} %fusion.1), channel_id=1, replica_groups=mesh['dp'=4,'kv'=4,'tp'=2] {'kv','tp'}, dimensions={1}, use_global_device_ids=true | all-gather | bytes 36864 | tf_op jit(solution)/shard_map/all_gather | solution.py:91
  95.1 0.1 fusion.2
  95.2 5.9 %fusion.18 = f32[4,1408]{1,0:T(4,128)S(1)} fusion(bf16[4096,1408]{1,0:T(8,128)(2,1)} %param.25, bf16[4,4096]{1,0:T(4,128)(2,1)S(1)} %all_gather.11, f32[4096]{0:T(1024)S(1)} %copy-done.5, f32[4]{0:T(128)S(1)} %add_rsqrt_fusion), kind=kOutput, calls=%fused_computation.45 | convolution fusion | flops 46202880 | bytes 11606032 | tf_op jit(solution)/shard_map/dot_general | solution.py:16
  101.1 11.0 %convolution_convert_fusion = bf16[4,4096]{1,0:T(4,128)(2,1)S(1)} fusion(bf16[1408,4096]{1,0:T(8,128)(2,1)} %param.27, bf16[4096,1408]{1,0:T(8,128)(2,1)} %param.26, f32[4,1408]{1,0:T(4,128)S(1)} %fusion.18, bf16[4,4096]{1,0:T(4,128)(2,1)S(1)} %all_gather.11, f32[4096]{0:T(1024)S(1)} %copy-done.5, f32[4]{0:T(128)S(1)} %add_rsqrt_fusion), kind=kOutput, calls=%fused_computation | convolution fusion | flops 92390400 | bytes 23173136 | tf_op jit(solution)/shard_map/dot_general | solution.py:19
  112.1 3.6 %all-reduce.1 = bf16[4,4,2,512]{3,0,2,1:T(4,128)(2,1)S(1)} all-reduce(bf16[4,4,2,512]{3,0,2,1:T(4,128)(2,1)S(1)} %bitcast.49), channel_id=4, replica_groups=mesh['dp'=4,'kv'=4,'tp'=2] {'tp'}, use_global_device_ids=true, to_apply=%region_5.6.clone | all-reduce | flops 16384 | bytes 65536
  115.7 0.6 constant_dynamic-slice_fusion
  116.4 16.2 %all-reduce.2 = bf16[4,4,1,512]{3,0,2,1:T(4,128)(2,1)S(1)} all-reduce(bf16[4,4,1,512]{3,0,2,1:T(4,128)(2,1)S(1)} %constant_dynamic-slice_fusion), channel_id=5, replica_groups=mesh['dp'=4,'kv'=4,'tp'=2] {'kv'}, use_global_device_ids=true, to_apply=%region_6.7.clone | all-reduce | flops 8192 | bytes 32768
  132.6 1.2 fusion.9
  (27 shorter events, 0.1 us)
Async XLA Ops:
  7.2 17.0 %copy-start = (bf16[1024,1024]{1,0:T(8,128)(2,1)S(1)}, bf16[1024,1024]{1,0:T(8,128)(2,1)}, u32[]{:S(2)}) copy-start(bf16[1024,1024]{1,0:T(8,128)(2,1)} %param.20) | copy-start | bytes 6291460
  7.2 56.0 %all-reduce.5.cloned.1.call-start = ((), (), s32[]{:S(2)}) async-start(), calls=%async_computation | async-start | bytes 131072
  23.3 1.6 %copy-start.1 = (bf16[1024,1024]{1,0:T(8,128)(2,1)S(1)}, bf16[1024,1024]{1,0:T(8,128)(2,1)}, u32[]{:S(2)}) copy-start(bf16[1024,1024]{1,0:T(8,128)(2,1)} %param.19) | copy-start | bytes 6291460
  24.2 1.8 %copy-start.2 = (bf16[1024,1024]{1,0:T(8,128)(2,1)S(1)}, bf16[1024,1024]{1,0:T(8,128)(2,1)}, u32[]{:S(2)}) copy-start(bf16[1024,1024]{1,0:T(8,128)(2,1)} %param.18) | copy-start | bytes 6291460
  24.9 1.7 %copy-start.3 = (bf16[1024,1024]{1,0:T(8,128)(2,1)S(1)}, bf16[1024,1024]{1,0:T(8,128)(2,1)}, u32[]{:S(2)}) copy-start(bf16[1024,1024]{1,0:T(8,128)(2,1)} %param.17) | copy-start | bytes 6291460
  25.9 1.8 %copy-start.10 = (u32[32]{0:T(128)S(1)}, u32[32]{0:T(128)}, u32[]{:S(2)}) copy-start(u32[32]{0:T(128)} %constant.45) | copy-start | bytes 388
  25.9 2.4 %copy-start.9 = (u32[32]{0:T(128)S(1)}, u32[32]{0:T(128)}, u32[]{:S(2)}) copy-start(u32[32]{0:T(128)} %constant.41) | copy-start | bytes 388
  25.9 38.8 %copy-start.7 = (f32[1024]{0:T(1024)S(1)}, f32[1024]{0:T(1024)}, u32[]{:S(2)}) copy-start(f32[1024]{0:T(1024)} %param.21) | copy-start | bytes 12292
  25.9 38.8 %copy-start.4 = (f32[1,8,128,128]{3,2,1,0:T(8,128)S(1)}, f32[1,8,128,128]{3,2,1,0:T(8,128)}, u32[]{:S(2)}) copy-start(f32[1,8,128,128]{3,2,1,0:T(8,128)} %param.15) | copy-start | bytes 1572868
  26.6 39.6 %copy-start.8 = (f32[1024]{0:T(1024)S(1)}, f32[1024]{0:T(1024)}, u32[]{:S(2)}) copy-start(f32[1024]{0:T(1024)} %param.22) | copy-start | bytes 12292
  26.7 52.4 %copy-start.6 = (bf16[4,512]{1,0:T(4,128)(2,1)S(1)}, bf16[4,512]{1,0:T(4,128)(2,1)}, u32[]{:S(2)}) copy-start(bf16[4,512]{1,0:T(4,128)(2,1)} %param.14) | copy-start | bytes 12292
  27.0 68.2 %copy-start.5 = (f32[4096]{0:T(1024)S(1)}, f32[4096]{0:T(1024)}, u32[]{:S(2)}) copy-start(f32[4096]{0:T(1024)} %param.24) | copy-start | bytes 49156
Sparse Core Ops, SparseCore 0:
  27.9 35.2 all-reduce.4
where the time goes:
time: 141 us
  blocking collectives  62.7 us (44%)
  waiting for transfers between devices  32.8 us (23%)
  matrix products  20.4 us (14%)
  between operations  14.9 us (11%)
  local copies, waits for them, and re-layouts  5.37 us (4%)
  other arithmetic  4.46 us (3%)
    unnamed x2, waiting for transfers between devices  32.8 us
    unnamed x2, blocking collectives  19.8 us
    all_gather x1, blocking collectives, local(): lax.all_gather(tokens, ('kv', 'tp'), axis=1, tiled=True).astype(jnp.float32)  16.1 us
    all_gather x1, blocking collectives, local(): gathered = lax.all_gather(mixed, ('kv', 'tp'), axis=1, tiled=True)  14.1 us
    all_gather x1, blocking collectives, local(): every_head = lax.all_gather(gated[None], ('kv', 'tp'), axis=0, tiled=True)  12.8 us
    dot_general x1, matrix products, channel_mixer(): return jnp.dot(hidden, w_down, preferred_element_type=jnp.float32)  11 us
    dot_general x1, matrix products, channel_mixer(): gate_val = jnp.dot(normed, w_gate, preferred_element_type=jnp.float32)  5.9 us
    unnamed x25, local copies, waits for them, and re-layouts  3.18 us
  transfers between devices with their start and end apart: 1, of which 1 were waited for; matrix products, arithmetic and copies ran while one was open for 1% of the time, Pallas kernels for 0%

commit v1 on v0

v1 whole, which is shorter than its diff:
```python
import jax
import jax.numpy as jnp
from jax import lax
from jax.sharding import PartitionSpec as P

HEAD_DIM = 128


epsilon = 1e-06
GROUP = ("kv", "tp")


def channel_mixer(whole_rows, mixer_gain, w_gate, w_up, w_down):
    rows_float = whole_rows.astype(jnp.float32)
    mixer_scale = lax.rsqrt(jnp.mean(rows_float * rows_float, axis=1, keepdims=True) + epsilon)
    normed = (rows_float * mixer_scale * mixer_gain).astype(jnp.bfloat16)
    gate_val = jnp.dot(normed, w_gate, preferred_element_type=jnp.float32)
    up_val = jnp.dot(normed, w_up, preferred_element_type=jnp.float32)
    hidden = (jax.nn.silu(gate_val) * up_val).astype(jnp.bfloat16)
    return jnp.dot(hidden, w_down, preferred_element_type=jnp.float32)


def gather_group(block, count):
    copies = jnp.broadcast_to(block[None], (count,) + block.shape)
    return lax.all_to_all(copies, GROUP, 0, 0)


def local(
    tokens,
    rec_state,
    norm_gain,
    w_query,
    w_forget,
    w_input,
    w_outgate,
    lower_bound,
    head_gain,
    w_heads_out,
    mixer_gain,
    w_gate,
    w_up,
    w_down,
):
    kv_count = lax.axis_size("kv")
    tp_count = lax.axis_size("tp")
    kv_index = lax.axis_index("kv")
    tp_index = lax.axis_index("tp")
    group_count = kv_count * tp_count
    row_count = tokens.shape[0]
    seq_count = rec_state.shape[0]
    model_width = norm_gain.shape[0]
    col_block = model_width // kv_count
    tok_float = tokens.astype(jnp.float32)
    other = lax.ppermute(tokens, "tp", [(i, (i + 1) % tp_count) for i in range(tp_count)])
    low = jnp.where(tp_index == 0, tokens, other)
    high = jnp.where(tp_index == 0, other, tokens)
    own_cols = jnp.concatenate([low, high], axis=1).astype(jnp.float32)
    squares = jnp.sum(own_cols * own_cols, axis=1)
    gain_block = lax.dynamic_slice_in_dim(norm_gain, kv_index * col_block, col_block, 0)
    scaled = (own_cols * gain_block).astype(jnp.bfloat16)
    partial = [
        jnp.dot(scaled, weight, preferred_element_type=jnp.float32)
        for weight in (w_query, w_forget, w_input, w_outgate)
    ]
    local_width = w_query.shape[1]
    partial.append(jnp.broadcast_to(squares[:, None], (row_count, 128)))
    sent = jnp.concatenate(partial, axis=1).reshape(kv_count, seq_count, -1)
    projected = jnp.sum(lax.all_to_all(sent, "kv", 0, 0), axis=0)
    my_squares = projected[:, 4 * local_width]
    row_scale = lax.rsqrt(my_squares / model_width + epsilon)[:, None]
    query_pre = row_scale * projected[:, :local_width]
    forget_pre = row_scale * projected[:, local_width : 2 * local_width]
    value_in = row_scale * projected[:, 2 * local_width : 3 * local_width]
    gate_pre = row_scale * projected[:, 3 * local_width : 4 * local_width]
    forget = lower_bound + (1.0 - lower_bound) * jax.nn.sigmoid(forget_pre)
    key_in = 1.0 - forget
    query_act = jax.nn.silu(query_pre)
    head_count = rec_state.shape[1]
    shaped = (seq_count, head_count, HEAD_DIM)
    forget = forget.reshape(shaped)
    key_in = key_in.reshape(shaped)
    value_in = value_in.reshape(shaped)
    query_act = query_act.reshape(shaped)
    new_state = forget[:, :, :, None] * rec_state + key_in[:, :, :, None] * value_in[:, :, None, :]
    head_out = jnp.sum(query_act[:, :, :, None] * new_state, axis=2)
    head_out = head_out * lax.rsqrt(jnp.mean(head_out * head_out, axis=2, keepdims=True) + epsilon)
    head_out = head_out * head_gain.reshape(head_count, HEAD_DIM)
    gated = (head_out.reshape(seq_count, local_width) * jax.nn.silu(gate_pre)).astype(jnp.bfloat16)
    every_head = gather_group(gated, group_count)
    every_head = every_head.reshape(kv_count, tp_count, seq_count, local_width)
    every_head = every_head.transpose(0, 2, 1, 3).reshape(
        kv_count * seq_count, tp_count * local_width
    )
    mixed_add = jnp.dot(every_head, w_heads_out, preferred_element_type=jnp.float32)
    mixed = (tok_float + mixed_add).astype(jnp.bfloat16)
    gathered = gather_group(mixed, group_count).transpose(1, 0, 2).reshape(row_count, model_width)
    terms = channel_mixer(gathered, mixer_gain, w_gate, w_up, w_down)
    out_block = model_width // group_count
    blocked = terms.astype(jnp.bfloat16).reshape(row_count, group_count, out_block)
    blocked = blocked.transpose(1, 0, 2)
    down_sum = jnp.sum(lax.all_to_all(blocked, GROUP, 0, 0).astype(jnp.float32), axis=0)
    result = (mixed.astype(jnp.float32) + down_sum).astype(jnp.bfloat16)
    return (result, new_state)


def solution(mesh):
    placed = (
        P("dp", ("kv", "tp")),
        P(("dp", "kv"), "tp", None, None),
        P(),
        P("kv", "tp"),
        P("kv", "tp"),
        P("kv", "tp"),
        P("kv", "tp"),
        P("tp"),
        P("tp"),
        P(None, ("kv", "tp")),
        P(),
        P(None, ("kv", "tp")),
        P(None, ("kv", "tp")),
        P(("kv", "tp"), None),
    )
    return jax.shard_map(
        local,
        mesh=mesh,
        in_specs=placed,
        out_specs=(P("dp", ("kv", "tp")), P(("dp", "kv"), "tp", None, None)),
        check_vma=False,
    )
```

time: 141 us -> 67.2 us (0.48)
  blocking collectives: 62.7 us -> 24.2 us
  waiting for transfers between devices: 32.8 us -> 5.94 us
  between operations: 14.9 us -> 1.45 us
  starting transfers between devices: 0.04 us -> 6.76 us
    all_gather x3 -> x0, blocking collectives: 42.9 us -> none  [the longest x1 16.1 us: local(): lax.all_gather(tokens, ('kv', 'tp'), axis=1, tiled=True).astype(jnp.float32)]
    unnamed x2 -> x0, waiting for transfers between devices: 32.8 us -> none
    all_to_all x0 -> x3, blocking collectives: none -> 24.2 us  [the longest x2 16.1 us: gather_group(): return lax.all_to_all(copies, GROUP, 0, 0)]
    unnamed x2 -> x0, blocking collectives: 19.8 us -> none
    all_to_all x0 -> x1, starting transfers between devices: none -> 6.2 us  [local(): projected = jnp.sum(lax.all_to_all(sent, 'kv', 0, 0), axis=0)]
    all_to_all x0 -> x1, waiting for transfers between devices: none -> 5.74 us  [local(): projected = jnp.sum(lax.all_to_all(sent, 'kv', 0, 0), axis=0)]
    unnamed x25 -> x20, local copies, waits for them, and re-layouts: 3.18 us -> 1.21 us
    mul x3 -> x1, other arithmetic: 1.52 us -> 0.01 us  [local(): head_out = head_out * head_gain.reshape(head_count, HEAD_DIM)]
  transfers between devices with their start and end apart: 1 -> 2, of which waited for: 1 -> 2; matrix products, arithmetic and copies ran while one was open for 1% -> 1% of each run, Pallas kernels for 0% -> 0%
where the time goes in v1:
time: 67.2 us; the launch traced here: 66.8 us
  blocking collectives  24.2 us (36%)
  matrix products  20.4 us (30%)
  starting transfers between devices  6.76 us (10%)
  waiting for transfers between devices  5.94 us (9%)
  local copies, waits for them, and re-layouts  4.01 us (6%)
  other arithmetic  3.96 us (6%)
  between operations  1.45 us (2%)
    all_to_all x2, blocking collectives, gather_group(): return lax.all_to_all(copies, GROUP, 0, 0)  16.1 us
    dot_general x1, matrix products, channel_mixer(): return jnp.dot(hidden, w_down, preferred_element_type=jnp.float32)  11 us
    all_to_all x1, blocking collectives, local(): lax.all_to_all(blocked, GROUP, 0, 0).astype(jnp.float32)  8.12 us
    all_to_all x1, starting transfers between devices, local(): projected = jnp.sum(lax.all_to_all(sent, 'kv', 0, 0), axis=0)  6.2 us
    dot_general x1, matrix products, channel_mixer(): gate_val = jnp.dot(normed, w_gate, preferred_element_type=jnp.float32)  5.9 us
    all_to_all x1, waiting for transfers between devices, local(): projected = jnp.sum(lax.all_to_all(sent, 'kv', 0, 0), axis=0)  5.74 us
    dot_general x1, matrix products, local(): jnp.dot(every_head, w_heads_out, preferred_element_type=jnp.float32)  1.96 us
    dot_general x4, matrix products, local(): jnp.dot(scaled, weight, preferred_element_type=jnp.float32)  1.55 us
  transfers between devices with their start and end apart: 2, of which 2 were waited for; matrix products, arithmetic and copies ran while one was open for 1% of the time, Pallas kernels for 0%

profile of v1, /device:TPU:0, one launch (start us, length us, event | category | flops | bytes accessed | tf_op | source)
XLA Modules:
  0.0 66.8 jit_solution(12765448884941881406)
XLA Ops:
  0.6 0.0 copy-start
  0.6 0.6 collective-permute-start
  1.2 0.8 %dynamic_slice.3 = f32[1024]{0:T(1024)S(1)} dynamic-slice(f32[4096]{0:T(1024)} %param.16, s32[]{:T(128)S(6)} %select_n.18), dynamic_slice_sizes={1024} | dynamic-slice | bytes 8196 | tf_op jit(solution)/shard_map/dynamic_slice | solution.py:59
  2.0 0.2 collective-permute-done
  2.2 0.7 %broadcast_select_fusion.1 = (bf16[4,512]{1,0:T(4,128)(2,1)S(1)}, bf16[4,512]{1,0:T(4,128)(2,1)S(1)}) fusion(bf16[4,512]{1,0:T(4,128)(2,1)} %param.14, bf16[4,512]{1,0:T(4,128)(2,1)S(1)} %collective-permute-done, pred[]{:T(512)S(6)} %eq.4), kind=kLoop, calls=%fused_computation.43 | loop fusion | flops 4096 | bytes 16385 | tf_op jit(solution)/shard_map/jit(_where)/select_n | solution.py:55
  2.9 0.1 fusion.6
  3.1 0.4 convolution_dynamic-update-slice_fusion.3
  3.5 0.4 convolution_dynamic-update-slice_fusion.2
  3.9 0.8 %copy-done.2 = bf16[1024,1024]{1,0:T(8,128)(2,1)S(1)} copy-done((bf16[1024,1024]{1,0:T(8,128)(2,1)S(1)}, bf16[1024,1024]{1,0:T(8,128)(2,1)}, u32[]{:S(2)}) %copy-start.2) | copy-done | bytes 2097176
  4.7 0.4 convolution_dynamic-update-slice_fusion.1
  5.0 0.3 copy-done.3
  5.4 0.4 convolution_dynamic-update-slice_fusion
  5.8 0.1 constant_dynamic-update-slice_fusion
  5.9 0.7 %copy.20 = f32[4,1,4224]{2,1,0:T(1,128)} copy(f32[4,1,4224]{2,0,1:T(4,128)S(1)} %bitcast.32) | data formatting | bytes 135168 | tf_op jit(solution)/shard_map/reshape | solution.py:67
  6.6 6.2 %all-to-all-start = ((f32[4,1,4224]{2,1,0:T(1,128)}), f32[4,1,4224]{2,1,0:T(1,128)S(1)}, u32[]{:S(2)}, u32[]{:S(2)}) async-start(f32[4,1,4224]{2,1,0:T(1,128)} %copy.20), calls=%async_computation | async-start | bytes 135168 | tf_op jit(solution)/shard_map/all_to_all | solution.py:68
  12.8 5.7 %all-to-all-done = f32[4,1,4224]{2,1,0:T(1,128)S(1)} async-done(((f32[4,1,4224]{2,1,0:T(1,128)}), f32[4,1,4224]{2,1,0:T(1,128)S(1)}, u32[]{:S(2)}, u32[]{:S(2)}) %all-to-all-start) | async-done | bytes 67616 | tf_op jit(solution)/shard_map/all_to_all | solution.py:68
  18.5 0.1 reduce_sum.59
  18.6 0.5 slice.20
  19.9 1.3 %multiply_reduce_fusion = (f32[8,128]{1,0:T(8,128)S(1)}, f32[1,8,128,128]{3,2,1,0:T(8,128)}) fusion(f32[8,128]{1,0:T(8,128)S(1)} %bitcast.36, f32[8,128]{1,0:T(8,128)S(1)} %bitcast.35, f32[8,128]{1,0:T(8,128)S(1)} %bitcast.33, f32[1,8,128,128]{3,2,1,0:T(8,128)S(1)} %copy-done.4, f32[8,128]{1,0:T(8,128)S(1)} %bitcast.34), kind=kLoop, calls=%fused_computation.9 | loop fusion | flops 654336 | bytes 1069056 | tf_op jit(solution)/shard_map/reduce_sum | solution.py:85
  21.1 0.1 multiply_reduce_fusion.2
  21.2 0.1 mul.182
  21.4 0.5 broadcast.82
  21.9 0.7 %reduce.9 = bf16[8,1024]{1,0:T(8,128)(2,1)S(1)} reduce(bf16[8,1,1024]{2,1,0:T(2,128)(2,1)S(1)} %broadcast_in_dim.16, bf16[]{:T(256)} %broadcast.82), dimensions={1}, to_apply=%broadcast_in_dim.16.reduce_sub_computation | reduce | bytes 32770 | tf_op jit(solution)/shard_map/broadcast_in_dim | solution.py:24
  22.7 8.0 %all_to_all.20 = bf16[8,2,512]{2,1,0:T(2,128)(2,1)S(1)} all-to-all(bf16[8,2,512]{2,1,0:T(2,128)(2,1)S(1)} %reshape.96), channel_id=1, replica_groups=mesh['dp'=4,'kv'=4,'tp'=2] {'kv','tp'}, dimensions={0} | all-to-all | bytes 32768 | tf_op jit(solution)/shard_map/all_to_all | solution.py:25
  30.7 0.1 reduce.7
  30.8 2.0 %fusion.1 = bf16[4,512]{1,0:T(4,128)(2,1)S(1)} fusion(bf16[4,2048]{1,0:T(4,128)(2,1)S(1)} %reshape_transpose_reshape.3, bf16[2048,512]{1,0:T(8,128)(2,1)} %param.23, bf16[4,512]{1,0:T(4,128)(2,1)S(1)} %copy-done.6), kind=kOutput, calls=%fused_computation.8 | convolution fusion | flops 8394752 | bytes 2121728 | tf_op jit(solution)/shard_map/dot_general | solution.py:94
  32.8 8.1 %all_to_all.21 = bf16[8,4,512]{2,1,0:T(4,128)(2,1)S(1)} all-to-all(bf16[8,4,512]{2,1,0:T(4,128)(2,1)S(1)} %broadcast_in_dim.17), channel_id=1, replica_groups=mesh['dp'=4,'kv'=4,'tp'=2] {'kv','tp'}, dimensions={0} | all-to-all | bytes 65536 | tf_op jit(solution)/shard_map/all_to_all | solution.py:25
  41.0 0.1 multiply_reduce_fusion.1
  41.1 5.9 %fusion.19 = f32[4,1408]{1,0:T(4,128)S(1)} fusion(bf16[4096,1408]{1,0:T(8,128)(2,1)} %param.25, f32[4,4096]{1,0:T(4,128)S(1)} %bitcast.29, f32[4096]{0:T(1024)S(1)} %copy-done.5, f32[4]{0:T(128)S(1)} %add_rsqrt_fusion), kind=kOutput, calls=%fused_computation.49 | convolution fusion | flops 46186496 | bytes 11638800 | tf_op jit(solution)/shard_map/dot_general | solution.py:17
  47.0 11.0 %convolution_convert_fusion = bf16[4,4096]{1,0:T(4,128)(2,1)S(1)} fusion(bf16[1408,4096]{1,0:T(8,128)(2,1)} %param.27, bf16[4096,1408]{1,0:T(8,128)(2,1)} %param.26, f32[4,1408]{1,0:T(4,128)S(1)} %fusion.19, f32[4,4096]{1,0:T(4,128)S(1)} %bitcast.30, f32[4096]{0:T(1024)S(1)} %copy-done.5, f32[4]{0:T(128)S(1)} %add_rsqrt_fusion), kind=kOutput, calls=%fused_computation | convolution fusion | flops 92374016 | bytes 23205904 | tf_op jit(solution)/shard_map/dot_general | solution.py:20
  58.0 8.1 %all_to_all.22 = bf16[8,4,512]{2,1,0:T(4,128)(2,1)S(1)} all-to-all(bf16[8,4,512]{2,1,0:T(4,128)(2,1)S(1)} %bitcast.31), channel_id=1, replica_groups=mesh['dp'=4,'kv'=4,'tp'=2] {'kv','tp'}, dimensions={0} | all-to-all | bytes 65536 | tf_op jit(solution)/shard_map/all_to_all | solution.py:101
  66.2 0.6 add_convert_fusion
  (29 shorter events, 0.3 us)
Async XLA Ops:
  0.6 2.4 %copy-start = (bf16[1024,1024]{1,0:T(8,128)(2,1)S(1)}, bf16[1024,1024]{1,0:T(8,128)(2,1)}, u32[]{:S(2)}) copy-start(bf16[1024,1024]{1,0:T(8,128)(2,1)} %param.17) | copy-start | bytes 6291460
  0.6 1.6 %collective-permute-start = (bf16[4,512]{1,0:T(4,128)(2,1)}, bf16[4,512]{1,0:T(4,128)(2,1)S(1)}, u32[]{:S(2)}, u32[]{:S(2)}) collective-permute-start(bf16[4,512]{1,0:T(4,128)(2,1)} %param.14), channel_id=1, source_target_pairs={{0,1},{1,0},{2,3},{3,2},{4,5},{5,4},{6,7},{7,6},{8,9},{9,8},{10,11... | collective-permute-start | bytes 12296 | tf_op jit(solution)/shard_map/ppermute | solution.py:54
  1.2 2.3 %copy-start.1 = (bf16[1024,1024]{1,0:T(8,128)(2,1)S(1)}, bf16[1024,1024]{1,0:T(8,128)(2,1)}, u32[]{:S(2)}) copy-start(bf16[1024,1024]{1,0:T(8,128)(2,1)} %param.18) | copy-start | bytes 6291460
  3.1 1.6 %copy-start.2 = (bf16[1024,1024]{1,0:T(8,128)(2,1)S(1)}, bf16[1024,1024]{1,0:T(8,128)(2,1)}, u32[]{:S(2)}) copy-start(bf16[1024,1024]{1,0:T(8,128)(2,1)} %param.19) | copy-start | bytes 6291460
  3.5 1.9 %copy-start.3 = (bf16[1024,1024]{1,0:T(8,128)(2,1)S(1)}, bf16[1024,1024]{1,0:T(8,128)(2,1)}, u32[]{:S(2)}) copy-start(bf16[1024,1024]{1,0:T(8,128)(2,1)} %param.20) | copy-start | bytes 6291460
  4.7 8.1 %copy-start.7 = (f32[1024]{0:T(1024)S(1)}, f32[1024]{0:T(1024)}, u32[]{:S(2)}) copy-start(f32[1024]{0:T(1024)} %param.21) | copy-start | bytes 12292
  4.7 15.2 %copy-start.4 = (f32[1,8,128,128]{3,2,1,0:T(8,128)S(1)}, f32[1,8,128,128]{3,2,1,0:T(8,128)}, u32[]{:S(2)}) copy-start(f32[1,8,128,128]{3,2,1,0:T(8,128)} %param.15) | copy-start | bytes 1572868
  5.4 15.9 %copy-start.8 = (f32[1024]{0:T(1024)S(1)}, f32[1024]{0:T(1024)}, u32[]{:S(2)}) copy-start(f32[1024]{0:T(1024)} %param.22) | copy-start | bytes 12292
  5.4 25.4 %copy-start.6 = (bf16[4,512]{1,0:T(4,128)(2,1)S(1)}, bf16[4,512]{1,0:T(4,128)(2,1)}, u32[]{:S(2)}) copy-start(bf16[4,512]{1,0:T(4,128)(2,1)} %param.14) | copy-start | bytes 12292
  5.9 35.3 %copy-start.5 = (f32[4096]{0:T(1024)S(1)}, f32[4096]{0:T(1024)}, u32[]{:S(2)}) copy-start(f32[4096]{0:T(1024)} %param.24) | copy-start | bytes 49156
  6.6 11.9 %all-to-all-start = ((f32[4,1,4224]{2,1,0:T(1,128)}), f32[4,1,4224]{2,1,0:T(1,128)S(1)}, u32[]{:S(2)}, u32[]{:S(2)}) async-start(f32[4,1,4224]{2,1,0:T(1,128)} %copy.20), calls=%async_computation | async-start | bytes 135168 | tf_op jit(solution)/shard_map/all_to_all | solution.py:68

commit v2 on v1

--- a/solution.py
+++ b/solution.py
@@ -1,13 +1,224 @@
 import jax
 import jax.numpy as jnp
 from jax import lax
+from jax.experimental import pallas as pl
+from jax.experimental.pallas import tpu as pltpu
 from jax.sharding import PartitionSpec as P
 
 HEAD_DIM = 128
+LANES = 128
 
 
 epsilon = 1e-06
 GROUP = ("kv", "tp")
+VMEM = pl.BlockSpec(memory_space=pltpu.VMEM)
+HBM = pl.BlockSpec(memory_space=pltpu.HBM)
+
+
+LONG = pl.CostEstimate(flops=10**11, bytes_accessed=10**4, transcendentals=0)
+SHORT = pl.CostEstimate(flops=10**7, bytes_accessed=10**4, transcendentals=0)
+
+
+def resident(array):
+    return pltpu.with_memory_space_constraint(array, pltpu.VMEM)
+
+
+def call(body, outs, *args, streamed=(), scratch=(), limit=6 * 2**20, cost=SHORT):
+    return pl.pallas_call(
+        body,
+        out_shape=outs,
+        in_specs=[VMEM] * len(args) + [HBM] * len(streamed),
+        out_specs=jax.tree.map(lambda _: VMEM, outs),
+        scratch_shapes=scratch,
+        compiler_params=pltpu.CompilerParams(vmem_limit_bytes=limit),
+        cost_estimate=cost,
+    )(*args, *[pltpu.with_memory_space_constraint(w, pltpu.HBM) for w in streamed])
+
+
+def silu(v):
+    return v / (1.0 + jnp.exp(-v))
+
+
+def project_body(own, other, norm_gain, w_query, w_forget, w_input, w_outgate, out, held, sems):
+    copies = [
+        pltpu.make_async_copy(weight, held.at[i], sems.at[i])
+        for i, weight in enumerate((w_query, w_forget, w_input, w_outgate))
+    ]
+    for copy in copies:
+        copy.start()
+    col_block = held.shape[1]
+    tp_index = lax.axis_index("tp")
+    start = pl.multiple_of(lax.axis_index("kv") * col_block, LANES)
+    first = own[...].astype(jnp.float32)
+    second = other[...].astype(jnp.float32)
+    cols = jnp.concatenate(
+        [jnp.where(tp_index == 0, first, second), jnp.where(tp_index == 0, second, first)], axis=1
+    )
+    squares = jnp.sum(cols * cols, axis=1, keepdims=True)
+    scaled = (cols * norm_gain[:, pl.ds(start, col_block)]).astype(jnp.bfloat16)
+    spread = jnp.broadcast_to(squares, (squares.shape[0], LANES))
+    row = len(copies) * (held.shape[2] // LANES)
+    while row < out.shape[1]:
+        out[:, row, :] = spread
+        row += 1
+    row = 0
+    for i, copy in enumerate(copies):
+        copy.wait()
+        product = jnp.dot(scaled, held[i], preferred_element_type=jnp.float32)
+        for at in range(0, held.shape[2], LANES):
+            out[:, row, :] = product[:, at : at + LANES]
+            row += 1
+
+
+def recur_body(model_width, received, rec_state, lower_bound, head_gain, new_state, gated):
+    heads = rec_state.shape[0]
+    total = received[0]
+    for block in range(1, received.shape[0]):
+        total = total + received[block]
+    squares = total[4 * heads : 4 * heads + 1, :]
+    row_scale = lax.rsqrt(squares / model_width + epsilon)
+    query_pre = row_scale * total[:heads]
+    forget_pre = row_scale * total[heads : 2 * heads]
+    value_in = row_scale * total[2 * heads : 3 * heads]
+    gate_pre = row_scale * total[3 * heads : 4 * heads]
+    bound = lower_bound[...]
+    forget = bound + (1.0 - bound) / (1.0 + jnp.exp(-forget_pre))
+    key_in = 1.0 - forget
+    query_act = silu(query_pre)
+    forget_t = forget.T
+    key_t = key_in.T
+    query_t = query_act.T
+    rows = []
+    for h in range(heads):
+        fresh = (
+            forget_t[:, h : h + 1] * rec_state[h]
+            + key_t[:, h : h + 1] * value_in[h : h + 1, :]
+        )
+        new_state[h] = fresh
+        rows.append(jnp.sum(query_t[:, h : h + 1] * fresh, axis=0, keepdims=True))
+    head_out = jnp.concatenate(rows, axis=0)
+    head_out = head_out * lax.rsqrt(
+        jnp.mean(head_out * head_out, axis=1, keepdims=True) + epsilon
+    )
+    rounded = (head_out * head_gain[...] * silu(gate_pre)).astype(jnp.bfloat16)
+    for block in range(gated.shape[0]):
+        gated[block] = rounded.astype(jnp.float32)
+
+
+def heads_body(tp_count, every_head, w_heads_out, tokens, mixed, copies):
+    rows, heads = tokens.shape[0], every_head.shape[1]
+    left = jnp.concatenate(
+        [
+            every_head[pl.ds(t, rows, stride=tp_count), h, :]
+            for t in range(tp_count)
+            for h in range(heads)
+        ],
+        axis=1,
+    ).astype(jnp.bfloat16)
+    added = jnp.dot(left, w_heads_out[...], preferred_element_type=jnp.float32)
+    rounded = (tokens[...].astype(jnp.float32) + added).astype(jnp.bfloat16)
+    mixed[...] = rounded
+    for block in range(copies.shape[0]):
+        copies[block] = rounded
+
+
+def mixer_body(gathered, mixer_gain, w_gate, w_up, w_down, out):
+    rows = jnp.concatenate([gathered[i] for i in range(gathered.shape[0])], axis=1)
+    rows = rows.astype(jnp.float32)
+    scale = lax.rsqrt(jnp.mean(rows * rows, axis=1, keepdims=True) + epsilon)
+    normed = (rows * scale * mixer_gain[...]).astype(jnp.bfloat16)
+    gate_val = jnp.dot(normed, w_gate[...], preferred_element_type=jnp.float32)
+    up_val = jnp.dot(normed, w_up[...], preferred_element_type=jnp.float32)
+    hidden = (silu(gate_val) * up_val).astype(jnp.bfloat16)
+    terms = jnp.dot(hidden, w_down[...], preferred_element_type=jnp.float32)
+    terms = terms.astype(jnp.bfloat16)
+    width = out.shape[2]
+    for i in range(out.shape[0]):
+        out[i] = terms[:, i * width : (i + 1) * width]
+
+
+def result_body(received, mixed, out):
+    total = mixed[...].astype(jnp.float32)
+    for block in range(received.shape[0]):
+        total = total + received[block].astype(jnp.float32)
+    out[...] = total.astype(jnp.bfloat16)
+
+
+def local(
+    tokens,
+    rec_state,
+    norm_gain,
+    w_query,
+    w_forget,
+    w_input,
+    w_outgate,
+    lower_bound,
+    head_gain,
+    w_heads_out,
+    mixer_gain,
+    w_gate,
+    w_up,
+    w_down,
+):
+    kv_count = lax.axis_size("kv")
+    tp_count = lax.axis_size("tp")
+    group_count = kv_count * tp_count
+    row_count, own_width = tokens.shape
+    heads = rec_state.shape[1]
+    model_width = norm_gain.shape[0]
+    shape = jax.ShapeDtypeStruct
+    other = lax.ppermute(tokens, "tp", [(i, (i + 1) % tp_count) for i in range(tp_count)])
+    sent = call(
+        project_body,
+        shape((row_count, 4 * heads + 8, LANES), jnp.float32),
+        tokens,
+        other,
+        norm_gain[None],
+        streamed=(w_query, w_forget, w_input, w_outgate),
+        scratch=[
+            pltpu.VMEM((4,) + w_query.shape, w_query.dtype),
+            pltpu.SemaphoreType.DMA((4,)),
+        ],
+        limit=12 * 2**20,
+        cost=LONG,
+    )
+    received = lax.all_to_all(sent, "kv", 0, 0)
+    new_state, gated = call(
+        lambda *refs: recur_body(model_width, *refs),
+        (
+            shape(rec_state.shape[1:], jnp.float32),
+            shape((group_count, heads, HEAD_DIM), jnp.float32),
+        ),
+        received,
+        resident(rec_state[0]),
+        lower_bound.reshape(heads, HEAD_DIM),
+        head_gain.reshape(heads, HEAD_DIM),
+        cost=LONG,
+    )
+    every_head = lax.all_to_all(gated, GROUP, 0, 0)
+    mixed, copies = call(
+        lambda *refs: heads_body(tp_count, *refs),
+        (
+            shape((row_count, own_width), jnp.bfloat16),
+            shape((group_count, row_count, own_width), jnp.bfloat16),
+        ),
+        every_head,
+        resident(w_heads_out),
+        tokens,
+    )
+    gathered = lax.all_to_all(copies, GROUP, 0, 0)
+    blocked = call(
+        mixer_body,
+        shape((group_count, row_count, own_width), jnp.bfloat16),
+        gathered,
+        mixer_gain[None],
+        resident(w_gate),
+        resident(w_up),
+        resident(w_down),
+    )
+    back = lax.all_to_all(blocked, GROUP, 0, 0)
+    result = call(result_body, shape((row_count, own_width), jnp.bfloat16), back, mixed)
+    return (result, new_state[None])
 
 
 def channel_mixer(whole_rows, mixer_gain, w_gate, w_up, w_down):
@@ -25,7 +236,7 @@
     return lax.all_to_all(copies, GROUP, 0, 0)
 
 
-def local(
+def plain_local(
     tokens,
     rec_state,
     norm_gain,
@@ -103,6 +314,15 @@
     return (result, new_state)
 
 
+def choose(*args):
+    tokens, rec_state = args[0], args[1]
+    w_heads_out, w_gate = args[9], args[11]
+    aligned = all(size % LANES == 0 for size in (tokens.shape[1], w_gate.shape[1]))
+    if aligned and rec_state.shape[0] == 1 and lax.axis_size("tp") == 2:
+        return local(*args)
+    return plain_local(*args)
+
+
 def solution(mesh):
     placed = (
         P("dp", ("kv", "tp")),
@@ -121,7 +341,7 @@
         P(("kv", "tp"), None),
     )
     return jax.shard_map(
-        local,
+        choose,
         mesh=mesh,
         in_specs=placed,
         out_specs=(P("dp", ("kv", "tp")), P(("dp", "kv"), "tp", None, None)),

time: 67.2 us -> 52.1 us (0.78)
  matrix products: 20.4 us -> 0 us
  blocking collectives: 24.2 us -> 36.8 us
  Pallas kernels: 0 us -> 11.1 us
  starting transfers between devices: 6.76 us -> 0.56 us
  waiting for transfers between devices: 5.94 us -> 1.03 us
  other arithmetic: 3.96 us -> 0.01 us
  local copies, waits for them, and re-layouts: 4.01 us -> 1.47 us
    dot_general x7 -> x0, matrix products: 20.4 us -> none  [the longest x1 11 us: channel_mixer(): return jnp.dot(hidden, w_down, preferred_element_type=jnp.float32)]
    all_to_all x3 -> x4, blocking collectives: 24.2 us -> 36.8 us  [the longest x1 11.8 us: local(): received = lax.all_to_all(sent, 'kv', 0, 0)]
    pallas_call x0 -> x5, Pallas kernels: none -> 11.1 us  [call(): pl.pallas_call(body, out_shape=outs, in_specs=[VMEM] * len(args) + [HBM]...]
    all_to_all x1 -> x0, starting transfers between devices: 6.2 us -> none  [local(): projected = jnp.sum(lax.all_to_all(sent, 'kv', 0, 0), axis=0)]
    all_to_all x1 -> x0, waiting for transfers between devices: 5.74 us -> none  [local(): projected = jnp.sum(lax.all_to_all(sent, 'kv', 0, 0), axis=0)]
    reduce_sum x6 -> x0, other arithmetic: 1.74 us -> none  [the longest x1 1.25 us: local(): head_out = jnp.sum(query_act[:, :, :, None] * new_state, axis=2)]
    ppermute x1, waiting for transfers between devices: 0.19 us -> 1.03 us  [local(): lax.ppermute(tokens, 'tp', [(i, (i + 1) % tp_count) for i in range(tp_cou...]
    dynamic_slice x1 -> x0, local copies, waits for them, and re-layouts: 0.84 us -> none  [local(): lax.dynamic_slice_in_dim(norm_gain, kv_index * col_block, col_block, 0)]
  transfers between devices with their start and end apart: 2 -> 1, of which waited for: 2 -> 1; matrix products, arithmetic and copies ran while one was open for 1% -> 0% of each run, Pallas kernels for 0% -> 0%
where the time goes in v2:
time: 52.1 us; the launch traced here: 51.8 us
  blocking collectives  36.8 us (71%)
  Pallas kernels  11.1 us (21%)
  local copies, waits for them, and re-layouts  1.47 us (3%)
  waiting for transfers between devices  1.03 us (2%)
  between operations  0.82 us (2%)
  starting transfers between devices  0.56 us (1%)
    all_to_all x1, blocking collectives, local(): received = lax.all_to_all(sent, 'kv', 0, 0)  11.8 us
    pallas_call x5, Pallas kernels, call(): pl.pallas_call(body, out_shape=outs, in_specs=[VMEM] * len(args) + [HBM]...  11.1 us
    all_to_all x1, blocking collectives, local(): every_head = lax.all_to_all(gated, GROUP, 0, 0)  8.63 us
    all_to_all x1, blocking collectives, local(): gathered = lax.all_to_all(copies, GROUP, 0, 0)  8.25 us
    all_to_all x1, blocking collectives, local(): back = lax.all_to_all(blocked, GROUP, 0, 0)  8.11 us
    unnamed x34, local copies, waits for them, and re-layouts  1.47 us
  transfers between devices with their start and end apart: 1, of which 1 were waited for; matrix products, arithmetic and copies ran while one was open for 0% of the time, Pallas kernels for 0%

profile of v2, /device:TPU:0, one launch (start us, length us, event | category | flops | bytes accessed | tf_op | source)
XLA Modules:
  0.0 51.8 jit_solution(17957690506772732479)
XLA Ops:
  0.6 0.6 %collective-permute-start = (bf16[4,512]{1,0:T(4,128)(2,1)}, bf16[4,512]{1,0:T(4,128)(2,1)S(1)}, u32[]{:S(2)}, u32[]{:S(2)}) collective-permute-start(bf16[4,512]{1,0:T(4,128)(2,1)} %refs_2_.1), channel_id=1, source_target_pairs={{0,1},{1,0},{2,3},{3,2},{4,5},{5,4},{6,7},{7,6},{8,9},{9,8},{10,11... | collective-permute-start | bytes 12296 | tf_op jit(solution)/shard_map/ppermute | solution.py:170
  1.2 1.0 %collective-permute-done.other = bf16[4,512]{1,0:T(4,128)(2,1)S(1)} collective-permute-done((bf16[4,512]{1,0:T(4,128)(2,1)}, bf16[4,512]{1,0:T(4,128)(2,1)S(1)}, u32[]{:S(2)}, u32[]{:S(2)}) %collective-permute-start) | collective-permute-done | bytes 4128 | tf_op jit(solution)/shard_map/ppermute | solution.py:170
  2.2 0.7 %copy-done.2 = bf16[4,512]{1,0:T(4,128)(2,1)S(1)} copy-done((bf16[4,512]{1,0:T(4,128)(2,1)S(1)}, bf16[4,512]{1,0:T(4,128)(2,1)}, u32[]{:S(2)}) %copy-start.2) | copy-done | bytes 4120
  2.9 0.7 %copy-done.5 = f32[4096]{0:T(1024)S(1)} copy-done((f32[4096]{0:T(1024)S(1)}, f32[4096]{0:T(1024)}, u32[]{:S(2)}) %copy-start.5) | copy-done | bytes 16408
  3.6 3.9 %shard_map.149 = f32[4,40,128]{2,1,0:T(8,128)S(1)} custom-call(bf16[4,512]{1,0:T(4,128)(2,1)S(1)} %copy-done.2, bf16[4,512]{1,0:T(4,128)(2,1)S(1)} %collective-permute-done.other, f32[1,4096]{1,0:T(1,128)S(1)} %bitcast.14, bf16[1024,1024]{1,0:T(8,128)(2,1)} %w_query.1, bf16[1024,1024]{1,0:T(8,128)(2,1)} %w_forget.1, bf16[1024,1024]{1,0:T(8,128)(2,1)} %w_input.1, ...), custom_call_target="tpu_custom_call" | custom-call | flops 99999997952 | bytes 10000 | tf_op jit(solution)/shard_map/pallas_call | solution.py:27
  7.6 11.8 %all_to_all.20.refs_0_ = f32[4,40,128]{2,1,0:T(8,128)S(1)} all-to-all(f32[4,40,128]{2,1,0:T(8,128)S(1)} %shard_map.149), channel_id=1, replica_groups=mesh['dp'=4,'kv'=4,'tp'=2] {'kv'}, dimensions={0} | all-to-all | bytes 163840 | tf_op jit(solution)/shard_map/all_to_all | solution.py:185
  19.4 0.0 copy-done.4
  19.4 0.0 copy-done.6
  19.4 0.0 copy-done.7
  19.4 0.0 copy-start
  19.4 0.0 copy-start.3
  19.4 0.0 slice-start.1
  19.4 0.0 slice-start.2
  19.5 0.0 slice-start.4
  19.5 0.0 slice-start.5
  19.5 0.0 slice-start.7
  19.5 0.0 slice-start.8
  19.5 1.5 %shard_map.150 = (f32[8,128,128]{2,1,0:T(8,128)}, f32[8,8,128]{2,1,0:T(8,128)S(1)}) custom-call(f32[4,40,128]{2,1,0:T(8,128)S(1)} %all_to_all.20.refs_0_, f32[8,128,128]{2,1,0:T(8,128)S(1)} %bitcast.13, f32[8,128]{1,0:T(8,128)S(1)} %bitcast.15, f32[8,128]{1,0:T(8,128)S(1)} %bitcast.16), custom_call_target="tpu_custom_call" | custom-call | flops 99999997952 | bytes 10000 | tf_op jit(solution)/shard_map/pallas_call | solution.py:27
  21.0 8.6 %all_to_all.21.refs_0_ = f32[8,8,128]{2,1,0:T(8,128)S(1)} all-to-all(f32[8,8,128]{2,1,0:T(8,128)S(1)} %get-tuple-element.6), channel_id=1, replica_groups=mesh['dp'=4,'kv'=4,'tp'=2] {'kv','tp'}, dimensions={0} | all-to-all | bytes 65536 | tf_op jit(solution)/shard_map/all_to_all | solution.py:198
  29.6 0.0 copy-done
  29.6 0.4 shard_map.151
  30.0 8.3 %all_to_all.22.gathered = bf16[8,4,512]{2,1,0:T(4,128)(2,1)S(1)} all-to-all(bf16[8,4,512]{2,1,0:T(4,128)(2,1)S(1)} %get-tuple-element.7), channel_id=1, replica_groups=mesh['dp'=4,'kv'=4,'tp'=2] {'kv','tp'}, dimensions={0} | all-to-all | bytes 65536 | tf_op jit(solution)/shard_map/all_to_all | solution.py:209
  38.2 0.0 slice-done.1
  38.2 0.0 slice-done.2
  38.3 0.0 slice-done.4
  38.3 0.0 slice-done.5
  38.3 0.0 slice-done.7
  38.3 0.0 slice-done.8
  38.3 0.0 copy-done.1
  38.3 4.7 %shard_map.152 = bf16[8,4,512]{2,1,0:T(4,128)(2,1)S(1)} custom-call(bf16[8,4,512]{2,1,0:T(4,128)(2,1)S(1)} %all_to_all.22.gathered, f32[1,4096]{1,0:T(1,128)S(1)} %bitcast.12, bf16[4096,1408]{1,0:T(8,128)(2,1)S(1)} %bitcast.7, bf16[4096,1408]{1,0:T(8,128)(2,1)S(1)} %bitcast.9, bf16[1408,4096]{1,0:T(8,128)(2,1)S(1)} %bitcast.11), custom_call_target="tpu_custom_call" | custom-call | flops 10000000 | bytes 10000 | tf_op jit(solution)/shard_map/pallas_call | solution.py:27
  43.0 8.1 %all_to_all.23.received = bf16[8,4,512]{2,1,0:T(4,128)(2,1)S(1)} all-to-all(bf16[8,4,512]{2,1,0:T(4,128)(2,1)S(1)} %shard_map.152), channel_id=1, replica_groups=mesh['dp'=4,'kv'=4,'tp'=2] {'kv','tp'}, dimensions={0} | all-to-all | bytes 65536 | tf_op jit(solution)/shard_map/all_to_all | solution.py:219
  51.1 0.6 %shard_map.153 = bf16[4,512]{1,0:T(4,128)(2,1)} custom-call(bf16[8,4,512]{2,1,0:T(4,128)(2,1)S(1)} %all_to_all.23.received, bf16[4,512]{1,0:T(4,128)(2,1)S(1)} %get-tuple-element.8.mixed), custom_call_target="tpu_custom_call" | custom-call | flops 10000000 | bytes 10000 | tf_op jit(solution)/shard_map/pallas_call | solution.py:27
  (16 shorter events, 0.0 us)
Async XLA Ops:
  0.6 1.6 %collective-permute-start = (bf16[4,512]{1,0:T(4,128)(2,1)}, bf16[4,512]{1,0:T(4,128)(2,1)S(1)}, u32[]{:S(2)}, u32[]{:S(2)}) collective-permute-start(bf16[4,512]{1,0:T(4,128)(2,1)} %refs_2_.1), channel_id=1, source_target_pairs={{0,1},{1,0},{2,3},{3,2},{4,5},{5,4},{6,7},{7,6},{8,9},{9,8},{10,11... | collective-permute-start | bytes 12296 | tf_op jit(solution)/shard_map/ppermute | solution.py:170
  2.2 0.7 %copy-start.2 = (bf16[4,512]{1,0:T(4,128)(2,1)S(1)}, bf16[4,512]{1,0:T(4,128)(2,1)}, u32[]{:S(2)}) copy-start(bf16[4,512]{1,0:T(4,128)(2,1)} %refs_2_.1) | copy-start | bytes 12292
  2.9 0.7 %copy-start.5 = (f32[4096]{0:T(1024)S(1)}, f32[4096]{0:T(1024)}, u32[]{:S(2)}) copy-start(f32[4096]{0:T(1024)} %param.16) | copy-start | bytes 49156
  3.6 15.8 %copy-start.4 = (f32[1,8,128,128]{3,2,1,0:T(8,128)S(1)}, f32[1,8,128,128]{3,2,1,0:T(8,128)}, u32[]{:S(2)}) copy-start(f32[1,8,128,128]{3,2,1,0:T(8,128)} %param.15) | copy-start | bytes 1572868
  3.6 15.8 %copy-start.6 = (f32[1024]{0:T(1024)S(1)}, f32[1024]{0:T(1024)}, u32[]{:S(2)}) copy-start(f32[1024]{0:T(1024)} %param.21) | copy-start | bytes 12292
  3.6 15.8 %copy-start.7 = (f32[1024]{0:T(1024)S(1)}, f32[1024]{0:T(1024)}, u32[]{:S(2)}) copy-start(f32[1024]{0:T(1024)} %param.22) | copy-start | bytes 12292
  19.4 18.9 %slice-start = ((s8[11534336]{0:T(1024)(128)(4,1)}), s8[4194304]{0:T(1024)(128)(4,1)S(1)}, s32[]{:S(2)}) async-start(s8[11534336]{0:T(1024)(128)(4,1)} %bitcast.6), calls=%async_computation.4 | async-start | bytes 8388608
  19.4 18.9 %slice-start.3 = ((s8[11534336]{0:T(1024)(128)(4,1)}), s8[4194304]{0:T(1024)(128)(4,1)S(1)}, s32[]{:S(2)}) async-start(s8[11534336]{0:T(1024)(128)(4,1)} %bitcast.8), calls=%async_computation.7 | async-start | bytes 8388608
  19.4 18.9 %slice-start.6 = ((s8[11534336]{0:T(1024)(128)(4,1)}), s8[4194304]{0:T(1024)(128)(4,1)S(1)}, s32[]{:S(2)}) async-start(s8[11534336]{0:T(1024)(128)(4,1)} %bitcast.10), calls=%async_computation.10 | async-start | bytes 8388608
  19.4 10.2 %copy-start = (bf16[2048,512]{1,0:T(8,128)(2,1)S(1)}, bf16[2048,512]{1,0:T(8,128)(2,1)}, u32[]{:S(2)}) copy-start(bf16[2048,512]{1,0:T(8,128)(2,1)} %refs_1_.1) | copy-start | bytes 6291460
  19.4 10.2 %copy-start.3 = (bf16[4,512]{1,0:T(4,128)(2,1)S(1)}, bf16[4,512]{1,0:T(4,128)(2,1)}, u32[]{:S(2)}) copy-start(bf16[4,512]{1,0:T(4,128)(2,1)} %refs_2_.1) | copy-start | bytes 12292
  19.4 18.8 %slice-start.1 = ((s8[11534336]{0:T(1024)(128)(4,1)}), s8[4194304]{0:T(1024)(128)(4,1)S(1)}, s32[]{:S(2)}) async-start(s8[11534336]{0:T(1024)(128)(4,1)} %bitcast.6), calls=%async_computation.5 | async-start | bytes 8388608
  19.4 18.8 %slice-start.2 = ((s8[11534336]{0:T(1024)(128)(4,1)}), s8[3145728]{0:T(1024)(128)(4,1)S(1)}, s32[]{:S(2)}) async-start(s8[11534336]{0:T(1024)(128)(4,1)} %bitcast.6), calls=%async_computation.6 | async-start | bytes 6291456
  19.5 18.8 %slice-start.4 = ((s8[11534336]{0:T(1024)(128)(4,1)}), s8[4194304]{0:T(1024)(128)(4,1)S(1)}, s32[]{:S(2)}) async-start(s8[11534336]{0:T(1024)(128)(4,1)} %bitcast.8), calls=%async_computation.8 | async-start | bytes 8388608
  19.5 18.8 %slice-start.5 = ((s8[11534336]{0:T(1024)(128)(4,1)}), s8[3145728]{0:T(1024)(128)(4,1)S(1)}, s32[]{:S(2)}) async-start(s8[11534336]{0:T(1024)(128)(4,1)} %bitcast.8), calls=%async_computation.9 | async-start | bytes 6291456
  19.5 18.8 %slice-start.7 = ((s8[11534336]{0:T(1024)(128)(4,1)}), s8[4194304]{0:T(1024)(128)(4,1)S(1)}, s32[]{:S(2)}) async-start(s8[11534336]{0:T(1024)(128)(4,1)} %bitcast.10), calls=%async_computation.11 | async-start | bytes 8388608
  19.5 18.8 %slice-start.8 = ((s8[11534336]{0:T(1024)(128)(4,1)}), s8[3145728]{0:T(1024)(128)(4,1)S(1)}, s32[]{:S(2)}) async-start(s8[11534336]{0:T(1024)(128)(4,1)} %bitcast.10), calls=%async_computation.12 | async-start | bytes 6291456
  21.0 17.3 %copy-start.1 = (f32[4096]{0:T(1024)S(1)}, f32[4096]{0:T(1024)}, u32[]{:S(2)}) copy-start(f32[4096]{0:T(1024)} %param.24) | copy-start | bytes 49156

commit v3 on v2

--- a/solution.py
+++ b/solution.py
@@ -39,44 +39,73 @@
     return v / (1.0 + jnp.exp(-v))
 
 
-def project_body(own, other, norm_gain, w_query, w_forget, w_input, w_outgate, out, held, sems):
-    copies = [
-        pltpu.make_async_copy(weight, held.at[i], sems.at[i])
-        for i, weight in enumerate((w_query, w_forget, w_input, w_outgate))
+def start_body(
+    tokens, norm_gain, w_query, w_forget, w_input, w_outgate,
+    own, squares, other_gain, rest, held, held_tokens, held_gain, sems,
+):
+    half = held.shape[1]
+    tp_index, base = lax.axis_index("tp"), lax.axis_index("kv") * 2 * half
+    mine = pl.multiple_of(tp_index * half, LANES)
+    theirs = pl.multiple_of((1 - tp_index) * half, LANES)
+    weights = (w_query, w_forget, w_input, w_outgate)
+    moves = [
+        (tokens, held_tokens),
+        (norm_gain.at[:, pl.ds(pl.multiple_of(base + mine, LANES), half)], held_gain),
+        *[(w.at[pl.ds(mine, half), :], held.at[i]) for i, w in enumerate(weights)],
+        (norm_gain.at[:, pl.ds(pl.multiple_of(base + theirs, LANES), half)], other_gain),
+        *[(w.at[pl.ds(theirs, half), :], rest.at[i]) for i, w in enumerate(weights)],
     ]
+    copies = [pltpu.make_async_copy(src, dst, sems.at[i]) for i, (src, dst) in enumerate(moves)]
     for copy in copies:
         copy.start()
-    col_block = held.shape[1]
-    tp_index = lax.axis_index("tp")
-    start = pl.multiple_of(lax.axis_index("kv") * col_block, LANES)
-    first = own[...].astype(jnp.float32)
-    second = other[...].astype(jnp.float32)
-    cols = jnp.concatenate(
-        [jnp.where(tp_index == 0, first, second), jnp.where(tp_index == 0, second, first)], axis=1
-    )
-    squares = jnp.sum(cols * cols, axis=1, keepdims=True)
-    scaled = (cols * norm_gain[:, pl.ds(start, col_block)]).astype(jnp.bfloat16)
-    spread = jnp.broadcast_to(squares, (squares.shape[0], LANES))
-    row = len(copies) * (held.shape[2] // LANES)
-    while row < out.shape[1]:
-        out[:, row, :] = spread
-        row += 1
+    copies[0].wait()
+    copies[1].wait()
+    cols = held_tokens[...].astype(jnp.float32)
+    squares[...] = jnp.broadcast_to(
+        jnp.sum(cols * cols, axis=1, keepdims=True), (cols.shape[0], LANES)
+    )
+    scaled = (cols * held_gain[...]).astype(jnp.bfloat16)
+    for i in range(len(weights)):
+        copies[2 + i].wait()
+        own[i] = jnp.dot(scaled, held[i], preferred_element_type=jnp.float32)
+    for copy in copies[2 + len(weights) :]:
+        copy.wait()
+
+
+def project_body(other, own, own_squares, other_gain, rest, kept, *sent_and_scratch):
+    *sent, every = sent_and_scratch
+    kv_index = lax.axis_index("kv")
+    cols = other[...].astype(jnp.float32)
+    squares = own_squares[...] + jnp.sum(cols * cols, axis=1, keepdims=True)
+    scaled = (cols * other_gain[...]).astype(jnp.bfloat16)
     row = 0
-    for i, copy in enumerate(copies):
-        copy.wait()
-        product = jnp.dot(scaled, held[i], preferred_element_type=jnp.float32)
-        for at in range(0, held.shape[2], LANES):
-            out[:, row, :] = product[:, at : at + LANES]
+    for i in range(rest.shape[0]):
+        product = own[i] + jnp.dot(scaled, rest[i], preferred_element_type=jnp.float32)
+        for at in range(0, product.shape[1], LANES):
+            every[:, row, :] = product[:, at : at + LANES]
             row += 1
-
-
-def recur_body(model_width, received, rec_state, lower_bound, head_gain, new_state, gated):
+    for at in range(row, every.shape[1]):
+        every[:, at, :] = squares
+    kept[...] = every[kv_index]
+    for j, out in enumerate(sent, 1):
+        block = every[kv_index ^ j]
+        high = block[row:].astype(jnp.bfloat16).astype(jnp.float32)
+        wide = jnp.concatenate([block[:row], high, block[row:] - high], axis=0)
+        out[...] = wide.astype(jnp.bfloat16)
+
+
+def recur_body(model_width, arrived, *refs):
+    kept, *received = refs[: arrived + 1]
+    rec_state, lower_bound, head_gain, new_state, gated = refs[arrived + 1 :]
     heads = rec_state.shape[0]
-    total = received[0]
-    for block in range(1, received.shape[0]):
-        total = total + received[block]
-    squares = total[4 * heads : 4 * heads + 1, :]
-    row_scale = lax.rsqrt(squares / model_width + epsilon)
+    row = 4 * heads
+    total = kept[:row]
+    squares = kept[row : row + 8]
+    for block in received:
+        wide = block[...].astype(jnp.float32)
+        total = total + wide[:row]
+        squares = squares + wide[row : row + 8] + wide[row + 8 : row + 16]
+    row_scale = lax.rsqrt(squares[:1] / model_width + epsilon)
     query_pre = row_scale * total[:heads]
     forget_pre = row_scale * total[heads : 2 * heads]
     value_in = row_scale * total[2 * heads : 3 * heads]
@@ -168,28 +197,52 @@
     model_width = norm_gain.shape[0]
     shape = jax.ShapeDtypeStruct
     other = lax.ppermute(tokens, "tp", [(i, (i + 1) % tp_count) for i in range(tp_count)])
-    sent = call(
-        project_body,
-        shape((row_count, 4 * heads + 8, LANES), jnp.float32),
-        tokens,
-        other,
-        norm_gain[None],
-        streamed=(w_query, w_forget, w_input, w_outgate),
+    weights = (w_query, w_forget, w_input, w_outgate)
+    half_shape = (4, own_width, w_query.shape[1])
+    own, squares, other_gain, rest = call(
+        start_body,
+        (
+            shape((4, row_count, w_query.shape[1]), jnp.float32),
+            shape((row_count, LANES), jnp.float32),
+            pltpu.VMEM((1, own_width), jnp.float32),
+            pltpu.VMEM(half_shape, w_query.dtype),
+        ),
+        streamed=(tokens, norm_gain[None], *weights),
         scratch=[
-            pltpu.VMEM((4,) + w_query.shape, w_query.dtype),
-            pltpu.SemaphoreType.DMA((4,)),
+            pltpu.VMEM(half_shape, w_query.dtype),
+            pltpu.VMEM(tokens.shape, tokens.dtype),
+            pltpu.VMEM((1, own_width), jnp.float32),
+            pltpu.SemaphoreType.DMA((3 + 2 * len(weights),)),
         ],
         limit=12 * 2**20,
+    )
+    rows = 4 * heads
+    kept, *sent = call(
+        project_body,
+        (
+            shape((rows + 8, LANES), jnp.float32),
+            *[shape((rows + 16, LANES), jnp.bfloat16)] * (kv_count - 1),
+        ),
+        other,
+        own,
+        squares,
+        resident(other_gain),
+        resident(rest),
+        scratch=[pltpu.VMEM((row_count, rows + 8, LANES), jnp.float32)],
         cost=LONG,
     )
-    received = lax.all_to_all(sent, "kv", 0, 0)
+    received = [
+        lax.ppermute(block, "kv", [(i, i ^ j) for i in range(kv_count)])
+        for j, block in enumerate(sent, 1)
+    ]
     new_state, gated = call(
-        lambda *refs: recur_body(model_width, *refs),
+        lambda *refs: recur_body(model_width, len(received), *refs),
         (
-            shape(rec_state.shape[1:], jnp.float32),
+            pltpu.VMEM(rec_state.shape[1:], jnp.float32),
             shape((group_count, heads, HEAD_DIM), jnp.float32),
         ),
-        received,
+        kept,
+        *received,
         resident(rec_state[0]),
         lower_bound.reshape(heads, HEAD_DIM),
         head_gain.reshape(heads, HEAD_DIM),
@@ -318,7 +371,8 @@
     tokens, rec_state = args[0], args[1]
     w_heads_out, w_gate = args[9], args[11]
     aligned = all(size % LANES == 0 for size in (tokens.shape[1], w_gate.shape[1]))
-    if aligned and rec_state.shape[0] == 1 and lax.axis_size("tp") == 2:
+    small = lax.axis_size("tp") == 2 and lax.axis_size("kv") in (2, 4)
+    if aligned and small and rec_state.shape[0] == 1:
         return local(*args)
     return plain_local(*args)
 

time: 52.1 us -> 49.7 us (0.954)
  blocking collectives: 36.8 us -> 16.9 us
  waiting for transfers between devices: 1.03 us -> 10.4 us
  starting transfers between devices: 0.56 us -> 9.14 us
  local copies, waits for them, and re-layouts: 1.47 us -> 0.87 us
    all_to_all x2 -> x0, blocking collectives: 19.9 us -> none  [the longest x1 11.8 us: local(): received = lax.all_to_all(sent, 'kv', 0, 0)]
    ppermute x0 -> x3, waiting for transfers between devices: none -> 5.49 us  [local(): lax.ppermute(block, 'kv', [(i, i ^ j) for i in range(kv_count)])]
    ppermute x0 -> x3, starting transfers between devices: none -> 5.25 us  [local(): lax.ppermute(block, 'kv', [(i, i ^ j) for i in range(kv_count)])]
    all_to_all x0 -> x1, waiting for transfers between devices: none -> 4.88 us  [local(): back = lax.all_to_all(blocked, GROUP, 0, 0)]
    all_to_all x0 -> x1, starting transfers between devices: none -> 3.33 us  [local(): back = lax.all_to_all(blocked, GROUP, 0, 0)]
    ppermute x1, waiting for transfers between devices: 1.03 us -> 0.01 us  [local(): lax.ppermute(tokens, 'tp', [(i, (i + 1) % tp_count) for i in range(tp_cou...]
    unnamed x34 -> x31, local copies, waits for them, and re-layouts: 1.47 us -> 0.87 us
    pallas_call x5 -> x6, Pallas kernels: 11.1 us -> 11.3 us  [call(): pl.pallas_call(body, out_shape=outs, in_specs=[VMEM] * len(args) + [HBM]...]
  transfers between devices with their start and end apart: 1 -> 5, of which waited for: 1 -> 3; matrix products, arithmetic and copies ran while one was open for 0% -> 2% of each run, Pallas kernels for 0% -> 7%
where the time goes in v3:
time: 49.7 us; the launch traced here: 49.4 us
  blocking collectives  16.9 us (34%)
  Pallas kernels  11.3 us (23%)
  waiting for transfers between devices  10.4 us (21%)
  starting transfers between devices  9.14 us (18%)
  local copies, waits for them, and re-layouts  0.87 us (2%)
  between operations  0.87 us (2%)
    pallas_call x6, Pallas kernels, call(): pl.pallas_call(body, out_shape=outs, in_specs=[VMEM] * len(args) + [HBM]...  11.3 us
    all_to_all x1, blocking collectives, local(): every_head = lax.all_to_all(gated, GROUP, 0, 0)  8.64 us
    all_to_all x1, blocking collectives, local(): gathered = lax.all_to_all(copies, GROUP, 0, 0)  8.25 us
    ppermute x3, waiting for transfers between devices, local(): lax.ppermute(block, 'kv', [(i, i ^ j) for i in range(kv_count)])  5.49 us
    ppermute x3, starting transfers between devices, local(): lax.ppermute(block, 'kv', [(i, i ^ j) for i in range(kv_count)])  5.25 us
    all_to_all x1, waiting for transfers between devices, local(): back = lax.all_to_all(blocked, GROUP, 0, 0)  4.88 us
    all_to_all x1, starting transfers between devices, local(): back = lax.all_to_all(blocked, GROUP, 0, 0)  3.33 us
  transfers between devices with their start and end apart: 5, of which 3 were waited for; matrix products, arithmetic and copies ran while one was open for 2% of the time, Pallas kernels for 7%

profile of v3, /device:TPU:0, one launch (start us, length us, event | category | flops | bytes accessed | tf_op | source)
XLA Modules:
  0.0 49.4 jit_solution(2946195948737093818)
XLA Ops:
  0.6 0.6 %collective-permute-start = (bf16[4,512]{1,0:T(4,128)(2,1)}, bf16[4,512]{1,0:T(4,128)(2,1)S(1)}, u32[]{:S(2)}, u32[]{:S(2)}) collective-permute-start(bf16[4,512]{1,0:T(4,128)(2,1)} %refs_2_.1), channel_id=1, source_target_pairs={{0,1},{1,0},{2,3},{3,2},{4,5},{5,4},{6,7},{7,6},{8,9},{9,8},{10,11... | collective-permute-start | bytes 12296 | tf_op jit(solution)/shard_map/ppermute | solution.py:199
  1.2 3.6 %shard_map.149 = (f32[4,4,1024]{2,1,0:T(4,128)S(1)}, f32[4,128]{1,0:T(4,128)S(1)}, f32[1,512]{1,0:T(1,128)S(1)}, bf16[4,512,1024]{2,1,0:T(8,128)(2,1)S(1)}) custom-call(bf16[4,512]{1,0:T(4,128)(2,1)} %refs_2_.1, f32[1,4096]{1,0:T(1,128)} %bitcast.17, bf16[1024,1024]{1,0:T(8,128)(2,1)} %w_query.1, bf16[1024,1024]{1,0:T(8,128)(2,1)} %w_forget.1, ...), custom_call_target="tpu_custom_call" | custom-call | flops 10000000 | bytes 10000 | tf_op jit(solution)/shard_map/pallas_call | solution.py:27
  4.8 0.0 collective-permute-done.other
  4.8 0.0 copy-start.3
  4.8 0.0 copy-start.4
  4.8 0.0 copy-start.5
  4.8 0.7 %shard_map.150 = (f32[40,128]{1,0:T(8,128)S(1)}, bf16[48,128]{1,0:T(8,128)(2,1)S(1)}, bf16[48,128]{1,0:T(8,128)(2,1)S(1)}, bf16[48,128]{1,0:T(8,128)(2,1)S(1)}) custom-call(bf16[4,512]{1,0:T(4,128)(2,1)S(1)} %collective-permute-done.other, f32[4,4,1024]{2,1,0:T(4,128)S(1)} %get-tuple-element.14.own, f32[4,128]{1,0:T(4,128)S(1)} %get-tuple-element.15.own_squares, ...), custom_call_target="tpu_custom_call" | custom-call | flops 99999997952 | bytes 10000 | tf_op jit(solution)/shard_map/pallas_call | solution.py:27
  5.5 2.7 %collective-permute-start.1 = (bf16[48,128]{1,0:T(8,128)(2,1)S(1)}, bf16[48,128]{1,0:T(8,128)(2,1)S(1)}, u32[]{:S(2)}, u32[]{:S(2)}) collective-permute-start(bf16[48,128]{1,0:T(8,128)(2,1)S(1)} %get-tuple-element.19), channel_id=1, source_target_pairs={{0,2},{2,0},{4,6},{6,4},{1,3},{3,1},{5,7},{7,5},{8,10},{10,8},{12,... | collective-permute-start | bytes 36872 | tf_op jit(solution)/shard_map/ppermute | solution.py:235
  8.2 2.6 %collective-permute-start.2 = (bf16[48,128]{1,0:T(8,128)(2,1)S(1)}, bf16[48,128]{1,0:T(8,128)(2,1)S(1)}, u32[]{:S(2)}, u32[]{:S(2)}) collective-permute-start(bf16[48,128]{1,0:T(8,128)(2,1)S(1)} %get-tuple-element.20), channel_id=1, source_target_pairs={{0,4},{2,6},{4,0},{6,2},{1,5},{3,7},{5,1},{7,3},{8,12},{10,14},{12... | collective-permute-start | bytes 36872 | tf_op jit(solution)/shard_map/ppermute | solution.py:235
  10.7 0.0 collective-permute-start.3
  10.7 0.0 collective-permute-done.1.refs_1_
  10.8 2.0 %collective-permute-done.2.refs_2_ = bf16[48,128]{1,0:T(8,128)(2,1)S(1)} collective-permute-done((bf16[48,128]{1,0:T(8,128)(2,1)S(1)}, bf16[48,128]{1,0:T(8,128)(2,1)S(1)}, u32[]{:S(2)}, u32[]{:S(2)}) %collective-permute-start.2) | collective-permute-done | bytes 12320 | tf_op jit(solution)/shard_map/ppermute | solution.py:235
  12.8 3.5 %collective-permute-done.3.refs_3_ = bf16[48,128]{1,0:T(8,128)(2,1)S(1)} collective-permute-done((bf16[48,128]{1,0:T(8,128)(2,1)S(1)}, bf16[48,128]{1,0:T(8,128)(2,1)S(1)}, u32[]{:S(2)}, u32[]{:S(2)}) %collective-permute-start.3) | collective-permute-done | bytes 12320 | tf_op jit(solution)/shard_map/ppermute | solution.py:235
  16.2 0.0 copy-done.3
  16.3 0.0 copy-start
  16.3 0.0 copy-start.2
  16.3 0.0 slice-start.1
  16.3 0.0 slice-start.2
  16.3 0.0 slice-start.4
  16.3 0.0 slice-start.5
  16.3 0.0 slice-start.7
  16.3 0.0 slice-start.8
  16.4 0.8 %shard_map.151 = (f32[8,128,128]{2,1,0:T(8,128)S(1)}, f32[8,8,128]{2,1,0:T(8,128)S(1)}) custom-call(f32[40,128]{1,0:T(8,128)S(1)} %get-tuple-element.18.refs_0_, bf16[48,128]{1,0:T(8,128)(2,1)S(1)} %collective-permute-done.1.refs_1_, bf16[48,128]{1,0:T(8,128)(2,1)S(1)} %collective-permute-done.2.refs_2_, bf16[48,128]{1,0:T(8,128)(2,1)S(1)} %collective-permute-done.3.refs_3_, ...), custom_call_target="tpu_custom_call" | custom-call | flops 99999997952 | bytes 10000 | tf_op jit(solution)/shard_map/pallas_call | solution.py:27
  17.1 8.6 %all_to_all.15.refs_0_ = f32[8,8,128]{2,1,0:T(8,128)S(1)} all-to-all(f32[8,8,128]{2,1,0:T(8,128)S(1)} %get-tuple-element.22), channel_id=1, replica_groups=mesh['dp'=4,'kv'=4,'tp'=2] {'kv','tp'}, dimensions={0} | all-to-all | bytes 65536 | tf_op jit(solution)/shard_map/all_to_all | solution.py:251
  25.8 0.0 copy-done
  25.8 0.4 shard_map.152
  26.2 8.3 %all_to_all.16.gathered = bf16[8,4,512]{2,1,0:T(4,128)(2,1)S(1)} all-to-all(bf16[8,4,512]{2,1,0:T(4,128)(2,1)S(1)} %get-tuple-element.23), channel_id=1, replica_groups=mesh['dp'=4,'kv'=4,'tp'=2] {'kv','tp'}, dimensions={0} | all-to-all | bytes 65536 | tf_op jit(solution)/shard_map/all_to_all | solution.py:262
  34.5 5.3 %shard_map.153 = bf16[8,4,512]{2,1,0:T(4,128)(2,1)} custom-call(bf16[8,4,512]{2,1,0:T(4,128)(2,1)S(1)} %all_to_all.16.gathered, f32[1,4096]{1,0:T(1,128)S(1)} %bitcast.13, bf16[4096,1408]{1,0:T(8,128)(2,1)S(1)} %bitcast.8, bf16[4096,1408]{1,0:T(8,128)(2,1)S(1)} %bitcast.10, bf16[1408,4096]{1,0:T(8,128)(2,1)S(1)} %bitcast.12), custom_call_target="tpu_custom_call" | custom-call | flops 10000000 | bytes 10000 | tf_op jit(solution)/shard_map/pallas_call | solution.py:27
  39.8 3.3 %all-to-all-start.2 = ((bf16[8,4,512]{2,1,0:T(4,128)(2,1)}), bf16[8,4,512]{2,1,0:T(4,128)(2,1)S(1)}, u32[]{:S(2)}, u32[]{:S(2)}) async-start(bf16[8,4,512]{2,1,0:T(4,128)(2,1)} %shard_map.153), calls=%async_computation.2 | async-start | bytes 65536 | tf_op jit(solution)/shard_map/all_to_all | solution.py:272
  43.2 0.8 %copy.16 = f32[1,8,128,128]{3,2,1,0:T(8,128)} copy(f32[1,8,128,128]{3,2,1,0:T(8,128)S(1)} %bitcast.6) | data formatting | bytes 1048576
  44.0 4.9 %all-to-all-done.2.received = bf16[8,4,512]{2,1,0:T(4,128)(2,1)S(1)} async-done(((bf16[8,4,512]{2,1,0:T(4,128)(2,1)}), bf16[8,4,512]{2,1,0:T(4,128)(2,1)S(1)}, u32[]{:S(2)}, u32[]{:S(2)}) %all-to-all-start.2) | async-done | bytes 32800 | tf_op jit(solution)/shard_map/all_to_all | solution.py:272
  48.8 0.6 %shard_map.154 = bf16[4,512]{1,0:T(4,128)(2,1)} custom-call(bf16[8,4,512]{2,1,0:T(4,128)(2,1)S(1)} %all-to-all-done.2.received, bf16[4,512]{1,0:T(4,128)(2,1)S(1)} %get-tuple-element.24.mixed), custom_call_target="tpu_custom_call" | custom-call | flops 10000000 | bytes 10000 | tf_op jit(solution)/shard_map/pallas_call | solution.py:27
  (20 shorter events, 0.0 us)
Async XLA Ops:
  0.6 4.1 %collective-permute-start = (bf16[4,512]{1,0:T(4,128)(2,1)}, bf16[4,512]{1,0:T(4,128)(2,1)S(1)}, u32[]{:S(2)}, u32[]{:S(2)}) collective-permute-start(bf16[4,512]{1,0:T(4,128)(2,1)} %refs_2_.1), channel_id=1, source_target_pairs={{0,1},{1,0},{2,3},{3,2},{4,5},{5,4},{6,7},{7,6},{8,9},{9,8},{10,11... | collective-permute-start | bytes 12296 | tf_op jit(solution)/shard_map/ppermute | solution.py:199
  4.8 11.5 %copy-start.3 = (f32[1,8,128,128]{3,2,1,0:T(8,128)S(1)}, f32[1,8,128,128]{3,2,1,0:T(8,128)}, u32[]{:S(2)}) copy-start(f32[1,8,128,128]{3,2,1,0:T(8,128)} %param.15) | copy-start | bytes 1572868
  4.8 11.5 %copy-start.4 = (f32[1024]{0:T(1024)S(1)}, f32[1024]{0:T(1024)}, u32[]{:S(2)}) copy-start(f32[1024]{0:T(1024)} %param.21) | copy-start | bytes 12292
  4.8 11.5 %copy-start.5 = (f32[1024]{0:T(1024)S(1)}, f32[1024]{0:T(1024)}, u32[]{:S(2)}) copy-start(f32[1024]{0:T(1024)} %param.22) | copy-start | bytes 12292
  5.5 5.3 %collective-permute-start.1 = (bf16[48,128]{1,0:T(8,128)(2,1)S(1)}, bf16[48,128]{1,0:T(8,128)(2,1)S(1)}, u32[]{:S(2)}, u32[]{:S(2)}) collective-permute-start(bf16[48,128]{1,0:T(8,128)(2,1)S(1)} %get-tuple-element.19), channel_id=1, source_target_pairs={{0,2},{2,0},{4,6},{6,4},{1,3},{3,1},{5,7},{7,5},{8,10},{10,8},{12,... | collective-permute-start | bytes 36872 | tf_op jit(solution)/shard_map/ppermute | solution.py:235
  8.2 4.6 %collective-permute-start.2 = (bf16[48,128]{1,0:T(8,128)(2,1)S(1)}, bf16[48,128]{1,0:T(8,128)(2,1)S(1)}, u32[]{:S(2)}, u32[]{:S(2)}) collective-permute-start(bf16[48,128]{1,0:T(8,128)(2,1)S(1)} %get-tuple-element.20), channel_id=1, source_target_pairs={{0,4},{2,6},{4,0},{6,2},{1,5},{3,7},{5,1},{7,3},{8,12},{10,14},{12... | collective-permute-start | bytes 36872 | tf_op jit(solution)/shard_map/ppermute | solution.py:235
  10.7 5.5 %collective-permute-start.3 = (bf16[48,128]{1,0:T(8,128)(2,1)S(1)}, bf16[48,128]{1,0:T(8,128)(2,1)S(1)}, u32[]{:S(2)}, u32[]{:S(2)}) collective-permute-start(bf16[48,128]{1,0:T(8,128)(2,1)S(1)} %get-tuple-element.21), channel_id=1, source_target_pairs={{0,6},{2,4},{4,2},{6,0},{1,7},{3,5},{5,3},{7,1},{8,14},{10,12},{12... | collective-permute-start | bytes 36872 | tf_op jit(solution)/shard_map/ppermute | solution.py:235
  16.2 18.2 %slice-start = ((s8[11534336]{0:T(1024)(128)(4,1)}), s8[4194304]{0:T(1024)(128)(4,1)S(1)}, s32[]{:S(2)}) async-start(s8[11534336]{0:T(1024)(128)(4,1)} %bitcast.7), calls=%async_computation.3 | async-start | bytes 8388608
  16.2 18.2 %slice-start.3 = ((s8[11534336]{0:T(1024)(128)(4,1)}), s8[4194304]{0:T(1024)(128)(4,1)S(1)}, s32[]{:S(2)}) async-start(s8[11534336]{0:T(1024)(128)(4,1)} %bitcast.9), calls=%async_computation.6 | async-start | bytes 8388608
  16.2 18.2 %slice-start.6 = ((s8[11534336]{0:T(1024)(128)(4,1)}), s8[4194304]{0:T(1024)(128)(4,1)S(1)}, s32[]{:S(2)}) async-start(s8[11534336]{0:T(1024)(128)(4,1)} %bitcast.11), calls=%async_computation.9 | async-start | bytes 8388608
  16.3 9.5 %copy-start = (bf16[2048,512]{1,0:T(8,128)(2,1)S(1)}, bf16[2048,512]{1,0:T(8,128)(2,1)}, u32[]{:S(2)}) copy-start(bf16[2048,512]{1,0:T(8,128)(2,1)} %refs_1_.1) | copy-start | bytes 6291460
  16.3 9.5 %copy-start.2 = (bf16[4,512]{1,0:T(4,128)(2,1)S(1)}, bf16[4,512]{1,0:T(4,128)(2,1)}, u32[]{:S(2)}) copy-start(bf16[4,512]{1,0:T(4,128)(2,1)} %refs_2_.1) | copy-start | bytes 12292
  16.3 18.1 %slice-start.1 = ((s8[11534336]{0:T(1024)(128)(4,1)}), s8[4194304]{0:T(1024)(128)(4,1)S(1)}, s32[]{:S(2)}) async-start(s8[11534336]{0:T(1024)(128)(4,1)} %bitcast.7), calls=%async_computation.4 | async-start | bytes 8388608
  16.3 18.1 %slice-start.2 = ((s8[11534336]{0:T(1024)(128)(4,1)}), s8[3145728]{0:T(1024)(128)(4,1)S(1)}, s32[]{:S(2)}) async-start(s8[11534336]{0:T(1024)(128)(4,1)} %bitcast.7), calls=%async_computation.5 | async-start | bytes 6291456
  16.3 18.1 %slice-start.4 = ((s8[11534336]{0:T(1024)(128)(4,1)}), s8[4194304]{0:T(1024)(128)(4,1)S(1)}, s32[]{:S(2)}) async-start(s8[11534336]{0:T(1024)(128)(4,1)} %bitcast.9), calls=%async_computation.7 | async-start | bytes 8388608
  16.3 18.1 %slice-start.5 = ((s8[11534336]{0:T(1024)(128)(4,1)}), s8[3145728]{0:T(1024)(128)(4,1)S(1)}, s32[]{:S(2)}) async-start(s8[11534336]{0:T(1024)(128)(4,1)} %bitcast.9), calls=%async_computation.8 | async-start | bytes 6291456
  16.3 18.1 %slice-start.7 = ((s8[11534336]{0:T(1024)(128)(4,1)}), s8[4194304]{0:T(1024)(128)(4,1)S(1)}, s32[]{:S(2)}) async-start(s8[11534336]{0:T(1024)(128)(4,1)} %bitcast.11), calls=%async_computation.10 | async-start | bytes 8388608
  16.3 18.1 %slice-start.8 = ((s8[11534336]{0:T(1024)(128)(4,1)}), s8[3145728]{0:T(1024)(128)(4,1)S(1)}, s32[]{:S(2)}) async-start(s8[11534336]{0:T(1024)(128)(4,1)} %bitcast.11), calls=%async_computation.11 | async-start | bytes 6291456
  17.1 17.4 %copy-start.1 = (f32[4096]{0:T(1024)S(1)}, f32[4096]{0:T(1024)}, u32[]{:S(2)}) copy-start(f32[4096]{0:T(1024)} %param.24) | copy-start | bytes 49156
  39.8 9.0 %all-to-all-start.2 = ((bf16[8,4,512]{2,1,0:T(4,128)(2,1)}), bf16[8,4,512]{2,1,0:T(4,128)(2,1)S(1)}, u32[]{:S(2)}, u32[]{:S(2)}) async-start(bf16[8,4,512]{2,1,0:T(4,128)(2,1)} %shard_map.153), calls=%async_computation.2 | async-start | bytes 65536 | tf_op jit(solution)/shard_map/all_to_all | solution.py:272

commit v4 on v3

--- a/solution.py
+++ b/solution.py
@@ -130,46 +130,90 @@
         jnp.mean(head_out * head_out, axis=1, keepdims=True) + epsilon
     )
     rounded = (head_out * head_gain[...] * silu(gate_pre)).astype(jnp.bfloat16)
-    for block in range(gated.shape[0]):
-        gated[block] = rounded.astype(jnp.float32)
-
-
-def heads_body(tp_count, every_head, w_heads_out, tokens, mixed, copies):
-    rows, heads = tokens.shape[0], every_head.shape[1]
-    left = jnp.concatenate(
-        [
-            every_head[pl.ds(t, rows, stride=tp_count), h, :]
-            for t in range(tp_count)
-            for h in range(heads)
-        ],
-        axis=1,
-    ).astype(jnp.bfloat16)
-    added = jnp.dot(left, w_heads_out[...], preferred_element_type=jnp.float32)
-    rounded = (tokens[...].astype(jnp.float32) + added).astype(jnp.bfloat16)
-    mixed[...] = rounded
-    for block in range(copies.shape[0]):
-        copies[block] = rounded
-
-
-def mixer_body(gathered, mixer_gain, w_gate, w_up, w_down, out):
-    rows = jnp.concatenate([gathered[i] for i in range(gathered.shape[0])], axis=1)
-    rows = rows.astype(jnp.float32)
-    scale = lax.rsqrt(jnp.mean(rows * rows, axis=1, keepdims=True) + epsilon)
-    normed = (rows * scale * mixer_gain[...]).astype(jnp.bfloat16)
-    gate_val = jnp.dot(normed, w_gate[...], preferred_element_type=jnp.float32)
-    up_val = jnp.dot(normed, w_up[...], preferred_element_type=jnp.float32)
-    hidden = (silu(gate_val) * up_val).astype(jnp.bfloat16)
-    terms = jnp.dot(hidden, w_down[...], preferred_element_type=jnp.float32)
-    terms = terms.astype(jnp.bfloat16)
-    width = out.shape[2]
-    for i in range(out.shape[0]):
-        out[i] = terms[:, i * width : (i + 1) * width]
-
-
-def result_body(received, mixed, out):
-    total = mixed[...].astype(jnp.float32)
-    for block in range(received.shape[0]):
-        total = total + received[block].astype(jnp.float32)
+    gated[...] = rounded.astype(jnp.float32)
+
+
+def pair_body(own, other, out):
+    first = lax.axis_index("tp") == 0
+    left = own[...].astype(jnp.float32)
+    right = other[...].astype(jnp.float32)
+    low, high = jnp.where(first, left, right), jnp.where(first, right, left)
+    out[...] = jnp.concatenate([low, high], axis=0).astype(out.dtype).reshape(out.shape)
+
+
+def heads_body(*refs):
+    *blocks, w_heads_out, tokens, mixed, every = refs
+    kv_index = lax.axis_index("kv")
+    for j, block in enumerate(blocks):
+        every[kv_index ^ j] = block[...].astype(jnp.float32)
+    left = jnp.concatenate([every[:, h, :] for h in range(every.shape[1])], axis=1)
+    added = jnp.dot(
+        left.astype(jnp.bfloat16), w_heads_out[...], preferred_element_type=jnp.float32
+    )
+    mixed[...] = (tokens[...].astype(jnp.float32) + added).astype(jnp.bfloat16)
+
+
+def mixer_block(j, block, mixer_gain, w_gate, w_up):
+    depth = block.shape[0] * block.shape[2]
+    start = pl.multiple_of((lax.axis_index("kv") ^ j) * depth, LANES)
+    cols = jnp.concatenate([block[t] for t in range(block.shape[0])], axis=1)
+    cols = cols.astype(jnp.float32)
+    squares = jnp.sum(cols * cols, axis=1, keepdims=True)
+    gained = (cols * mixer_gain[:, pl.ds(start, depth)]).astype(jnp.bfloat16)
+    return (
+        jnp.dot(gained, w_gate[pl.ds(start, depth), :], preferred_element_type=jnp.float32),
+        jnp.dot(gained, w_up[pl.ds(start, depth), :], preferred_element_type=jnp.float32),
+        squares,
+    )
+
+
+def mixer_own_body(block, mixer_gain, w_gate, w_up, w_down, gate, up, squares):
+    gate[...], up[...], summed = mixer_block(0, block, mixer_gain, w_gate, w_up)
+    squares[...] = jnp.broadcast_to(summed, squares.shape)
+
+
+def down_block(hidden, w_down, chip, core, width):
+    start = pl.multiple_of((chip * 2 + core) * width, LANES)
+    return jnp.dot(hidden, w_down[:, pl.ds(start, width)], preferred_element_type=jnp.float32)
+
+
+def mixer_body(*refs):
+    gate, up, squares, *blocks = refs[:-6]
+    mixer_gain, w_gate, w_up, w_down, hidden, passed = refs[-6:]
+    gate_val, up_val, total = gate[...], up[...], squares[:, :1]
+    for j, block in enumerate(blocks, 1):
+        more_gate, more_up, more = mixer_block(j, block, mixer_gain, w_gate, w_up)
+        gate_val, up_val, total = gate_val + more_gate, up_val + more_up, total + more
+    scale = lax.rsqrt(total / w_gate.shape[0] + epsilon)
+    gate_val, up_val = scale * gate_val, scale * up_val
+    active = (silu(gate_val) * up_val).astype(jnp.bfloat16)
+    hidden[...] = active
+    kv_index, tp_index = lax.axis_index("kv"), lax.axis_index("tp")
+    for j in range(passed.shape[0]):
+        core = 1 - tp_index if j == 0 else tp_index
+        passed[j] = down_block(active, w_down, kv_index ^ j, core, passed.shape[2]).astype(
+            jnp.bfloat16
+        )
+
+
+def down_body(hidden, w_down, sums):
+    kv_index, tp_index = lax.axis_index("kv"), lax.axis_index("tp")
+    for j in range(sums.shape[0]):
+        core = tp_index if j == 0 else 1 - tp_index
+        sums[j] = down_block(hidden[...], w_down, kv_index ^ j, core, sums.shape[2])
+
+
+def chip_sum_body(sums, passed, mixed, base, *sent):
+    base[...] = mixed[...].astype(jnp.float32) + sums[0] + passed[0].astype(jnp.float32)
+    for j, out in enumerate(sent, 1):
+        out[...] = (sums[j] + passed[j].astype(jnp.float32)).astype(jnp.bfloat16)
+
+
+def result_body(base, *refs):
+    *received, out = refs
+    total = base[...]
+    for block in received:
+        total = total + block[...].astype(jnp.float32)
     out[...] = total.astype(jnp.bfloat16)
 
 
@@ -239,7 +283,7 @@
         lambda *refs: recur_body(model_width, len(received), *refs),
         (
             pltpu.VMEM(rec_state.shape[1:], jnp.float32),
-            shape((group_count, heads, HEAD_DIM), jnp.float32),
+            shape((heads, HEAD_DIM), jnp.float32),
         ),
         kept,
         *received,
@@ -248,29 +292,77 @@
         head_gain.reshape(heads, HEAD_DIM),
         cost=LONG,
     )
-    every_head = lax.all_to_all(gated, GROUP, 0, 0)
-    mixed, copies = call(
-        lambda *refs: heads_body(tp_count, *refs),
-        (
-            shape((row_count, own_width), jnp.bfloat16),
-            shape((group_count, row_count, own_width), jnp.bfloat16),
-        ),
-        every_head,
+
+    def swapped(block):
+        return lax.ppermute(block, "tp", [(0, 1), (1, 0)])
+
+    def crossed(block, j):
+        return lax.ppermute(block, GROUP, [(i, i ^ (2 * j + 1)) for i in range(group_count)])
+
+    others = range(1, kv_count)
+    pair = call(
+        pair_body, shape((2 * heads, HEAD_DIM), jnp.bfloat16), gated, swapped(gated)
+    )
+    mixed = call(
+        heads_body,
+        shape((row_count, own_width), jnp.bfloat16),
+        pair,
+        *[crossed(pair, j) for j in others],
         resident(w_heads_out),
         tokens,
-    )
-    gathered = lax.all_to_all(copies, GROUP, 0, 0)
-    blocked = call(
+        scratch=[pltpu.VMEM((kv_count, 2 * heads, HEAD_DIM), jnp.float32)],
+    )
+    pair = call(
+        pair_body, shape((2, row_count, own_width), jnp.bfloat16), mixed, swapped(mixed)
+    )
+    blocks = [crossed(pair, j) for j in others]
+    gain = mixer_gain[None]
+    w_gate, w_up, w_down = resident(w_gate), resident(w_up), resident(w_down)
+    width = w_gate.shape[1]
+    products = call(
+        mixer_own_body,
+        (
+            shape((row_count, width), jnp.float32),
+            shape((row_count, width), jnp.float32),
+            shape((row_count, LANES), jnp.float32),
+        ),
+        pair,
+        gain,
+        w_gate,
+        w_up,
+        w_down,
+    )
+    hidden, passed = call(
         mixer_body,
-        shape((group_count, row_count, own_width), jnp.bfloat16),
-        gathered,
-        mixer_gain[None],
-        resident(w_gate),
-        resident(w_up),
-        resident(w_down),
-    )
-    back = lax.all_to_all(blocked, GROUP, 0, 0)
-    result = call(result_body, shape((row_count, own_width), jnp.bfloat16), back, mixed)
+        (
+            shape((row_count, width), jnp.bfloat16),
+            shape((kv_count, row_count, own_width), jnp.bfloat16),
+        ),
+        *products,
+        *blocks,
+        gain,
+        w_gate,
+        w_up,
+        w_down,
+    )
+    passed = swapped(passed)
+    sums = call(down_body, shape(passed.shape, jnp.float32), hidden, w_down)
+    base, *sent = call(
+        chip_sum_body,
+        (
+            shape(mixed.shape, jnp.float32),
+            *[shape(mixed.shape, jnp.bfloat16)] * (kv_count - 1),
+        ),
+        sums,
+        passed,
+        mixed,
+    )
+    result = call(
+        result_body,
+        shape(mixed.shape, jnp.bfloat16),
+        base,
+        *[crossed(block, j) for j, block in enumerate(sent, 1)],
+    )
     return (result, new_state[None])
 
 

time: 49.7 us -> 43.4 us (0.87)
  blocking collectives: 16.9 us -> 0 us
  starting transfers between devices: 9.14 us -> 18.3 us
  waiting for transfers between devices: 10.4 us -> 12.3 us
  Pallas kernels: 11.3 us -> 10.8 us
    all_to_all x2 -> x0, blocking collectives: 16.9 us -> none  [the longest x1 8.64 us: local(): every_head = lax.all_to_all(gated, GROUP, 0, 0)]
    ppermute x0 -> x12, starting transfers between devices: none -> 12.5 us  [the longest x9 11.9 us: crossed(): lax.ppermute(block, GROUP, [(i, i ^ 2 * j + 1) for i in range(group_count)])]
    ppermute x0 -> x12, waiting for transfers between devices: none -> 6.82 us  [the longest x9 4.64 us: crossed(): lax.ppermute(block, GROUP, [(i, i ^ 2 * j + 1) for i in range(group_count)])]
    all_to_all x1 -> x0, waiting for transfers between devices: 4.88 us -> none  [local(): back = lax.all_to_all(blocked, GROUP, 0, 0)]
    all_to_all x1 -> x0, starting transfers between devices: 3.33 us -> none  [local(): back = lax.all_to_all(blocked, GROUP, 0, 0)]
    pallas_call x6 -> x11, Pallas kernels: 11.3 us -> 10.8 us  [call(): pl.pallas_call(body, out_shape=outs, in_specs=[VMEM] * len(args) + [HBM]...]
  transfers between devices with their start and end apart: 5 -> 16, of which waited for: 3 -> 9; matrix products, arithmetic and copies ran while one was open for 2% -> 2% of each run, Pallas kernels for 7% -> 12%
where the time goes in v4:
time: 43.4 us; the launch traced here: 43.2 us
  starting transfers between devices  18.3 us (42%)
  waiting for transfers between devices  12.3 us (28%)
  Pallas kernels  10.8 us (25%)
  between operations  0.88 us (2%)
  local copies, waits for them, and re-layouts  0.87 us (2%)
    ppermute x9, starting transfers between devices, crossed(): lax.ppermute(block, GROUP, [(i, i ^ 2 * j + 1) for i in range(group_count)])  11.9 us
    pallas_call x11, Pallas kernels, call(): pl.pallas_call(body, out_shape=outs, in_specs=[VMEM] * len(args) + [HBM]...  10.8 us
    ppermute x3, waiting for transfers between devices, local(): lax.ppermute(block, 'kv', [(i, i ^ j) for i in range(kv_count)])  5.49 us
    ppermute x3, starting transfers between devices, local(): lax.ppermute(block, 'kv', [(i, i ^ j) for i in range(kv_count)])  5.25 us
    ppermute x9, waiting for transfers between devices, crossed(): lax.ppermute(block, GROUP, [(i, i ^ 2 * j + 1) for i in range(group_count)])  4.64 us
    ppermute x3, waiting for transfers between devices, swapped(): return lax.ppermute(block, 'tp', [(0, 1), (1, 0)])  2.18 us
  transfers between devices with their start and end apart: 16, of which 9 were waited for; matrix products, arithmetic and copies ran while one was open for 2% of the time, Pallas kernels for 12%

profile of v4, /device:TPU:0, one launch (start us, length us, event | category | flops | bytes accessed | tf_op | source)
XLA Modules:
  0.0 43.2 jit_solution(18047938785900338754)
XLA Ops:
  0.6 0.6 %collective-permute-start = (bf16[4,512]{1,0:T(4,128)(2,1)}, bf16[4,512]{1,0:T(4,128)(2,1)S(1)}, u32[]{:S(2)}, u32[]{:S(2)}) collective-permute-start(bf16[4,512]{1,0:T(4,128)(2,1)} %refs_5_.1), channel_id=1, source_target_pairs={{0,1},{1,0},{2,3},{3,2},{4,5},{5,4},{6,7},{7,6},{8,9},{9,8},{10,11... | collective-permute-start | bytes 12296 | tf_op jit(solution)/shard_map/ppermute | solution.py:243
  1.2 3.6 %shard_map.149 = (f32[4,4,1024]{2,1,0:T(4,128)S(1)}, f32[4,128]{1,0:T(4,128)S(1)}, f32[1,512]{1,0:T(1,128)S(1)}, bf16[4,512,1024]{2,1,0:T(8,128)(2,1)S(1)}) custom-call(bf16[4,512]{1,0:T(4,128)(2,1)} %refs_5_.1, f32[1,4096]{1,0:T(1,128)} %bitcast.18, bf16[1024,1024]{1,0:T(8,128)(2,1)} %w_query.1, bf16[1024,1024]{1,0:T(8,128)(2,1)} %w_forget.1, ...), custom_call_target="tpu_custom_call" | custom-call | flops 10000000 | bytes 10000 | tf_op jit(solution)/shard_map/pallas_call | solution.py:27
  4.8 0.7 %shard_map.150 = (f32[40,128]{1,0:T(8,128)S(1)}, bf16[48,128]{1,0:T(8,128)(2,1)S(1)}, bf16[48,128]{1,0:T(8,128)(2,1)S(1)}, bf16[48,128]{1,0:T(8,128)(2,1)S(1)}) custom-call(bf16[4,512]{1,0:T(4,128)(2,1)S(1)} %collective-permute-done.other, f32[4,4,1024]{2,1,0:T(4,128)S(1)} %get-tuple-element.21.own, f32[4,128]{1,0:T(4,128)S(1)} %get-tuple-element.22.own_squares, ...), custom_call_target="tpu_custom_call" | custom-call | flops 99999997952 | bytes 10000 | tf_op jit(solution)/shard_map/pallas_call | solution.py:27
  5.5 2.7 %collective-permute-start.1 = (bf16[48,128]{1,0:T(8,128)(2,1)S(1)}, bf16[48,128]{1,0:T(8,128)(2,1)S(1)}, u32[]{:S(2)}, u32[]{:S(2)}) collective-permute-start(bf16[48,128]{1,0:T(8,128)(2,1)S(1)} %get-tuple-element.26), channel_id=1, source_target_pairs={{0,2},{2,0},{4,6},{6,4},{1,3},{3,1},{5,7},{7,5},{8,10},{10,8},{12,... | collective-permute-start | bytes 36872 | tf_op jit(solution)/shard_map/ppermute | solution.py:279
  8.2 2.6 %collective-permute-start.2 = (bf16[48,128]{1,0:T(8,128)(2,1)S(1)}, bf16[48,128]{1,0:T(8,128)(2,1)S(1)}, u32[]{:S(2)}, u32[]{:S(2)}) collective-permute-start(bf16[48,128]{1,0:T(8,128)(2,1)S(1)} %get-tuple-element.27), channel_id=1, source_target_pairs={{0,4},{2,6},{4,0},{6,2},{1,5},{3,7},{5,1},{7,3},{8,12},{10,14},{12... | collective-permute-start | bytes 36872 | tf_op jit(solution)/shard_map/ppermute | solution.py:279
  10.8 2.0 %collective-permute-done.2.refs_2_ = bf16[48,128]{1,0:T(8,128)(2,1)S(1)} collective-permute-done((bf16[48,128]{1,0:T(8,128)(2,1)S(1)}, bf16[48,128]{1,0:T(8,128)(2,1)S(1)}, u32[]{:S(2)}, u32[]{:S(2)}) %collective-permute-start.2) | collective-permute-done | bytes 12320 | tf_op jit(solution)/shard_map/ppermute | solution.py:279
  12.8 3.5 %collective-permute-done.3.refs_3_ = bf16[48,128]{1,0:T(8,128)(2,1)S(1)} collective-permute-done((bf16[48,128]{1,0:T(8,128)(2,1)S(1)}, bf16[48,128]{1,0:T(8,128)(2,1)S(1)}, u32[]{:S(2)}, u32[]{:S(2)}) %collective-permute-start.3) | collective-permute-done | bytes 12320 | tf_op jit(solution)/shard_map/ppermute | solution.py:279
  16.4 0.8 %shard_map.151 = (f32[8,128,128]{2,1,0:T(8,128)S(1)}, f32[8,128]{1,0:T(8,128)S(1)}) custom-call(f32[40,128]{1,0:T(8,128)S(1)} %get-tuple-element.25.refs_0_, bf16[48,128]{1,0:T(8,128)(2,1)S(1)} %collective-permute-done.1.refs_1_, bf16[48,128]{1,0:T(8,128)(2,1)S(1)} %collective-permute-done.2.refs_2_, bf16[48,128]{1,0:T(8,128)(2,1)S(1)} %collective-permute-done.3.refs_3_, ...), custom_call_target="tpu_custom_call" | custom-call | flops 99999997952 | bytes 10000 | tf_op jit(solution)/shard_map/pallas_call | solution.py:27
  17.1 0.0 collective-permute-start.4
  17.2 1.2 %collective-permute-done.4.other = f32[8,128]{1,0:T(8,128)S(1)} collective-permute-done((f32[8,128]{1,0:T(8,128)S(1)}, f32[8,128]{1,0:T(8,128)S(1)}, u32[]{:S(2)}, u32[]{:S(2)}) %collective-permute-start.4) | collective-permute-done | bytes 4128 | tf_op jit(solution)/shard_map/ppermute | solution.py:297
  18.3 0.1 collective-permute-start.6
  18.4 3.8 %collective-permute-start.5 = (bf16[16,128]{1,0:T(8,128)(2,1)S(1)}, bf16[16,128]{1,0:T(8,128)(2,1)S(1)}, u32[]{:S(2)}, u32[]{:S(2)}) collective-permute-start(bf16[16,128]{1,0:T(8,128)(2,1)S(1)} %shard_map.152.refs_0_), channel_id=1, source_target_pairs={{0,3},{1,2},{2,1},{3,0},{4,7},{5,6},{6,5},{7,4},{8,11},{9,10},{10,... | collective-permute-start | bytes 12296 | tf_op jit(solution)/shard_map/ppermute | solution.py:300
  22.2 0.9 %collective-permute-done.7.refs_3_ = bf16[16,128]{1,0:T(8,128)(2,1)S(1)} collective-permute-done((bf16[16,128]{1,0:T(8,128)(2,1)S(1)}, bf16[16,128]{1,0:T(8,128)(2,1)S(1)}, u32[]{:S(2)}, u32[]{:S(2)}) %collective-permute-start.7) | collective-permute-done | bytes 4128 | tf_op jit(solution)/shard_map/ppermute | solution.py:300
  23.2 0.4 collective-permute-done.5.refs_1_
  23.5 0.4 shard_map.153.own.mixed
  23.9 0.3 collective-permute-start.8
  24.2 0.9 %collective-permute-done.8.other = bf16[4,512]{1,0:T(4,128)(2,1)S(1)} collective-permute-done((bf16[4,512]{1,0:T(4,128)(2,1)S(1)}, bf16[4,512]{1,0:T(4,128)(2,1)S(1)}, u32[]{:S(2)}, u32[]{:S(2)}) %collective-permute-start.8) | collective-permute-done | bytes 4128 | tf_op jit(solution)/shard_map/ppermute | solution.py:297
  25.1 2.3 %collective-permute-start.11 = (bf16[2,4,512]{2,1,0:T(4,128)(2,1)S(1)}, bf16[2,4,512]{2,1,0:T(4,128)(2,1)S(1)}, u32[]{:S(2)}, u32[]{:S(2)}) collective-permute-start(bf16[2,4,512]{2,1,0:T(4,128)(2,1)S(1)} %shard_map.154.block), channel_id=1, source_target_pairs={{0,7},{1,6},{2,5},{3,4},{4,3},{5,2},{6,1},{7,0},{8,15},{9,14},{10,... | collective-permute-start | bytes 24584 | tf_op jit(solution)/shard_map/ppermute | solution.py:300
  27.4 0.8 %collective-permute-start.10 = (bf16[2,4,512]{2,1,0:T(4,128)(2,1)S(1)}, bf16[2,4,512]{2,1,0:T(4,128)(2,1)S(1)}, u32[]{:S(2)}, u32[]{:S(2)}) collective-permute-start(bf16[2,4,512]{2,1,0:T(4,128)(2,1)S(1)} %shard_map.154.block), channel_id=1, source_target_pairs={{0,5},{1,4},{2,7},{3,6},{4,1},{5,0},{6,3},{7,2},{8,13},{9,12},{10,... | collective-permute-start | bytes 24584 | tf_op jit(solution)/shard_map/ppermute | solution.py:300
  28.3 0.9 %collective-permute-start.9 = (bf16[2,4,512]{2,1,0:T(4,128)(2,1)S(1)}, bf16[2,4,512]{2,1,0:T(4,128)(2,1)S(1)}, u32[]{:S(2)}, u32[]{:S(2)}) collective-permute-start(bf16[2,4,512]{2,1,0:T(4,128)(2,1)S(1)} %shard_map.154.block), channel_id=1, source_target_pairs={{0,3},{1,2},{2,1},{3,0},{4,7},{5,6},{6,5},{7,4},{8,11},{9,10},{10,... | collective-permute-start | bytes 24584 | tf_op jit(solution)/shard_map/ppermute | solution.py:300
  29.3 0.9 %shard_map.155 = (f32[4,1408]{1,0:T(4,128)S(1)}, f32[4,1408]{1,0:T(4,128)S(1)}, f32[4,128]{1,0:T(4,128)S(1)}) custom-call(bf16[2,4,512]{2,1,0:T(4,128)(2,1)S(1)} %shard_map.154.block, f32[1,4096]{1,0:T(1,128)S(1)} %bitcast.13, bf16[4096,1408]{1,0:T(8,128)(2,1)S(1)} %bitcast.10, bf16[4096,1408]{1,0:T(8,128)(2,1)S(1)} %bitcast.12, bf16[1408,4096]{1,0:T(8,128)(2,1)S(1)} %bitcast.8), custom_call_target="tpu_custom_call" | custom-call | flops 10000000 | bytes 10000 | tf_op jit(solution)/shard_map/pallas_call | solution.py:27
  30.2 1.3 %collective-permute-done.10.refs_4_ = bf16[2,4,512]{2,1,0:T(4,128)(2,1)S(1)} collective-permute-done((bf16[2,4,512]{2,1,0:T(4,128)(2,1)S(1)}, bf16[2,4,512]{2,1,0:T(4,128)(2,1)S(1)}, u32[]{:S(2)}, u32[]{:S(2)}) %collective-permute-start.10) | collective-permute-done | bytes 8224 | tf_op jit(solution)/shard_map/ppermute | solution.py:300
  31.5 3.1 %shard_map.156 = (bf16[4,1408]{1,0:T(4,128)(2,1)S(1)}, bf16[4,4,512]{2,1,0:T(4,128)(2,1)S(1)}) custom-call(f32[4,1408]{1,0:T(4,128)S(1)} %get-tuple-element.30.refs_0_, f32[4,1408]{1,0:T(4,128)S(1)} %get-tuple-element.31.refs_1_, f32[4,128]{1,0:T(4,128)S(1)} %get-tuple-element.32.refs_2_, bf16[2,4,512]{2,1,0:T(4,128)(2,1)S(1)} %collective-permute-done.9.refs_3_, ...), custom_call_target="tpu_custom_call" | custom-call | flops 10000000 | bytes 10000 | tf_op jit(solution)/shard_map/pallas_call | solution.py:27
  34.6 0.2 collective-permute-start.12
  34.8 0.9 %shard_map.157.sums = f32[4,4,512]{2,1,0:T(4,128)S(1)} custom-call(bf16[4,1408]{1,0:T(4,128)(2,1)S(1)} %get-tuple-element.33.hidden, bf16[1408,4096]{1,0:T(8,128)(2,1)S(1)} %bitcast.8), custom_call_target="tpu_custom_call" | custom-call | flops 10000000 | bytes 10000 | tf_op jit(solution)/shard_map/pallas_call | solution.py:27
  35.6 0.2 collective-permute-done.12.passed
  35.8 0.9 %collective-permute-start.13 = (bf16[4,512]{1,0:T(4,128)(2,1)S(1)}, bf16[4,512]{1,0:T(4,128)(2,1)S(1)}, u32[]{:S(2)}, u32[]{:S(2)}) collective-permute-start(bf16[4,512]{1,0:T(4,128)(2,1)S(1)} %get-tuple-element.36), channel_id=1, source_target_pairs={{0,3},{1,2},{2,1},{3,0},{4,7},{5,6},{6,5},{7,4},{8,11},{9,10},{10,... | collective-permute-start | bytes 12296 | tf_op jit(solution)/shard_map/ppermute | solution.py:300
  36.7 1.1 %collective-permute-start.14 = (bf16[4,512]{1,0:T(4,128)(2,1)S(1)}, bf16[4,512]{1,0:T(4,128)(2,1)S(1)}, u32[]{:S(2)}, u32[]{:S(2)}) collective-permute-start(bf16[4,512]{1,0:T(4,128)(2,1)S(1)} %get-tuple-element.37), channel_id=1, source_target_pairs={{0,5},{1,4},{2,7},{3,6},{4,1},{5,0},{6,3},{7,2},{8,13},{9,12},{10,... | collective-permute-start | bytes 12296 | tf_op jit(solution)/shard_map/ppermute | solution.py:300
  37.7 2.0 %collective-permute-start.15 = (bf16[4,512]{1,0:T(4,128)(2,1)S(1)}, bf16[4,512]{1,0:T(4,128)(2,1)S(1)}, u32[]{:S(2)}, u32[]{:S(2)}) collective-permute-start(bf16[4,512]{1,0:T(4,128)(2,1)S(1)} %get-tuple-element.38), channel_id=1, source_target_pairs={{0,7},{1,6},{2,5},{3,4},{4,3},{5,2},{6,1},{7,0},{8,15},{9,14},{10,... | collective-permute-start | bytes 12296 | tf_op jit(solution)/shard_map/ppermute | solution.py:300
  39.8 0.8 %copy.16 = f32[1,8,128,128]{3,2,1,0:T(8,128)} copy(f32[1,8,128,128]{3,2,1,0:T(8,128)S(1)} %bitcast.6) | data formatting | bytes 1048576
  40.6 2.0 %collective-permute-done.15.refs_2_ = bf16[4,512]{1,0:T(4,128)(2,1)S(1)} collective-permute-done((bf16[4,512]{1,0:T(4,128)(2,1)S(1)}, bf16[4,512]{1,0:T(4,128)(2,1)S(1)}, u32[]{:S(2)}, u32[]{:S(2)}) %collective-permute-start.15) | collective-permute-done | bytes 4128 | tf_op jit(solution)/shard_map/ppermute | solution.py:300
  42.6 0.6 %shard_map.159 = bf16[4,512]{1,0:T(4,128)(2,1)} custom-call(f32[4,512]{1,0:T(4,128)S(1)} %get-tuple-element.35.base, bf16[4,512]{1,0:T(4,128)(2,1)S(1)} %collective-permute-done.13.refs_0_, bf16[4,512]{1,0:T(4,128)(2,1)S(1)} %collective-permute-done.14.refs_1_, bf16[4,512]{1,0:T(4,128)(2,1)S(1)} %collective-permute-done.15.refs_2_), custom_call_target="tpu_custom_call" | custom-call | flops 10000000 | bytes 10000 | tf_op jit(solution)/shard_map/pallas_call | solution.py:27
  (45 shorter events, 0.2 us)
Async XLA Ops:
  0.6 4.1 %collective-permute-start = (bf16[4,512]{1,0:T(4,128)(2,1)}, bf16[4,512]{1,0:T(4,128)(2,1)S(1)}, u32[]{:S(2)}, u32[]{:S(2)}) collective-permute-start(bf16[4,512]{1,0:T(4,128)(2,1)} %refs_5_.1), channel_id=1, source_target_pairs={{0,1},{1,0},{2,3},{3,2},{4,5},{5,4},{6,7},{7,6},{8,9},{9,8},{10,11... | collective-permute-start | bytes 12296 | tf_op jit(solution)/shard_map/ppermute | solution.py:243
  4.8 11.5 %copy-start.3 = (f32[1,8,128,128]{3,2,1,0:T(8,128)S(1)}, f32[1,8,128,128]{3,2,1,0:T(8,128)}, u32[]{:S(2)}) copy-start(f32[1,8,128,128]{3,2,1,0:T(8,128)} %param.15) | copy-start | bytes 1572868
  4.8 11.5 %copy-start.4 = (f32[1024]{0:T(1024)S(1)}, f32[1024]{0:T(1024)}, u32[]{:S(2)}) copy-start(f32[1024]{0:T(1024)} %param.21) | copy-start | bytes 12292
  4.8 11.5 %copy-start.5 = (f32[1024]{0:T(1024)S(1)}, f32[1024]{0:T(1024)}, u32[]{:S(2)}) copy-start(f32[1024]{0:T(1024)} %param.22) | copy-start | bytes 12292
  5.5 5.3 %collective-permute-start.1 = (bf16[48,128]{1,0:T(8,128)(2,1)S(1)}, bf16[48,128]{1,0:T(8,128)(2,1)S(1)}, u32[]{:S(2)}, u32[]{:S(2)}) collective-permute-start(bf16[48,128]{1,0:T(8,128)(2,1)S(1)} %get-tuple-element.26), channel_id=1, source_target_pairs={{0,2},{2,0},{4,6},{6,4},{1,3},{3,1},{5,7},{7,5},{8,10},{10,8},{12,... | collective-permute-start | bytes 36872 | tf_op jit(solution)/shard_map/ppermute | solution.py:279
  8.2 4.6 %collective-permute-start.2 = (bf16[48,128]{1,0:T(8,128)(2,1)S(1)}, bf16[48,128]{1,0:T(8,128)(2,1)S(1)}, u32[]{:S(2)}, u32[]{:S(2)}) collective-permute-start(bf16[48,128]{1,0:T(8,128)(2,1)S(1)} %get-tuple-element.27), channel_id=1, source_target_pairs={{0,4},{2,6},{4,0},{6,2},{1,5},{3,7},{5,1},{7,3},{8,12},{10,14},{12... | collective-permute-start | bytes 36872 | tf_op jit(solution)/shard_map/ppermute | solution.py:279
  10.7 5.5 %collective-permute-start.3 = (bf16[48,128]{1,0:T(8,128)(2,1)S(1)}, bf16[48,128]{1,0:T(8,128)(2,1)S(1)}, u32[]{:S(2)}, u32[]{:S(2)}) collective-permute-start(bf16[48,128]{1,0:T(8,128)(2,1)S(1)} %get-tuple-element.28), channel_id=1, source_target_pairs={{0,6},{2,4},{4,2},{6,0},{1,7},{3,5},{5,3},{7,1},{8,14},{10,12},{12... | collective-permute-start | bytes 36872 | tf_op jit(solution)/shard_map/ppermute | solution.py:279
  16.2 13.0 %slice-start = ((s8[11534336]{0:T(1024)(128)(4,1)}), s8[4194304]{0:T(1024)(128)(4,1)S(1)}, s32[]{:S(2)}) async-start(s8[11534336]{0:T(1024)(128)(4,1)} %bitcast.7), calls=%async_computation | async-start | bytes 8388608
  16.2 13.0 %slice-start.3 = ((s8[11534336]{0:T(1024)(128)(4,1)}), s8[4194304]{0:T(1024)(128)(4,1)S(1)}, s32[]{:S(2)}) async-start(s8[11534336]{0:T(1024)(128)(4,1)} %bitcast.9), calls=%async_computation.3 | async-start | bytes 8388608
  16.2 13.0 %slice-start.6 = ((s8[11534336]{0:T(1024)(128)(4,1)}), s8[4194304]{0:T(1024)(128)(4,1)S(1)}, s32[]{:S(2)}) async-start(s8[11534336]{0:T(1024)(128)(4,1)} %bitcast.11), calls=%async_computation.6 | async-start | bytes 8388608
  16.3 7.3 %copy-start = (bf16[2048,512]{1,0:T(8,128)(2,1)S(1)}, bf16[2048,512]{1,0:T(8,128)(2,1)}, u32[]{:S(2)}) copy-start(bf16[2048,512]{1,0:T(8,128)(2,1)} %refs_4_.1) | copy-start | bytes 6291460
  16.3 7.3 %copy-start.2 = (bf16[4,512]{1,0:T(4,128)(2,1)S(1)}, bf16[4,512]{1,0:T(4,128)(2,1)}, u32[]{:S(2)}) copy-start(bf16[4,512]{1,0:T(4,128)(2,1)} %refs_5_.1) | copy-start | bytes 12292
  16.3 12.9 %slice-start.1 = ((s8[11534336]{0:T(1024)(128)(4,1)}), s8[4194304]{0:T(1024)(128)(4,1)S(1)}, s32[]{:S(2)}) async-start(s8[11534336]{0:T(1024)(128)(4,1)} %bitcast.7), calls=%async_computation.1 | async-start | bytes 8388608
  16.3 12.9 %slice-start.2 = ((s8[11534336]{0:T(1024)(128)(4,1)}), s8[3145728]{0:T(1024)(128)(4,1)S(1)}, s32[]{:S(2)}) async-start(s8[11534336]{0:T(1024)(128)(4,1)} %bitcast.7), calls=%async_computation.2 | async-start | bytes 6291456
  16.3 12.9 %slice-start.4 = ((s8[11534336]{0:T(1024)(128)(4,1)}), s8[4194304]{0:T(1024)(128)(4,1)S(1)}, s32[]{:S(2)}) async-start(s8[11534336]{0:T(1024)(128)(4,1)} %bitcast.9), calls=%async_computation.4 | async-start | bytes 8388608
  16.3 12.9 %slice-start.5 = ((s8[11534336]{0:T(1024)(128)(4,1)}), s8[3145728]{0:T(1024)(128)(4,1)S(1)}, s32[]{:S(2)}) async-start(s8[11534336]{0:T(1024)(128)(4,1)} %bitcast.9), calls=%async_computation.5 | async-start | bytes 6291456
  16.3 12.9 %slice-start.7 = ((s8[11534336]{0:T(1024)(128)(4,1)}), s8[4194304]{0:T(1024)(128)(4,1)S(1)}, s32[]{:S(2)}) async-start(s8[11534336]{0:T(1024)(128)(4,1)} %bitcast.11), calls=%async_computation.7 | async-start | bytes 8388608
  16.3 12.9 %slice-start.8 = ((s8[11534336]{0:T(1024)(128)(4,1)}), s8[3145728]{0:T(1024)(128)(4,1)S(1)}, s32[]{:S(2)}) async-start(s8[11534336]{0:T(1024)(128)(4,1)} %bitcast.11), calls=%async_computation.8 | async-start | bytes 6291456
  17.1 12.1 %copy-start.1 = (f32[4096]{0:T(1024)S(1)}, f32[4096]{0:T(1024)}, u32[]{:S(2)}) copy-start(f32[4096]{0:T(1024)} %param.24) | copy-start | bytes 49156
  17.1 1.2 %collective-permute-start.4 = (f32[8,128]{1,0:T(8,128)S(1)}, f32[8,128]{1,0:T(8,128)S(1)}, u32[]{:S(2)}, u32[]{:S(2)}) collective-permute-start(f32[8,128]{1,0:T(8,128)S(1)} %get-tuple-element.29.own), channel_id=1, source_target_pairs={{0,1},{1,0},{2,3},{3,2},{4,5},{5,4},{6,7},{7,6},{8,9},{9,8},{10,11... | collective-permute-start | bytes 12296 | tf_op jit(solution)/shard_map/ppermute | solution.py:297
  18.3 4.8 %collective-permute-start.7 = (bf16[16,128]{1,0:T(8,128)(2,1)S(1)}, bf16[16,128]{1,0:T(8,128)(2,1)S(1)}, u32[]{:S(2)}, u32[]{:S(2)}) collective-permute-start(bf16[16,128]{1,0:T(8,128)(2,1)S(1)} %shard_map.152.refs_0_), channel_id=1, source_target_pairs={{0,7},{1,6},{2,5},{3,4},{4,3},{5,2},{6,1},{7,0},{8,15},{9,14},{10,... | collective-permute-start | bytes 12296 | tf_op jit(solution)/shard_map/ppermute | solution.py:300
  18.3 4.8 %collective-permute-start.6 = (bf16[16,128]{1,0:T(8,128)(2,1)S(1)}, bf16[16,128]{1,0:T(8,128)(2,1)S(1)}, u32[]{:S(2)}, u32[]{:S(2)}) collective-permute-start(bf16[16,128]{1,0:T(8,128)(2,1)S(1)} %shard_map.152.refs_0_), channel_id=1, source_target_pairs={{0,5},{1,4},{2,7},{3,6},{4,1},{5,0},{6,3},{7,2},{8,13},{9,12},{10,... | collective-permute-start | bytes 12296 | tf_op jit(solution)/shard_map/ppermute | solution.py:300
  18.4 5.1 %collective-permute-start.5 = (bf16[16,128]{1,0:T(8,128)(2,1)S(1)}, bf16[16,128]{1,0:T(8,128)(2,1)S(1)}, u32[]{:S(2)}, u32[]{:S(2)}) collective-permute-start(bf16[16,128]{1,0:T(8,128)(2,1)S(1)} %shard_map.152.refs_0_), channel_id=1, source_target_pairs={{0,3},{1,2},{2,1},{3,0},{4,7},{5,6},{6,5},{7,4},{8,11},{9,10},{10,... | collective-permute-start | bytes 12296 | tf_op jit(solution)/shard_map/ppermute | solution.py:300
  23.9 1.2 %collective-permute-start.8 = (bf16[4,512]{1,0:T(4,128)(2,1)S(1)}, bf16[4,512]{1,0:T(4,128)(2,1)S(1)}, u32[]{:S(2)}, u32[]{:S(2)}) collective-permute-start(bf16[4,512]{1,0:T(4,128)(2,1)S(1)} %shard_map.153.own.mixed), channel_id=1, source_target_pairs={{0,1},{1,0},{2,3},{3,2},{4,5},{5,4},{6,7},{7,6},{8,9},{9,8},{10,11... | collective-permute-start | bytes 12296 | tf_op jit(solution)/shard_map/ppermute | solution.py:297
  25.1 5.0 %collective-permute-start.11 = (bf16[2,4,512]{2,1,0:T(4,128)(2,1)S(1)}, bf16[2,4,512]{2,1,0:T(4,128)(2,1)S(1)}, u32[]{:S(2)}, u32[]{:S(2)}) collective-permute-start(bf16[2,4,512]{2,1,0:T(4,128)(2,1)S(1)} %shard_map.154.block), channel_id=1, source_target_pairs={{0,7},{1,6},{2,5},{3,4},{4,3},{5,2},{6,1},{7,0},{8,15},{9,14},{10,... | collective-permute-start | bytes 24584 | tf_op jit(solution)/shard_map/ppermute | solution.py:300
  27.4 4.0 %collective-permute-start.10 = (bf16[2,4,512]{2,1,0:T(4,128)(2,1)S(1)}, bf16[2,4,512]{2,1,0:T(4,128)(2,1)S(1)}, u32[]{:S(2)}, u32[]{:S(2)}) collective-permute-start(bf16[2,4,512]{2,1,0:T(4,128)(2,1)S(1)} %shard_map.154.block), channel_id=1, source_target_pairs={{0,5},{1,4},{2,7},{3,6},{4,1},{5,0},{6,3},{7,2},{8,13},{9,12},{10,... | collective-permute-start | bytes 24584 | tf_op jit(solution)/shard_map/ppermute | solution.py:300
  28.3 3.2 %collective-permute-start.9 = (bf16[2,4,512]{2,1,0:T(4,128)(2,1)S(1)}, bf16[2,4,512]{2,1,0:T(4,128)(2,1)S(1)}, u32[]{:S(2)}, u32[]{:S(2)}) collective-permute-start(bf16[2,4,512]{2,1,0:T(4,128)(2,1)S(1)} %shard_map.154.block), channel_id=1, source_target_pairs={{0,3},{1,2},{2,1},{3,0},{4,7},{5,6},{6,5},{7,4},{8,11},{9,10},{10,... | collective-permute-start | bytes 24584 | tf_op jit(solution)/shard_map/ppermute | solution.py:300
  34.6 1.2 %collective-permute-start.12 = (bf16[4,4,512]{2,1,0:T(4,128)(2,1)S(1)}, bf16[4,4,512]{2,1,0:T(4,128)(2,1)S(1)}, u32[]{:S(2)}, u32[]{:S(2)}) collective-permute-start(bf16[4,4,512]{2,1,0:T(4,128)(2,1)S(1)} %get-tuple-element.34), channel_id=1, source_target_pairs={{0,1},{1,0},{2,3},{3,2},{4,5},{5,4},{6,7},{7,6},{8,9},{9,8},{10,11... | collective-permute-start | bytes 49160 | tf_op jit(solution)/shard_map/ppermute | solution.py:297
  35.8 4.8 %collective-permute-start.13 = (bf16[4,512]{1,0:T(4,128)(2,1)S(1)}, bf16[4,512]{1,0:T(4,128)(2,1)S(1)}, u32[]{:S(2)}, u32[]{:S(2)}) collective-permute-start(bf16[4,512]{1,0:T(4,128)(2,1)S(1)} %get-tuple-element.36), channel_id=1, source_target_pairs={{0,3},{1,2},{2,1},{3,0},{4,7},{5,6},{6,5},{7,4},{8,11},{9,10},{10,... | collective-permute-start | bytes 12296 | tf_op jit(solution)/shard_map/ppermute | solution.py:300
  36.7 3.9 %collective-permute-start.14 = (bf16[4,512]{1,0:T(4,128)(2,1)S(1)}, bf16[4,512]{1,0:T(4,128)(2,1)S(1)}, u32[]{:S(2)}, u32[]{:S(2)}) collective-permute-start(bf16[4,512]{1,0:T(4,128)(2,1)S(1)} %get-tuple-element.37), channel_id=1, source_target_pairs={{0,5},{1,4},{2,7},{3,6},{4,1},{5,0},{6,3},{7,2},{8,13},{9,12},{10,... | collective-permute-start | bytes 12296 | tf_op jit(solution)/shard_map/ppermute | solution.py:300
  37.7 4.8 %collective-permute-start.15 = (bf16[4,512]{1,0:T(4,128)(2,1)S(1)}, bf16[4,512]{1,0:T(4,128)(2,1)S(1)}, u32[]{:S(2)}, u32[]{:S(2)}) collective-permute-start(bf16[4,512]{1,0:T(4,128)(2,1)S(1)} %get-tuple-element.38), channel_id=1, source_target_pairs={{0,7},{1,6},{2,5},{3,4},{4,3},{5,2},{6,1},{7,0},{8,15},{9,14},{10,... | collective-permute-start | bytes 12296 | tf_op jit(solution)/shard_map/ppermute | solution.py:300

commit v5 on v4

--- a/solution.py
+++ b/solution.py
@@ -23,16 +23,22 @@
     return pltpu.with_memory_space_constraint(array, pltpu.VMEM)
 
 
-def call(body, outs, *args, streamed=(), scratch=(), limit=6 * 2**20, cost=SHORT):
+def call(
+    body, outs, *args, streamed=(), scratch=(), out_specs=None, limit=6 * 2**20, cost=SHORT
+):
     return pl.pallas_call(
         body,
         out_shape=outs,
         in_specs=[VMEM] * len(args) + [HBM] * len(streamed),
-        out_specs=jax.tree.map(lambda _: VMEM, outs),
+        out_specs=out_specs or jax.tree.map(lambda _: VMEM, outs),
         scratch_shapes=scratch,
         compiler_params=pltpu.CompilerParams(vmem_limit_bytes=limit),
         cost_estimate=cost,
     )(*args, *[pltpu.with_memory_space_constraint(w, pltpu.HBM) for w in streamed])
+
+
+def chip_order(kv_count):
+    return [*range(2, kv_count), 1]
 
 
 def silu(v):
@@ -87,7 +93,7 @@
     for at in range(row, every.shape[1]):
         every[:, at, :] = squares
     kept[...] = every[kv_index]
-    for j, out in enumerate(sent, 1):
+    for j, out in zip(chip_order(len(sent) + 1), sent):
         block = every[kv_index ^ j]
         high = block[row:].astype(jnp.bfloat16).astype(jnp.float32)
         wide = jnp.concatenate([block[:row], high, block[row:] - high], axis=0)
@@ -144,7 +150,7 @@
 def heads_body(*refs):
     *blocks, w_heads_out, tokens, mixed, every = refs
     kv_index = lax.axis_index("kv")
-    for j, block in enumerate(blocks):
+    for j, block in zip([0, *reversed(chip_order(len(blocks)))], blocks):
         every[kv_index ^ j] = block[...].astype(jnp.float32)
     left = jnp.concatenate([every[:, h, :] for h in range(every.shape[1])], axis=1)
     added = jnp.dot(
@@ -167,9 +173,23 @@
     )
 
 
-def mixer_own_body(block, mixer_gain, w_gate, w_up, w_down, gate, up, squares):
+def mixer_own_body(
+    block, mixer_gain, w_gate, w_up, w_down, new_state, gate, up, squares, state_out, sem
+):
+    leave = pltpu.make_async_copy(new_state, state_out, sem)
+    leave.start()
     gate[...], up[...], summed = mixer_block(0, block, mixer_gain, w_gate, w_up)
     squares[...] = jnp.broadcast_to(summed, squares.shape)
+    leave.wait()
+
+
+def mixer_next_body(
+    j, gate_in, up_in, squares_in, block, mixer_gain, w_gate, w_up, w_down, gate, up, squares
+):
+    more_gate, more_up, more = mixer_block(j, block, mixer_gain, w_gate, w_up)
+    gate[...] = gate_in[...] + more_gate
+    up[...] = up_in[...] + more_up
+    squares[...] = squares_in[...] + more
 
 
 def down_block(hidden, w_down, chip, core, width):
@@ -181,7 +201,7 @@
     gate, up, squares, *blocks = refs[:-6]
     mixer_gain, w_gate, w_up, w_down, hidden, passed = refs[-6:]
     gate_val, up_val, total = gate[...], up[...], squares[:, :1]
-    for j, block in enumerate(blocks, 1):
+    for j, block in zip(reversed(chip_order(lax.axis_size("kv"))), blocks):
         more_gate, more_up, more = mixer_block(j, block, mixer_gain, w_gate, w_up)
         gate_val, up_val, total = gate_val + more_gate, up_val + more_up, total + more
     scale = lax.rsqrt(total / w_gate.shape[0] + epsilon)
@@ -205,7 +225,7 @@
 
 def chip_sum_body(sums, passed, mixed, base, *sent):
     base[...] = mixed[...].astype(jnp.float32) + sums[0] + passed[0].astype(jnp.float32)
-    for j, out in enumerate(sent, 1):
+    for j, out in zip(chip_order(sums.shape[0]), sent):
         out[...] = (sums[j] + passed[j].astype(jnp.float32)).astype(jnp.bfloat16)
 
 
@@ -240,6 +260,7 @@
     heads = rec_state.shape[1]
     model_width = norm_gain.shape[0]
     shape = jax.ShapeDtypeStruct
+    others = chip_order(kv_count)
     other = lax.ppermute(tokens, "tp", [(i, (i + 1) % tp_count) for i in range(tp_count)])
     weights = (w_query, w_forget, w_input, w_outgate)
     half_shape = (4, own_width, w_query.shape[1])
@@ -277,7 +298,7 @@
     )
     received = [
         lax.ppermute(block, "kv", [(i, i ^ j) for i in range(kv_count)])
-        for j, block in enumerate(sent, 1)
+        for j, block in zip(others, sent)
     ]
     new_state, gated = call(
         lambda *refs: recur_body(model_width, len(received), *refs),
@@ -299,7 +320,10 @@
     def crossed(block, j):
         return lax.ppermute(block, GROUP, [(i, i ^ (2 * j + 1)) for i in range(group_count)])
 
-    others = range(1, kv_count)
+    def gather(block):
+        blocks = {j: crossed(block, j) for j in range(1, kv_count)}
+        return [blocks[j] for j in reversed(others)]
+
     pair = call(
         pair_body, shape((2 * heads, HEAD_DIM), jnp.bfloat16), gated, swapped(gated)
     )
@@ -307,7 +331,7 @@
         heads_body,
         shape((row_count, own_width), jnp.bfloat16),
         pair,
-        *[crossed(pair, j) for j in others],
+        *gather(pair),
         resident(w_heads_out),
         tokens,
         scratch=[pltpu.VMEM((kv_count, 2 * heads, HEAD_DIM), jnp.float32)],
@@ -315,23 +339,40 @@
     pair = call(
         pair_body, shape((2, row_count, own_width), jnp.bfloat16), mixed, swapped(mixed)
     )
-    blocks = [crossed(pair, j) for j in others]
+    *blocks, first = gather(pair)
     gain = mixer_gain[None]
     w_gate, w_up, w_down = resident(w_gate), resident(w_up), resident(w_down)
     width = w_gate.shape[1]
-    products = call(
+    product_shapes = (
+        shape((row_count, width), jnp.float32),
+        shape((row_count, width), jnp.float32),
+        shape((row_count, LANES), jnp.float32),
+    )
+    *products, new_state = call(
         mixer_own_body,
-        (
-            shape((row_count, width), jnp.float32),
-            shape((row_count, width), jnp.float32),
-            shape((row_count, LANES), jnp.float32),
-        ),
+        (*product_shapes, pltpu.HBM(new_state.shape, jnp.float32)),
         pair,
         gain,
         w_gate,
         w_up,
         w_down,
-    )
+        resident(new_state),
+        out_specs=(VMEM, VMEM, VMEM, HBM),
+        scratch=[pltpu.SemaphoreType.DMA],
+    )
+    if blocks:
+        products = call(
+            lambda *refs: mixer_next_body(others[0], *refs),
+            product_shapes,
+            *products,
+            first,
+            gain,
+            w_gate,
+            w_up,
+            w_down,
+        )
+    else:
+        blocks = [first]
     hidden, passed = call(
         mixer_body,
         (
@@ -361,7 +402,7 @@
         result_body,
         shape(mixed.shape, jnp.bfloat16),
         base,
-        *[crossed(block, j) for j, block in enumerate(sent, 1)],
+        *[crossed(block, j) for j, block in zip(others, sent)],
     )
     return (result, new_state[None])
 

time: 43.4 us -> 40.2 us (0.926)
  starting transfers between devices: 18.3 us -> 15.9 us
  local copies, waits for them, and re-layouts: 0.87 us -> 0.07 us
    ppermute x9, starting transfers between devices: 11.9 us -> 9.37 us  [crossed(): lax.ppermute(block, GROUP, [(i, i ^ 2 * j + 1) for i in range(group_count)])]
    ppermute x9, waiting for transfers between devices: 4.64 us -> 6.24 us  [crossed(): lax.ppermute(block, GROUP, [(i, i ^ 2 * j + 1) for i in range(group_count)])]
    ppermute x3, waiting for transfers between devices: 5.49 us -> 3.91 us  [local(): lax.ppermute(block, 'kv', [(i, i ^ j) for i in range(kv_count)])]
    unnamed x31 -> x30, local copies, waits for them, and re-layouts: 0.87 us -> 0.07 us
    pallas_call x11 -> x12, Pallas kernels: 10.8 us -> 11 us  [call(): pl.pallas_call(body, out_shape=outs, in_specs=[VMEM] * len(args) + [HBM]...]
  transfers between devices with their start and end apart: 16 -> 16, of which waited for: 9 -> 9; matrix products, arithmetic and copies ran while one was open for 2% -> 0% of each run, Pallas kernels for 12% -> 15%
where the time goes in v5:
time: 40.2 us; the launch traced here: 40 us
  starting transfers between devices  15.9 us (40%)
  waiting for transfers between devices  12.2 us (30%)
  Pallas kernels  11 us (27%)
  between operations  0.9 us (2%)
    pallas_call x12, Pallas kernels, call(): pl.pallas_call(body, out_shape=outs, in_specs=[VMEM] * len(args) + [HBM]...  11 us
    ppermute x9, starting transfers between devices, crossed(): lax.ppermute(block, GROUP, [(i, i ^ 2 * j + 1) for i in range(group_count)])  9.37 us
    ppermute x9, waiting for transfers between devices, crossed(): lax.ppermute(block, GROUP, [(i, i ^ 2 * j + 1) for i in range(group_count)])  6.24 us
    ppermute x3, starting transfers between devices, local(): lax.ppermute(block, 'kv', [(i, i ^ j) for i in range(kv_count)])  5.25 us
    ppermute x3, waiting for transfers between devices, local(): lax.ppermute(block, 'kv', [(i, i ^ j) for i in range(kv_count)])  3.91 us
    ppermute x3, waiting for transfers between devices, swapped(): return lax.ppermute(block, 'tp', [(0, 1), (1, 0)])  2.01 us
  transfers between devices with their start and end apart: 16, of which 9 were waited for; matrix products, arithmetic and copies ran while one was open for 0% of the time, Pallas kernels for 15%

profile of v5, /device:TPU:0, one launch (start us, length us, event | category | flops | bytes accessed | tf_op | source)
XLA Modules:
  0.0 40.0 jit_solution(8960996999142180213)
XLA Ops:
  0.6 0.6 %collective-permute-start = (bf16[4,512]{1,0:T(4,128)(2,1)}, bf16[4,512]{1,0:T(4,128)(2,1)S(1)}, u32[]{:S(2)}, u32[]{:S(2)}) collective-permute-start(bf16[4,512]{1,0:T(4,128)(2,1)} %refs_5_.2), channel_id=1, source_target_pairs={{0,1},{1,0},{2,3},{3,2},{4,5},{5,4},{6,7},{7,6},{8,9},{9,8},{10,11... | collective-permute-start | bytes 12296 | tf_op jit(solution)/shard_map/ppermute | solution.py:264
  1.2 3.6 %shard_map.149 = (f32[4,4,1024]{2,1,0:T(4,128)S(1)}, f32[4,128]{1,0:T(4,128)S(1)}, f32[1,512]{1,0:T(1,128)S(1)}, bf16[4,512,1024]{2,1,0:T(8,128)(2,1)S(1)}) custom-call(bf16[4,512]{1,0:T(4,128)(2,1)} %refs_5_.2, f32[1,4096]{1,0:T(1,128)} %bitcast.18, bf16[1024,1024]{1,0:T(8,128)(2,1)} %w_query.1, bf16[1024,1024]{1,0:T(8,128)(2,1)} %w_forget.1, ...), custom_call_target="tpu_custom_call" | custom-call | flops 10000000 | bytes 10000 | tf_op jit(solution)/shard_map/pallas_call | solution.py:29
  4.8 0.7 %shard_map.150 = (f32[40,128]{1,0:T(8,128)S(1)}, bf16[48,128]{1,0:T(8,128)(2,1)S(1)}, bf16[48,128]{1,0:T(8,128)(2,1)S(1)}, bf16[48,128]{1,0:T(8,128)(2,1)S(1)}) custom-call(bf16[4,512]{1,0:T(4,128)(2,1)S(1)} %collective-permute-done.other, f32[4,4,1024]{2,1,0:T(4,128)S(1)} %get-tuple-element.25.own, f32[4,128]{1,0:T(4,128)S(1)} %get-tuple-element.26.own_squares, ...), custom_call_target="tpu_custom_call" | custom-call | flops 99999997952 | bytes 10000 | tf_op jit(solution)/shard_map/pallas_call | solution.py:29
  5.5 3.7 %collective-permute-start.1 = (bf16[48,128]{1,0:T(8,128)(2,1)S(1)}, bf16[48,128]{1,0:T(8,128)(2,1)S(1)}, u32[]{:S(2)}, u32[]{:S(2)}) collective-permute-start(bf16[48,128]{1,0:T(8,128)(2,1)S(1)} %get-tuple-element.30), channel_id=1, source_target_pairs={{0,4},{2,6},{4,0},{6,2},{1,5},{3,7},{5,1},{7,3},{8,12},{10,14},{12... | collective-permute-start | bytes 36872 | tf_op jit(solution)/shard_map/ppermute | solution.py:300
  9.2 1.3 %collective-permute-start.2 = (bf16[48,128]{1,0:T(8,128)(2,1)S(1)}, bf16[48,128]{1,0:T(8,128)(2,1)S(1)}, u32[]{:S(2)}, u32[]{:S(2)}) collective-permute-start(bf16[48,128]{1,0:T(8,128)(2,1)S(1)} %get-tuple-element.31), channel_id=1, source_target_pairs={{0,6},{2,4},{4,2},{6,0},{1,7},{3,5},{5,3},{7,1},{8,14},{10,12},{12... | collective-permute-start | bytes 36872 | tf_op jit(solution)/shard_map/ppermute | solution.py:300
  10.5 0.2 collective-permute-start.3
  10.8 3.8 %collective-permute-done.2.refs_2_ = bf16[48,128]{1,0:T(8,128)(2,1)S(1)} collective-permute-done((bf16[48,128]{1,0:T(8,128)(2,1)S(1)}, bf16[48,128]{1,0:T(8,128)(2,1)S(1)}, u32[]{:S(2)}, u32[]{:S(2)}) %collective-permute-start.2) | collective-permute-done | bytes 12320 | tf_op jit(solution)/shard_map/ppermute | solution.py:300
  14.8 0.8 %shard_map.151 = (f32[8,128,128]{2,1,0:T(8,128)S(1)}, f32[8,128]{1,0:T(8,128)S(1)}) custom-call(f32[40,128]{1,0:T(8,128)S(1)} %get-tuple-element.29.refs_0_, bf16[48,128]{1,0:T(8,128)(2,1)S(1)} %collective-permute-done.1.refs_1_, bf16[48,128]{1,0:T(8,128)(2,1)S(1)} %collective-permute-done.2.refs_2_, bf16[48,128]{1,0:T(8,128)(2,1)S(1)} %collective-permute-done.3.refs_3_, ...), custom_call_target="tpu_custom_call" | custom-call | flops 99999997952 | bytes 10000 | tf_op jit(solution)/shard_map/pallas_call | solution.py:29
  15.6 1.2 %collective-permute-done.4.other = f32[8,128]{1,0:T(8,128)S(1)} collective-permute-done((f32[8,128]{1,0:T(8,128)S(1)}, f32[8,128]{1,0:T(8,128)S(1)}, u32[]{:S(2)}, u32[]{:S(2)}) %collective-permute-start.4) | collective-permute-done | bytes 4128 | tf_op jit(solution)/shard_map/ppermute | solution.py:318
  16.8 1.0 %collective-permute-start.7 = (bf16[16,128]{1,0:T(8,128)(2,1)S(1)}, bf16[16,128]{1,0:T(8,128)(2,1)S(1)}, u32[]{:S(2)}, u32[]{:S(2)}) collective-permute-start(bf16[16,128]{1,0:T(8,128)(2,1)S(1)} %shard_map.152.refs_0_), channel_id=1, source_target_pairs={{0,5},{1,4},{2,7},{3,6},{4,1},{5,0},{6,3},{7,2},{8,13},{9,12},{10,... | collective-permute-start | bytes 12296 | tf_op jit(solution)/shard_map/ppermute | solution.py:321
  17.8 1.0 %collective-permute-start.6 = (bf16[16,128]{1,0:T(8,128)(2,1)S(1)}, bf16[16,128]{1,0:T(8,128)(2,1)S(1)}, u32[]{:S(2)}, u32[]{:S(2)}) collective-permute-start(bf16[16,128]{1,0:T(8,128)(2,1)S(1)} %shard_map.152.refs_0_), channel_id=1, source_target_pairs={{0,7},{1,6},{2,5},{3,4},{4,3},{5,2},{6,1},{7,0},{8,15},{9,14},{10,... | collective-permute-start | bytes 12296 | tf_op jit(solution)/shard_map/ppermute | solution.py:321
  18.7 1.0 %collective-permute-start.5 = (bf16[16,128]{1,0:T(8,128)(2,1)S(1)}, bf16[16,128]{1,0:T(8,128)(2,1)S(1)}, u32[]{:S(2)}, u32[]{:S(2)}) collective-permute-start(bf16[16,128]{1,0:T(8,128)(2,1)S(1)} %shard_map.152.refs_0_), channel_id=1, source_target_pairs={{0,3},{1,2},{2,1},{3,0},{4,7},{5,6},{6,5},{7,4},{8,11},{9,10},{10,... | collective-permute-start | bytes 12296 | tf_op jit(solution)/shard_map/ppermute | solution.py:321
  19.7 0.9 %collective-permute-done.7.refs_3_ = bf16[16,128]{1,0:T(8,128)(2,1)S(1)} collective-permute-done((bf16[16,128]{1,0:T(8,128)(2,1)S(1)}, bf16[16,128]{1,0:T(8,128)(2,1)S(1)}, u32[]{:S(2)}, u32[]{:S(2)}) %collective-permute-start.7) | collective-permute-done | bytes 4128 | tf_op jit(solution)/shard_map/ppermute | solution.py:321
  20.7 1.9 %collective-permute-done.6.refs_2_ = bf16[16,128]{1,0:T(8,128)(2,1)S(1)} collective-permute-done((bf16[16,128]{1,0:T(8,128)(2,1)S(1)}, bf16[16,128]{1,0:T(8,128)(2,1)S(1)}, u32[]{:S(2)}, u32[]{:S(2)}) %collective-permute-start.6) | collective-permute-done | bytes 4128 | tf_op jit(solution)/shard_map/ppermute | solution.py:321
  22.6 0.4 shard_map.153.own.mixed
  23.0 0.4 collective-permute-start.8
  23.3 0.8 %collective-permute-done.8.other = bf16[4,512]{1,0:T(4,128)(2,1)S(1)} collective-permute-done((bf16[4,512]{1,0:T(4,128)(2,1)S(1)}, bf16[4,512]{1,0:T(4,128)(2,1)S(1)}, u32[]{:S(2)}, u32[]{:S(2)}) %collective-permute-start.8) | collective-permute-done | bytes 4128 | tf_op jit(solution)/shard_map/ppermute | solution.py:318
  24.2 0.8 %collective-permute-start.9 = (bf16[2,4,512]{2,1,0:T(4,128)(2,1)S(1)}, bf16[2,4,512]{2,1,0:T(4,128)(2,1)S(1)}, u32[]{:S(2)}, u32[]{:S(2)}) collective-permute-start(bf16[2,4,512]{2,1,0:T(4,128)(2,1)S(1)} %shard_map.154.block), channel_id=1, source_target_pairs={{0,5},{1,4},{2,7},{3,6},{4,1},{5,0},{6,3},{7,2},{8,13},{9,12},{10,... | collective-permute-start | bytes 24584 | tf_op jit(solution)/shard_map/ppermute | solution.py:321
  25.0 1.8 %collective-permute-start.11 = (bf16[2,4,512]{2,1,0:T(4,128)(2,1)S(1)}, bf16[2,4,512]{2,1,0:T(4,128)(2,1)S(1)}, u32[]{:S(2)}, u32[]{:S(2)}) collective-permute-start(bf16[2,4,512]{2,1,0:T(4,128)(2,1)S(1)} %shard_map.154.block), channel_id=1, source_target_pairs={{0,7},{1,6},{2,5},{3,4},{4,3},{5,2},{6,1},{7,0},{8,15},{9,14},{10,... | collective-permute-start | bytes 24584 | tf_op jit(solution)/shard_map/ppermute | solution.py:321
  26.7 0.7 %collective-permute-start.10 = (bf16[2,4,512]{2,1,0:T(4,128)(2,1)S(1)}, bf16[2,4,512]{2,1,0:T(4,128)(2,1)S(1)}, u32[]{:S(2)}, u32[]{:S(2)}) collective-permute-start(bf16[2,4,512]{2,1,0:T(4,128)(2,1)S(1)} %shard_map.154.block), channel_id=1, source_target_pairs={{0,3},{1,2},{2,1},{3,0},{4,7},{5,6},{6,5},{7,4},{8,11},{9,10},{10,... | collective-permute-start | bytes 24584 | tf_op jit(solution)/shard_map/ppermute | solution.py:321
  27.5 0.9 %shard_map.155 = (f32[4,1408]{1,0:T(4,128)S(1)}, f32[4,1408]{1,0:T(4,128)S(1)}, f32[4,128]{1,0:T(4,128)S(1)}, f32[8,128,128]{2,1,0:T(8,128)}) custom-call(bf16[2,4,512]{2,1,0:T(4,128)(2,1)S(1)} %shard_map.154.block, f32[1,4096]{1,0:T(1,128)S(1)} %bitcast.12, bf16[4096,1408]{1,0:T(8,128)(2,1)S(1)} %bitcast.9, bf16[4096,1408]{1,0:T(8,128)(2,1)S(1)} %bitcast.11, ...), custom_call_target="tpu_custom_call" | custom-call | flops 10000000 | bytes 10000 | tf_op jit(solution)/shard_map/pallas_call | solution.py:29
  28.4 0.9 %shard_map.156 = (f32[4,1408]{1,0:T(4,128)S(1)}, f32[4,1408]{1,0:T(4,128)S(1)}, f32[4,128]{1,0:T(4,128)S(1)}) custom-call(f32[4,1408]{1,0:T(4,128)S(1)} %get-tuple-element.35.refs_0_, f32[4,1408]{1,0:T(4,128)S(1)} %get-tuple-element.36.refs_1_, f32[4,128]{1,0:T(4,128)S(1)} %get-tuple-element.37.refs_2_, ...), custom_call_target="tpu_custom_call" | custom-call | flops 10000000 | bytes 10000 | tf_op jit(solution)/shard_map/pallas_call | solution.py:29
  29.3 0.6 %collective-permute-done.11.refs_4_ = bf16[2,4,512]{2,1,0:T(4,128)(2,1)S(1)} collective-permute-done((bf16[2,4,512]{2,1,0:T(4,128)(2,1)S(1)}, bf16[2,4,512]{2,1,0:T(4,128)(2,1)S(1)}, u32[]{:S(2)}, u32[]{:S(2)}) %collective-permute-start.11) | collective-permute-done | bytes 8224 | tf_op jit(solution)/shard_map/ppermute | solution.py:321
  29.9 2.4 %shard_map.157 = (bf16[4,1408]{1,0:T(4,128)(2,1)S(1)}, bf16[4,4,512]{2,1,0:T(4,128)(2,1)S(1)}) custom-call(f32[4,1408]{1,0:T(4,128)S(1)} %get-tuple-element.38.refs_0_, f32[4,1408]{1,0:T(4,128)S(1)} %get-tuple-element.39.refs_1_, f32[4,128]{1,0:T(4,128)S(1)} %get-tuple-element.40.refs_2_, bf16[2,4,512]{2,1,0:T(4,128)(2,1)S(1)} %collective-permute-done.10.refs_3_, ...), custom_call_target="tpu_custom_call" | custom-call | flops 10000000 | bytes 10000 | tf_op jit(solution)/shard_map/pallas_call | solution.py:29
  32.3 0.3 collective-permute-start.12
  32.6 0.9 %shard_map.158.sums = f32[4,4,512]{2,1,0:T(4,128)S(1)} custom-call(bf16[4,1408]{1,0:T(4,128)(2,1)S(1)} %get-tuple-element.41.hidden, bf16[1408,4096]{1,0:T(8,128)(2,1)S(1)} %bitcast.7), custom_call_target="tpu_custom_call" | custom-call | flops 10000000 | bytes 10000 | tf_op jit(solution)/shard_map/pallas_call | solution.py:29
  33.5 1.1 %collective-permute-start.13 = (bf16[4,512]{1,0:T(4,128)(2,1)S(1)}, bf16[4,512]{1,0:T(4,128)(2,1)S(1)}, u32[]{:S(2)}, u32[]{:S(2)}) collective-permute-start(bf16[4,512]{1,0:T(4,128)(2,1)S(1)} %get-tuple-element.44), channel_id=1, source_target_pairs={{0,5},{1,4},{2,7},{3,6},{4,1},{5,0},{6,3},{7,2},{8,13},{9,12},{10,... | collective-permute-start | bytes 12296 | tf_op jit(solution)/shard_map/ppermute | solution.py:321
  34.6 1.7 %collective-permute-start.14 = (bf16[4,512]{1,0:T(4,128)(2,1)S(1)}, bf16[4,512]{1,0:T(4,128)(2,1)S(1)}, u32[]{:S(2)}, u32[]{:S(2)}) collective-permute-start(bf16[4,512]{1,0:T(4,128)(2,1)S(1)} %get-tuple-element.45), channel_id=1, source_target_pairs={{0,7},{1,6},{2,5},{3,4},{4,3},{5,2},{6,1},{7,0},{8,15},{9,14},{10,... | collective-permute-start | bytes 12296 | tf_op jit(solution)/shard_map/ppermute | solution.py:321
  36.3 0.4 collective-permute-start.15
  36.6 0.8 %collective-permute-done.13.refs_0_ = bf16[4,512]{1,0:T(4,128)(2,1)S(1)} collective-permute-done((bf16[4,512]{1,0:T(4,128)(2,1)S(1)}, bf16[4,512]{1,0:T(4,128)(2,1)S(1)}, u32[]{:S(2)}, u32[]{:S(2)}) %collective-permute-start.13) | collective-permute-done | bytes 4128 | tf_op jit(solution)/shard_map/ppermute | solution.py:321
  37.5 1.9 %collective-permute-done.14.refs_1_ = bf16[4,512]{1,0:T(4,128)(2,1)S(1)} collective-permute-done((bf16[4,512]{1,0:T(4,128)(2,1)S(1)}, bf16[4,512]{1,0:T(4,128)(2,1)S(1)}, u32[]{:S(2)}, u32[]{:S(2)}) %collective-permute-start.14) | collective-permute-done | bytes 4128 | tf_op jit(solution)/shard_map/ppermute | solution.py:321
  39.4 0.6 %shard_map.160 = bf16[4,512]{1,0:T(4,128)(2,1)} custom-call(f32[4,512]{1,0:T(4,128)S(1)} %get-tuple-element.43.base, bf16[4,512]{1,0:T(4,128)(2,1)S(1)} %collective-permute-done.13.refs_0_, bf16[4,512]{1,0:T(4,128)(2,1)S(1)} %collective-permute-done.14.refs_1_, bf16[4,512]{1,0:T(4,128)(2,1)S(1)} %collective-permute-done.15.refs_2_), custom_call_target="tpu_custom_call" | custom-call | flops 10000000 | bytes 10000 | tf_op jit(solution)/shard_map/pallas_call | solution.py:29
  (45 shorter events, 0.3 us)
Async XLA Ops:
  0.6 4.1 %collective-permute-start = (bf16[4,512]{1,0:T(4,128)(2,1)}, bf16[4,512]{1,0:T(4,128)(2,1)S(1)}, u32[]{:S(2)}, u32[]{:S(2)}) collective-permute-start(bf16[4,512]{1,0:T(4,128)(2,1)} %refs_5_.2), channel_id=1, source_target_pairs={{0,1},{1,0},{2,3},{3,2},{4,5},{5,4},{6,7},{7,6},{8,9},{9,8},{10,11... | collective-permute-start | bytes 12296 | tf_op jit(solution)/shard_map/ppermute | solution.py:264
  4.8 9.9 %copy-start.3 = (f32[1,8,128,128]{3,2,1,0:T(8,128)S(1)}, f32[1,8,128,128]{3,2,1,0:T(8,128)}, u32[]{:S(2)}) copy-start(f32[1,8,128,128]{3,2,1,0:T(8,128)} %param.15) | copy-start | bytes 1572868
  4.8 9.9 %copy-start.4 = (f32[1024]{0:T(1024)S(1)}, f32[1024]{0:T(1024)}, u32[]{:S(2)}) copy-start(f32[1024]{0:T(1024)} %param.21) | copy-start | bytes 12292
  4.8 9.9 %copy-start.5 = (f32[1024]{0:T(1024)S(1)}, f32[1024]{0:T(1024)}, u32[]{:S(2)}) copy-start(f32[1024]{0:T(1024)} %param.22) | copy-start | bytes 12292
  5.5 5.3 %collective-permute-start.1 = (bf16[48,128]{1,0:T(8,128)(2,1)S(1)}, bf16[48,128]{1,0:T(8,128)(2,1)S(1)}, u32[]{:S(2)}, u32[]{:S(2)}) collective-permute-start(bf16[48,128]{1,0:T(8,128)(2,1)S(1)} %get-tuple-element.30), channel_id=1, source_target_pairs={{0,4},{2,6},{4,0},{6,2},{1,5},{3,7},{5,1},{7,3},{8,12},{10,14},{12... | collective-permute-start | bytes 36872 | tf_op jit(solution)/shard_map/ppermute | solution.py:300
  9.2 5.5 %collective-permute-start.2 = (bf16[48,128]{1,0:T(8,128)(2,1)S(1)}, bf16[48,128]{1,0:T(8,128)(2,1)S(1)}, u32[]{:S(2)}, u32[]{:S(2)}) collective-permute-start(bf16[48,128]{1,0:T(8,128)(2,1)S(1)} %get-tuple-element.31), channel_id=1, source_target_pairs={{0,6},{2,4},{4,2},{6,0},{1,7},{3,5},{5,3},{7,1},{8,14},{10,12},{12... | collective-permute-start | bytes 36872 | tf_op jit(solution)/shard_map/ppermute | solution.py:300
  10.5 4.1 %collective-permute-start.3 = (bf16[48,128]{1,0:T(8,128)(2,1)S(1)}, bf16[48,128]{1,0:T(8,128)(2,1)S(1)}, u32[]{:S(2)}, u32[]{:S(2)}) collective-permute-start(bf16[48,128]{1,0:T(8,128)(2,1)S(1)} %get-tuple-element.32), channel_id=1, source_target_pairs={{0,2},{2,0},{4,6},{6,4},{1,3},{3,1},{5,7},{7,5},{8,10},{10,8},{12,... | collective-permute-start | bytes 36872 | tf_op jit(solution)/shard_map/ppermute | solution.py:300
  14.7 12.7 %slice-start = ((s8[11534336]{0:T(1024)(128)(4,1)}), s8[4194304]{0:T(1024)(128)(4,1)S(1)}, s32[]{:S(2)}) async-start(s8[11534336]{0:T(1024)(128)(4,1)} %bitcast.6), calls=%async_computation | async-start | bytes 8388608
  14.7 12.7 %slice-start.3 = ((s8[11534336]{0:T(1024)(128)(4,1)}), s8[4194304]{0:T(1024)(128)(4,1)S(1)}, s32[]{:S(2)}) async-start(s8[11534336]{0:T(1024)(128)(4,1)} %bitcast.8), calls=%async_computation.3 | async-start | bytes 8388608
  14.7 12.7 %slice-start.6 = ((s8[11534336]{0:T(1024)(128)(4,1)}), s8[4194304]{0:T(1024)(128)(4,1)S(1)}, s32[]{:S(2)}) async-start(s8[11534336]{0:T(1024)(128)(4,1)} %bitcast.10), calls=%async_computation.6 | async-start | bytes 8388608
  14.7 7.9 %copy-start = (bf16[2048,512]{1,0:T(8,128)(2,1)S(1)}, bf16[2048,512]{1,0:T(8,128)(2,1)}, u32[]{:S(2)}) copy-start(bf16[2048,512]{1,0:T(8,128)(2,1)} %refs_4_.1) | copy-start | bytes 6291460
  14.7 7.9 %copy-start.2 = (bf16[4,512]{1,0:T(4,128)(2,1)S(1)}, bf16[4,512]{1,0:T(4,128)(2,1)}, u32[]{:S(2)}) copy-start(bf16[4,512]{1,0:T(4,128)(2,1)} %refs_5_.2) | copy-start | bytes 12292
  14.7 12.7 %slice-start.1 = ((s8[11534336]{0:T(1024)(128)(4,1)}), s8[4194304]{0:T(1024)(128)(4,1)S(1)}, s32[]{:S(2)}) async-start(s8[11534336]{0:T(1024)(128)(4,1)} %bitcast.6), calls=%async_computation.1 | async-start | bytes 8388608
  14.7 12.7 %slice-start.2 = ((s8[11534336]{0:T(1024)(128)(4,1)}), s8[3145728]{0:T(1024)(128)(4,1)S(1)}, s32[]{:S(2)}) async-start(s8[11534336]{0:T(1024)(128)(4,1)} %bitcast.6), calls=%async_computation.2 | async-start | bytes 6291456
  14.8 12.7 %slice-start.4 = ((s8[11534336]{0:T(1024)(128)(4,1)}), s8[4194304]{0:T(1024)(128)(4,1)S(1)}, s32[]{:S(2)}) async-start(s8[11534336]{0:T(1024)(128)(4,1)} %bitcast.8), calls=%async_computation.4 | async-start | bytes 8388608
  14.8 12.7 %slice-start.5 = ((s8[11534336]{0:T(1024)(128)(4,1)}), s8[3145728]{0:T(1024)(128)(4,1)S(1)}, s32[]{:S(2)}) async-start(s8[11534336]{0:T(1024)(128)(4,1)} %bitcast.8), calls=%async_computation.5 | async-start | bytes 6291456
  14.8 12.7 %slice-start.7 = ((s8[11534336]{0:T(1024)(128)(4,1)}), s8[4194304]{0:T(1024)(128)(4,1)S(1)}, s32[]{:S(2)}) async-start(s8[11534336]{0:T(1024)(128)(4,1)} %bitcast.10), calls=%async_computation.7 | async-start | bytes 8388608
  14.8 12.7 %slice-start.8 = ((s8[11534336]{0:T(1024)(128)(4,1)}), s8[3145728]{0:T(1024)(128)(4,1)S(1)}, s32[]{:S(2)}) async-start(s8[11534336]{0:T(1024)(128)(4,1)} %bitcast.10), calls=%async_computation.8 | async-start | bytes 6291456
  15.5 11.9 %copy-start.1 = (f32[4096]{0:T(1024)S(1)}, f32[4096]{0:T(1024)}, u32[]{:S(2)}) copy-start(f32[4096]{0:T(1024)} %param.24) | copy-start | bytes 49156
  15.6 1.2 %collective-permute-start.4 = (f32[8,128]{1,0:T(8,128)S(1)}, f32[8,128]{1,0:T(8,128)S(1)}, u32[]{:S(2)}, u32[]{:S(2)}) collective-permute-start(f32[8,128]{1,0:T(8,128)S(1)} %get-tuple-element.33.own), channel_id=1, source_target_pairs={{0,1},{1,0},{2,3},{3,2},{4,5},{5,4},{6,7},{7,6},{8,9},{9,8},{10,11... | collective-permute-start | bytes 12296 | tf_op jit(solution)/shard_map/ppermute | solution.py:318
  16.8 3.9 %collective-permute-start.7 = (bf16[16,128]{1,0:T(8,128)(2,1)S(1)}, bf16[16,128]{1,0:T(8,128)(2,1)S(1)}, u32[]{:S(2)}, u32[]{:S(2)}) collective-permute-start(bf16[16,128]{1,0:T(8,128)(2,1)S(1)} %shard_map.152.refs_0_), channel_id=1, source_target_pairs={{0,5},{1,4},{2,7},{3,6},{4,1},{5,0},{6,3},{7,2},{8,13},{9,12},{10,... | collective-permute-start | bytes 12296 | tf_op jit(solution)/shard_map/ppermute | solution.py:321
  17.8 4.8 %collective-permute-start.6 = (bf16[16,128]{1,0:T(8,128)(2,1)S(1)}, bf16[16,128]{1,0:T(8,128)(2,1)S(1)}, u32[]{:S(2)}, u32[]{:S(2)}) collective-permute-start(bf16[16,128]{1,0:T(8,128)(2,1)S(1)} %shard_map.152.refs_0_), channel_id=1, source_target_pairs={{0,7},{1,6},{2,5},{3,4},{4,3},{5,2},{6,1},{7,0},{8,15},{9,14},{10,... | collective-permute-start | bytes 12296 | tf_op jit(solution)/shard_map/ppermute | solution.py:321
  18.7 3.8 %collective-permute-start.5 = (bf16[16,128]{1,0:T(8,128)(2,1)S(1)}, bf16[16,128]{1,0:T(8,128)(2,1)S(1)}, u32[]{:S(2)}, u32[]{:S(2)}) collective-permute-start(bf16[16,128]{1,0:T(8,128)(2,1)S(1)} %shard_map.152.refs_0_), channel_id=1, source_target_pairs={{0,3},{1,2},{2,1},{3,0},{4,7},{5,6},{6,5},{7,4},{8,11},{9,10},{10,... | collective-permute-start | bytes 12296 | tf_op jit(solution)/shard_map/ppermute | solution.py:321
  23.0 1.2 %collective-permute-start.8 = (bf16[4,512]{1,0:T(4,128)(2,1)S(1)}, bf16[4,512]{1,0:T(4,128)(2,1)S(1)}, u32[]{:S(2)}, u32[]{:S(2)}) collective-permute-start(bf16[4,512]{1,0:T(4,128)(2,1)S(1)} %shard_map.153.own.mixed), channel_id=1, source_target_pairs={{0,1},{1,0},{2,3},{3,2},{4,5},{5,4},{6,7},{7,6},{8,9},{9,8},{10,11... | collective-permute-start | bytes 12296 | tf_op jit(solution)/shard_map/ppermute | solution.py:318
  24.2 4.2 %collective-permute-start.9 = (bf16[2,4,512]{2,1,0:T(4,128)(2,1)S(1)}, bf16[2,4,512]{2,1,0:T(4,128)(2,1)S(1)}, u32[]{:S(2)}, u32[]{:S(2)}) collective-permute-start(bf16[2,4,512]{2,1,0:T(4,128)(2,1)S(1)} %shard_map.154.block), channel_id=1, source_target_pairs={{0,5},{1,4},{2,7},{3,6},{4,1},{5,0},{6,3},{7,2},{8,13},{9,12},{10,... | collective-permute-start | bytes 24584 | tf_op jit(solution)/shard_map/ppermute | solution.py:321
  25.0 4.9 %collective-permute-start.11 = (bf16[2,4,512]{2,1,0:T(4,128)(2,1)S(1)}, bf16[2,4,512]{2,1,0:T(4,128)(2,1)S(1)}, u32[]{:S(2)}, u32[]{:S(2)}) collective-permute-start(bf16[2,4,512]{2,1,0:T(4,128)(2,1)S(1)} %shard_map.154.block), channel_id=1, source_target_pairs={{0,7},{1,6},{2,5},{3,4},{4,3},{5,2},{6,1},{7,0},{8,15},{9,14},{10,... | collective-permute-start | bytes 24584 | tf_op jit(solution)/shard_map/ppermute | solution.py:321
  26.7 3.2 %collective-permute-start.10 = (bf16[2,4,512]{2,1,0:T(4,128)(2,1)S(1)}, bf16[2,4,512]{2,1,0:T(4,128)(2,1)S(1)}, u32[]{:S(2)}, u32[]{:S(2)}) collective-permute-start(bf16[2,4,512]{2,1,0:T(4,128)(2,1)S(1)} %shard_map.154.block), channel_id=1, source_target_pairs={{0,3},{1,2},{2,1},{3,0},{4,7},{5,6},{6,5},{7,4},{8,11},{9,10},{10,... | collective-permute-start | bytes 24584 | tf_op jit(solution)/shard_map/ppermute | solution.py:321
  32.3 1.2 %collective-permute-start.12 = (bf16[4,4,512]{2,1,0:T(4,128)(2,1)S(1)}, bf16[4,4,512]{2,1,0:T(4,128)(2,1)S(1)}, u32[]{:S(2)}, u32[]{:S(2)}) collective-permute-start(bf16[4,4,512]{2,1,0:T(4,128)(2,1)S(1)} %get-tuple-element.42), channel_id=1, source_target_pairs={{0,1},{1,0},{2,3},{3,2},{4,5},{5,4},{6,7},{7,6},{8,9},{9,8},{10,11... | collective-permute-start | bytes 49160 | tf_op jit(solution)/shard_map/ppermute | solution.py:318
  33.5 4.0 %collective-permute-start.13 = (bf16[4,512]{1,0:T(4,128)(2,1)S(1)}, bf16[4,512]{1,0:T(4,128)(2,1)S(1)}, u32[]{:S(2)}, u32[]{:S(2)}) collective-permute-start(bf16[4,512]{1,0:T(4,128)(2,1)S(1)} %get-tuple-element.44), channel_id=1, source_target_pairs={{0,5},{1,4},{2,7},{3,6},{4,1},{5,0},{6,3},{7,2},{8,13},{9,12},{10,... | collective-permute-start | bytes 12296 | tf_op jit(solution)/shard_map/ppermute | solution.py:321
  34.6 4.8 %collective-permute-start.14 = (bf16[4,512]{1,0:T(4,128)(2,1)S(1)}, bf16[4,512]{1,0:T(4,128)(2,1)S(1)}, u32[]{:S(2)}, u32[]{:S(2)}) collective-permute-start(bf16[4,512]{1,0:T(4,128)(2,1)S(1)} %get-tuple-element.45), channel_id=1, source_target_pairs={{0,7},{1,6},{2,5},{3,4},{4,3},{5,2},{6,1},{7,0},{8,15},{9,14},{10,... | collective-permute-start | bytes 12296 | tf_op jit(solution)/shard_map/ppermute | solution.py:321
  36.3 3.1 %collective-permute-start.15 = (bf16[4,512]{1,0:T(4,128)(2,1)S(1)}, bf16[4,512]{1,0:T(4,128)(2,1)S(1)}, u32[]{:S(2)}, u32[]{:S(2)}) collective-permute-start(bf16[4,512]{1,0:T(4,128)(2,1)S(1)} %get-tuple-element.46), channel_id=1, source_target_pairs={{0,3},{1,2},{2,1},{3,0},{4,7},{5,6},{6,5},{7,4},{8,11},{9,10},{10,... | collective-permute-start | bytes 12296 | tf_op jit(solution)/shard_map/ppermute | solution.py:321

commit v6 on v5

--- a/solution.py
+++ b/solution.py
@@ -148,15 +148,22 @@
 
 
 def heads_body(*refs):
-    *blocks, w_heads_out, tokens, mixed, every = refs
+    *blocks, w_own, w_other, tokens, other_tokens, mixed, own_mixed, every = refs
     kv_index = lax.axis_index("kv")
     for j, block in zip([0, *reversed(chip_order(len(blocks)))], blocks):
         every[kv_index ^ j] = block[...].astype(jnp.float32)
     left = jnp.concatenate([every[:, h, :] for h in range(every.shape[1])], axis=1)
-    added = jnp.dot(
-        left.astype(jnp.bfloat16), w_heads_out[...], preferred_element_type=jnp.float32
-    )
-    mixed[...] = (tokens[...].astype(jnp.float32) + added).astype(jnp.bfloat16)
+    left = left.astype(jnp.bfloat16)
+    tp_index = lax.axis_index("tp")
+    for place, weight, start in (
+        (tp_index, w_own, tokens),
+        (1 - tp_index, w_other, other_tokens),
+    ):
+        added = jnp.dot(left, weight[...], preferred_element_type=jnp.float32)
+        rounded = (start[...].astype(jnp.float32) + added).astype(jnp.bfloat16)
+        mixed[place] = rounded
+        if weight is w_own:
+            own_mixed[...] = rounded
 
 
 def mixer_block(j, block, mixer_gain, w_gate, w_up):
@@ -261,7 +268,11 @@
     model_width = norm_gain.shape[0]
     shape = jax.ShapeDtypeStruct
     others = chip_order(kv_count)
-    other = lax.ppermute(tokens, "tp", [(i, (i + 1) % tp_count) for i in range(tp_count)])
+
+    def swapped(block):
+        return lax.ppermute(block, "tp", [(0, 1), (1, 0)])
+
+    other = swapped(tokens)
     weights = (w_query, w_forget, w_input, w_outgate)
     half_shape = (4, own_width, w_query.shape[1])
     own, squares, other_gain, rest = call(
@@ -296,6 +307,8 @@
         scratch=[pltpu.VMEM((row_count, rows + 8, LANES), jnp.float32)],
         cost=LONG,
     )
+    w_early, kept = lax.optimization_barrier((w_heads_out, kept))
+    w_other = swapped(w_early)
     received = [
         lax.ppermute(block, "kv", [(i, i ^ j) for i in range(kv_count)])
         for j, block in zip(others, sent)
@@ -314,9 +327,6 @@
         cost=LONG,
     )
 
-    def swapped(block):
-        return lax.ppermute(block, "tp", [(0, 1), (1, 0)])
-
     def crossed(block, j):
         return lax.ppermute(block, GROUP, [(i, i ^ (2 * j + 1)) for i in range(group_count)])
 
@@ -327,17 +337,19 @@
     pair = call(
         pair_body, shape((2 * heads, HEAD_DIM), jnp.bfloat16), gated, swapped(gated)
     )
-    mixed = call(
+    pair, mixed = call(
         heads_body,
-        shape((row_count, own_width), jnp.bfloat16),
+        (
+            shape((2, row_count, own_width), jnp.bfloat16),
+            shape((row_count, own_width), jnp.bfloat16),
+        ),
         pair,
         *gather(pair),
         resident(w_heads_out),
+        resident(w_other),
         tokens,
+        other,
         scratch=[pltpu.VMEM((kv_count, 2 * heads, HEAD_DIM), jnp.float32)],
-    )
-    pair = call(
-        pair_body, shape((2, row_count, own_width), jnp.bfloat16), mixed, swapped(mixed)
     )
     *blocks, first = gather(pair)
     gain = mixer_gain[None]

time: 40.2 us -> 39.2 us (0.975)
  waiting for transfers between devices: 12.2 us -> 11.3 us
    ppermute x3 -> x4, waiting for transfers between devices: 2.01 us -> 1.2 us  [swapped(): return lax.ppermute(block, 'tp', [(0, 1), (1, 0)])]
    ppermute x1 -> x0, starting transfers between devices: 0.56 us -> none  [local(): lax.ppermute(tokens, 'tp', [(i, (i + 1) % tp_count) for i in range(tp_cou...]
    pallas_call x12 -> x11, Pallas kernels: 11 us -> 11.3 us  [call(): pl.pallas_call(body, out_shape=outs, in_specs=[VMEM] * len(args) + [HBM]...]
    ppermute x3 -> x4, starting transfers between devices: 0.7 us -> 0.88 us  [swapped(): return lax.ppermute(block, 'tp', [(0, 1), (1, 0)])]
  transfers between devices with their start and end apart: 16 -> 16, of which waited for: 9 -> 8; matrix products, arithmetic and copies ran while one was open for 0% -> 0% of each run, Pallas kernels for 15% -> 18%
where the time goes in v6:
time: 39.2 us; the launch traced here: 39 us
  starting transfers between devices  15.5 us (40%)
  Pallas kernels  11.3 us (29%)
  waiting for transfers between devices  11.3 us (29%)
  between operations  0.9 us (2%)
    pallas_call x11, Pallas kernels, call(): pl.pallas_call(body, out_shape=outs, in_specs=[VMEM] * len(args) + [HBM]...  11.3 us
    ppermute x9, starting transfers between devices, crossed(): lax.ppermute(block, GROUP, [(i, i ^ 2 * j + 1) for i in range(group_count)])  9.33 us
    ppermute x9, waiting for transfers between devices, crossed(): lax.ppermute(block, GROUP, [(i, i ^ 2 * j + 1) for i in range(group_count)])  6.24 us
    ppermute x3, starting transfers between devices, local(): lax.ppermute(block, 'kv', [(i, i ^ j) for i in range(kv_count)])  5.25 us
    ppermute x3, waiting for transfers between devices, local(): lax.ppermute(block, 'kv', [(i, i ^ j) for i in range(kv_count)])  3.91 us
    ppermute x4, waiting for transfers between devices, swapped(): return lax.ppermute(block, 'tp', [(0, 1), (1, 0)])  1.2 us
    ppermute x4, starting transfers between devices, swapped(): return lax.ppermute(block, 'tp', [(0, 1), (1, 0)])  0.88 us
  transfers between devices with their start and end apart: 16, of which 8 were waited for; matrix products, arithmetic and copies ran while one was open for 0% of the time, Pallas kernels for 18%

profile of v6, /device:TPU:0, one launch (start us, length us, event | category | flops | bytes accessed | tf_op | source)
XLA Modules:
  0.0 39.0 jit_solution(11925705781144894414)
XLA Ops:
  0.6 0.6 %collective-permute-start = (bf16[4,512]{1,0:T(4,128)(2,1)}, bf16[4,512]{1,0:T(4,128)(2,1)S(1)}, u32[]{:S(2)}, u32[]{:S(2)}) collective-permute-start(bf16[4,512]{1,0:T(4,128)(2,1)} %refs_6_.3), channel_id=1, source_target_pairs={{0,1},{1,0},{2,3},{3,2},{4,5},{5,4},{6,7},{7,6},{8,9},{9,8},{10,11... | collective-permute-start | bytes 12296 | tf_op jit(solution)/shard_map/ppermute | solution.py:273
  1.2 3.6 %shard_map.149 = (f32[4,4,1024]{2,1,0:T(4,128)S(1)}, f32[4,128]{1,0:T(4,128)S(1)}, f32[1,512]{1,0:T(1,128)S(1)}, bf16[4,512,1024]{2,1,0:T(8,128)(2,1)S(1)}) custom-call(bf16[4,512]{1,0:T(4,128)(2,1)} %refs_6_.3, f32[1,4096]{1,0:T(1,128)} %bitcast.18, bf16[1024,1024]{1,0:T(8,128)(2,1)} %w_query.1, bf16[1024,1024]{1,0:T(8,128)(2,1)} %w_forget.1, ...), custom_call_target="tpu_custom_call" | custom-call | flops 10000000 | bytes 10000 | tf_op jit(solution)/shard_map/pallas_call | solution.py:29
  4.8 0.7 %shard_map.150 = (f32[40,128]{1,0:T(8,128)S(1)}, bf16[48,128]{1,0:T(8,128)(2,1)S(1)}, bf16[48,128]{1,0:T(8,128)(2,1)S(1)}, bf16[48,128]{1,0:T(8,128)(2,1)S(1)}) custom-call(bf16[4,512]{1,0:T(4,128)(2,1)S(1)} %collective-permute-done.other.refs_7_, f32[4,4,1024]{2,1,0:T(4,128)S(1)} %get-tuple-element.29.own, f32[4,128]{1,0:T(4,128)S(1)} %get-tuple-element.30.own_squares, ...), custom_call_target="tpu_custom_call" | custom-call | flops 99999997952 | bytes 10000 | tf_op jit(solution)/shard_map/pallas_call | solution.py:29
  5.5 3.7 %collective-permute-start.1 = (bf16[48,128]{1,0:T(8,128)(2,1)S(1)}, bf16[48,128]{1,0:T(8,128)(2,1)S(1)}, u32[]{:S(2)}, u32[]{:S(2)}) collective-permute-start(bf16[48,128]{1,0:T(8,128)(2,1)S(1)} %get-tuple-element.35), channel_id=1, source_target_pairs={{0,4},{2,6},{4,0},{6,2},{1,5},{3,7},{5,1},{7,3},{8,12},{10,14},{12... | collective-permute-start | bytes 36872 | tf_op jit(solution)/shard_map/ppermute | solution.py:313
  9.2 1.3 %collective-permute-start.2 = (bf16[48,128]{1,0:T(8,128)(2,1)S(1)}, bf16[48,128]{1,0:T(8,128)(2,1)S(1)}, u32[]{:S(2)}, u32[]{:S(2)}) collective-permute-start(bf16[48,128]{1,0:T(8,128)(2,1)S(1)} %get-tuple-element.36), channel_id=1, source_target_pairs={{0,6},{2,4},{4,2},{6,0},{1,7},{3,5},{5,3},{7,1},{8,14},{10,12},{12... | collective-permute-start | bytes 36872 | tf_op jit(solution)/shard_map/ppermute | solution.py:313
  10.5 0.2 collective-permute-start.3
  10.8 0.1 collective-permute-done.1.refs_1_
  10.9 3.8 %collective-permute-done.2.refs_2_ = bf16[48,128]{1,0:T(8,128)(2,1)S(1)} collective-permute-done((bf16[48,128]{1,0:T(8,128)(2,1)S(1)}, bf16[48,128]{1,0:T(8,128)(2,1)S(1)}, u32[]{:S(2)}, u32[]{:S(2)}) %collective-permute-start.2) | collective-permute-done | bytes 12320 | tf_op jit(solution)/shard_map/ppermute | solution.py:313
  14.8 0.8 %shard_map.151 = (f32[8,128,128]{2,1,0:T(8,128)S(1)}, f32[8,128]{1,0:T(8,128)S(1)}) custom-call(f32[40,128]{1,0:T(8,128)S(1)} %get-tuple-element.34.refs_0_, bf16[48,128]{1,0:T(8,128)(2,1)S(1)} %collective-permute-done.1.refs_1_, bf16[48,128]{1,0:T(8,128)(2,1)S(1)} %collective-permute-done.2.refs_2_, bf16[48,128]{1,0:T(8,128)(2,1)S(1)} %collective-permute-done.3.refs_3_, ...), custom_call_target="tpu_custom_call" | custom-call | flops 99999997952 | bytes 10000 | tf_op jit(solution)/shard_map/pallas_call | solution.py:29
  15.6 1.2 %collective-permute-done.4.other = f32[8,128]{1,0:T(8,128)S(1)} collective-permute-done((f32[8,128]{1,0:T(8,128)S(1)}, f32[8,128]{1,0:T(8,128)S(1)}, u32[]{:S(2)}, u32[]{:S(2)}) %collective-permute-start.4) | collective-permute-done | bytes 4128 | tf_op jit(solution)/shard_map/ppermute | solution.py:273
  16.7 1.0 %collective-permute-start.7 = (bf16[16,128]{1,0:T(8,128)(2,1)S(1)}, bf16[16,128]{1,0:T(8,128)(2,1)S(1)}, u32[]{:S(2)}, u32[]{:S(2)}) collective-permute-start(bf16[16,128]{1,0:T(8,128)(2,1)S(1)} %shard_map.152.refs_0_), channel_id=1, source_target_pairs={{0,5},{1,4},{2,7},{3,6},{4,1},{5,0},{6,3},{7,2},{8,13},{9,12},{10,... | collective-permute-start | bytes 12296 | tf_op jit(solution)/shard_map/ppermute | solution.py:331
  17.7 1.1 %collective-permute-start.6 = (bf16[16,128]{1,0:T(8,128)(2,1)S(1)}, bf16[16,128]{1,0:T(8,128)(2,1)S(1)}, u32[]{:S(2)}, u32[]{:S(2)}) collective-permute-start(bf16[16,128]{1,0:T(8,128)(2,1)S(1)} %shard_map.152.refs_0_), channel_id=1, source_target_pairs={{0,7},{1,6},{2,5},{3,4},{4,3},{5,2},{6,1},{7,0},{8,15},{9,14},{10,... | collective-permute-start | bytes 12296 | tf_op jit(solution)/shard_map/ppermute | solution.py:331
  18.8 0.9 %collective-permute-start.5 = (bf16[16,128]{1,0:T(8,128)(2,1)S(1)}, bf16[16,128]{1,0:T(8,128)(2,1)S(1)}, u32[]{:S(2)}, u32[]{:S(2)}) collective-permute-start(bf16[16,128]{1,0:T(8,128)(2,1)S(1)} %shard_map.152.refs_0_), channel_id=1, source_target_pairs={{0,3},{1,2},{2,1},{3,0},{4,7},{5,6},{6,5},{7,4},{8,11},{9,10},{10,... | collective-permute-start | bytes 12296 | tf_op jit(solution)/shard_map/ppermute | solution.py:331
  19.7 0.9 %collective-permute-done.7.refs_3_ = bf16[16,128]{1,0:T(8,128)(2,1)S(1)} collective-permute-done((bf16[16,128]{1,0:T(8,128)(2,1)S(1)}, bf16[16,128]{1,0:T(8,128)(2,1)S(1)}, u32[]{:S(2)}, u32[]{:S(2)}) %collective-permute-start.7) | collective-permute-done | bytes 4128 | tf_op jit(solution)/shard_map/ppermute | solution.py:331
  20.7 1.9 %collective-permute-done.6.refs_2_ = bf16[16,128]{1,0:T(8,128)(2,1)S(1)} collective-permute-done((bf16[16,128]{1,0:T(8,128)(2,1)S(1)}, bf16[16,128]{1,0:T(8,128)(2,1)S(1)}, u32[]{:S(2)}, u32[]{:S(2)}) %collective-permute-start.6) | collective-permute-done | bytes 4128 | tf_op jit(solution)/shard_map/ppermute | solution.py:331
  22.6 0.7 %shard_map.153 = (bf16[2,4,512]{2,1,0:T(4,128)(2,1)S(1)}, bf16[4,512]{1,0:T(4,128)(2,1)S(1)}) custom-call(bf16[16,128]{1,0:T(8,128)(2,1)S(1)} %shard_map.152.refs_0_, bf16[16,128]{1,0:T(8,128)(2,1)S(1)} %collective-permute-done.5.refs_1_, bf16[16,128]{1,0:T(8,128)(2,1)S(1)} %collective-permute-done.6.refs_2_, ...), custom_call_target="tpu_custom_call" | custom-call | flops 10000000 | bytes 10000 | tf_op jit(solution)/shard_map/pallas_call | solution.py:29
  23.2 0.7 %collective-permute-start.9 = (bf16[2,4,512]{2,1,0:T(4,128)(2,1)S(1)}, bf16[2,4,512]{2,1,0:T(4,128)(2,1)S(1)}, u32[]{:S(2)}, u32[]{:S(2)}) collective-permute-start(bf16[2,4,512]{2,1,0:T(4,128)(2,1)S(1)} %get-tuple-element.40.block), channel_id=1, source_target_pairs={{0,5},{1,4},{2,7},{3,6},{4,1},{5,0},{6,3},{7,2},{8,13},{9,12},{10,... | collective-permute-start | bytes 24584 | tf_op jit(solution)/shard_map/ppermute | solution.py:331
  24.0 1.8 %collective-permute-start.11 = (bf16[2,4,512]{2,1,0:T(4,128)(2,1)S(1)}, bf16[2,4,512]{2,1,0:T(4,128)(2,1)S(1)}, u32[]{:S(2)}, u32[]{:S(2)}) collective-permute-start(bf16[2,4,512]{2,1,0:T(4,128)(2,1)S(1)} %get-tuple-element.40.block), channel_id=1, source_target_pairs={{0,7},{1,6},{2,5},{3,4},{4,3},{5,2},{6,1},{7,0},{8,15},{9,14},{10,... | collective-permute-start | bytes 24584 | tf_op jit(solution)/shard_map/ppermute | solution.py:331
  25.7 0.7 %collective-permute-start.10 = (bf16[2,4,512]{2,1,0:T(4,128)(2,1)S(1)}, bf16[2,4,512]{2,1,0:T(4,128)(2,1)S(1)}, u32[]{:S(2)}, u32[]{:S(2)}) collective-permute-start(bf16[2,4,512]{2,1,0:T(4,128)(2,1)S(1)} %get-tuple-element.40.block), channel_id=1, source_target_pairs={{0,3},{1,2},{2,1},{3,0},{4,7},{5,6},{6,5},{7,4},{8,11},{9,10},{10,... | collective-permute-start | bytes 24584 | tf_op jit(solution)/shard_map/ppermute | solution.py:331
  26.5 0.9 %shard_map.154 = (f32[4,1408]{1,0:T(4,128)S(1)}, f32[4,1408]{1,0:T(4,128)S(1)}, f32[4,128]{1,0:T(4,128)S(1)}, f32[8,128,128]{2,1,0:T(8,128)}) custom-call(bf16[2,4,512]{2,1,0:T(4,128)(2,1)S(1)} %get-tuple-element.40.block, f32[1,4096]{1,0:T(1,128)S(1)} %bitcast.12, bf16[4096,1408]{1,0:T(8,128)(2,1)S(1)} %bitcast.9, bf16[4096,1408]{1,0:T(8,128)(2,1)S(1)} %bitcast.11, ...), custom_call_target="tpu_custom_call" | custom-call | flops 10000000 | bytes 10000 | tf_op jit(solution)/shard_map/pallas_call | solution.py:29
  27.4 0.9 %shard_map.155 = (f32[4,1408]{1,0:T(4,128)S(1)}, f32[4,1408]{1,0:T(4,128)S(1)}, f32[4,128]{1,0:T(4,128)S(1)}) custom-call(f32[4,1408]{1,0:T(4,128)S(1)} %get-tuple-element.42.refs_0_, f32[4,1408]{1,0:T(4,128)S(1)} %get-tuple-element.43.refs_1_, f32[4,128]{1,0:T(4,128)S(1)} %get-tuple-element.44.refs_2_, ...), custom_call_target="tpu_custom_call" | custom-call | flops 10000000 | bytes 10000 | tf_op jit(solution)/shard_map/pallas_call | solution.py:29
  28.3 0.6 %collective-permute-done.11.refs_4_ = bf16[2,4,512]{2,1,0:T(4,128)(2,1)S(1)} collective-permute-done((bf16[2,4,512]{2,1,0:T(4,128)(2,1)S(1)}, bf16[2,4,512]{2,1,0:T(4,128)(2,1)S(1)}, u32[]{:S(2)}, u32[]{:S(2)}) %collective-permute-start.11) | collective-permute-done | bytes 8224 | tf_op jit(solution)/shard_map/ppermute | solution.py:331
  28.9 2.4 %shard_map.156 = (bf16[4,1408]{1,0:T(4,128)(2,1)S(1)}, bf16[4,4,512]{2,1,0:T(4,128)(2,1)S(1)}) custom-call(f32[4,1408]{1,0:T(4,128)S(1)} %get-tuple-element.45.refs_0_, f32[4,1408]{1,0:T(4,128)S(1)} %get-tuple-element.46.refs_1_, f32[4,128]{1,0:T(4,128)S(1)} %get-tuple-element.47.refs_2_, bf16[2,4,512]{2,1,0:T(4,128)(2,1)S(1)} %collective-permute-done.10.refs_3_, ...), custom_call_target="tpu_custom_call" | custom-call | flops 10000000 | bytes 10000 | tf_op jit(solution)/shard_map/pallas_call | solution.py:29
  31.3 0.3 collective-permute-start.12
  31.6 0.9 %shard_map.157.sums = f32[4,4,512]{2,1,0:T(4,128)S(1)} custom-call(bf16[4,1408]{1,0:T(4,128)(2,1)S(1)} %get-tuple-element.48.hidden, bf16[1408,4096]{1,0:T(8,128)(2,1)S(1)} %bitcast.7), custom_call_target="tpu_custom_call" | custom-call | flops 10000000 | bytes 10000 | tf_op jit(solution)/shard_map/pallas_call | solution.py:29
  32.4 0.0 collective-permute-done.12.passed
  32.5 1.1 %collective-permute-start.13 = (bf16[4,512]{1,0:T(4,128)(2,1)S(1)}, bf16[4,512]{1,0:T(4,128)(2,1)S(1)}, u32[]{:S(2)}, u32[]{:S(2)}) collective-permute-start(bf16[4,512]{1,0:T(4,128)(2,1)S(1)} %get-tuple-element.52), channel_id=1, source_target_pairs={{0,5},{1,4},{2,7},{3,6},{4,1},{5,0},{6,3},{7,2},{8,13},{9,12},{10,... | collective-permute-start | bytes 12296 | tf_op jit(solution)/shard_map/ppermute | solution.py:331
  33.6 1.7 %collective-permute-start.14 = (bf16[4,512]{1,0:T(4,128)(2,1)S(1)}, bf16[4,512]{1,0:T(4,128)(2,1)S(1)}, u32[]{:S(2)}, u32[]{:S(2)}) collective-permute-start(bf16[4,512]{1,0:T(4,128)(2,1)S(1)} %get-tuple-element.53), channel_id=1, source_target_pairs={{0,7},{1,6},{2,5},{3,4},{4,3},{5,2},{6,1},{7,0},{8,15},{9,14},{10,... | collective-permute-start | bytes 12296 | tf_op jit(solution)/shard_map/ppermute | solution.py:331
  35.3 0.4 collective-permute-start.15
  35.7 0.8 %collective-permute-done.13.refs_0_ = bf16[4,512]{1,0:T(4,128)(2,1)S(1)} collective-permute-done((bf16[4,512]{1,0:T(4,128)(2,1)S(1)}, bf16[4,512]{1,0:T(4,128)(2,1)S(1)}, u32[]{:S(2)}, u32[]{:S(2)}) %collective-permute-start.13) | collective-permute-done | bytes 4128 | tf_op jit(solution)/shard_map/ppermute | solution.py:331
  36.5 1.9 %collective-permute-done.14.refs_1_ = bf16[4,512]{1,0:T(4,128)(2,1)S(1)} collective-permute-done((bf16[4,512]{1,0:T(4,128)(2,1)S(1)}, bf16[4,512]{1,0:T(4,128)(2,1)S(1)}, u32[]{:S(2)}, u32[]{:S(2)}) %collective-permute-start.14) | collective-permute-done | bytes 4128 | tf_op jit(solution)/shard_map/ppermute | solution.py:331
  38.4 0.6 %shard_map.159 = bf16[4,512]{1,0:T(4,128)(2,1)} custom-call(f32[4,512]{1,0:T(4,128)S(1)} %get-tuple-element.51.base, bf16[4,512]{1,0:T(4,128)(2,1)S(1)} %collective-permute-done.13.refs_0_, bf16[4,512]{1,0:T(4,128)(2,1)S(1)} %collective-permute-done.14.refs_1_, bf16[4,512]{1,0:T(4,128)(2,1)S(1)} %collective-permute-done.15.refs_2_), custom_call_target="tpu_custom_call" | custom-call | flops 10000000 | bytes 10000 | tf_op jit(solution)/shard_map/pallas_call | solution.py:29
  (44 shorter events, 0.1 us)
Async XLA Ops:
  0.6 4.1 %collective-permute-start = (bf16[4,512]{1,0:T(4,128)(2,1)}, bf16[4,512]{1,0:T(4,128)(2,1)S(1)}, u32[]{:S(2)}, u32[]{:S(2)}) collective-permute-start(bf16[4,512]{1,0:T(4,128)(2,1)} %refs_6_.3), channel_id=1, source_target_pairs={{0,1},{1,0},{2,3},{3,2},{4,5},{5,4},{6,7},{7,6},{8,9},{9,8},{10,11... | collective-permute-start | bytes 12296 | tf_op jit(solution)/shard_map/ppermute | solution.py:273
  4.8 6.0 %copy-start = (bf16[2048,512]{1,0:T(8,128)(2,1)S(1)}, bf16[2048,512]{1,0:T(8,128)(2,1)}, u32[]{:S(2)}) copy-start(bf16[2048,512]{1,0:T(8,128)(2,1)} %refs_4_.1) | copy-start | bytes 6291460
  4.8 9.9 %copy-start.3 = (f32[1,8,128,128]{3,2,1,0:T(8,128)S(1)}, f32[1,8,128,128]{3,2,1,0:T(8,128)}, u32[]{:S(2)}) copy-start(f32[1,8,128,128]{3,2,1,0:T(8,128)} %param.15) | copy-start | bytes 1572868
  4.8 9.9 %copy-start.4 = (f32[1024]{0:T(1024)S(1)}, f32[1024]{0:T(1024)}, u32[]{:S(2)}) copy-start(f32[1024]{0:T(1024)} %param.21) | copy-start | bytes 12292
  4.8 9.9 %copy-start.5 = (f32[1024]{0:T(1024)S(1)}, f32[1024]{0:T(1024)}, u32[]{:S(2)}) copy-start(f32[1024]{0:T(1024)} %param.22) | copy-start | bytes 12292
  5.5 5.3 %collective-permute-start.1 = (bf16[48,128]{1,0:T(8,128)(2,1)S(1)}, bf16[48,128]{1,0:T(8,128)(2,1)S(1)}, u32[]{:S(2)}, u32[]{:S(2)}) collective-permute-start(bf16[48,128]{1,0:T(8,128)(2,1)S(1)} %get-tuple-element.35), channel_id=1, source_target_pairs={{0,4},{2,6},{4,0},{6,2},{1,5},{3,7},{5,1},{7,3},{8,12},{10,14},{12... | collective-permute-start | bytes 36872 | tf_op jit(solution)/shard_map/ppermute | solution.py:313
  9.2 5.5 %collective-permute-start.2 = (bf16[48,128]{1,0:T(8,128)(2,1)S(1)}, bf16[48,128]{1,0:T(8,128)(2,1)S(1)}, u32[]{:S(2)}, u32[]{:S(2)}) collective-permute-start(bf16[48,128]{1,0:T(8,128)(2,1)S(1)} %get-tuple-element.36), channel_id=1, source_target_pairs={{0,6},{2,4},{4,2},{6,0},{1,7},{3,5},{5,3},{7,1},{8,14},{10,12},{12... | collective-permute-start | bytes 36872 | tf_op jit(solution)/shard_map/ppermute | solution.py:313
  10.5 4.1 %collective-permute-start.3 = (bf16[48,128]{1,0:T(8,128)(2,1)S(1)}, bf16[48,128]{1,0:T(8,128)(2,1)S(1)}, u32[]{:S(2)}, u32[]{:S(2)}) collective-permute-start(bf16[48,128]{1,0:T(8,128)(2,1)S(1)} %get-tuple-element.37), channel_id=1, source_target_pairs={{0,2},{2,0},{4,6},{6,4},{1,3},{3,1},{5,7},{7,5},{8,10},{10,8},{12,... | collective-permute-start | bytes 36872 | tf_op jit(solution)/shard_map/ppermute | solution.py:313
  10.8 11.8 %collective-permute-start.8 = (bf16[2048,512]{1,0:T(8,128)(2,1)S(1)}, bf16[2048,512]{1,0:T(8,128)(2,1)S(1)}, u32[]{:S(2)}, u32[]{:S(2)}) collective-permute-start(bf16[2048,512]{1,0:T(8,128)(2,1)S(1)} %copy-done), channel_id=1, source_target_pairs={{0,1},{1,0},{2,3},{3,2},{4,5},{5,4},{6,7},{7,6},{8,9},{9,8},{10,11... | collective-permute-start | bytes 6291464 | tf_op jit(solution)/shard_map/ppermute | solution.py:273
  14.7 11.7 %slice-start = ((s8[11534336]{0:T(1024)(128)(4,1)}), s8[4194304]{0:T(1024)(128)(4,1)S(1)}, s32[]{:S(2)}) async-start(s8[11534336]{0:T(1024)(128)(4,1)} %bitcast.6), calls=%async_computation | async-start | bytes 8388608
  14.7 11.7 %slice-start.3 = ((s8[11534336]{0:T(1024)(128)(4,1)}), s8[4194304]{0:T(1024)(128)(4,1)S(1)}, s32[]{:S(2)}) async-start(s8[11534336]{0:T(1024)(128)(4,1)} %bitcast.8), calls=%async_computation.3 | async-start | bytes 8388608
  14.7 11.7 %slice-start.6 = ((s8[11534336]{0:T(1024)(128)(4,1)}), s8[4194304]{0:T(1024)(128)(4,1)S(1)}, s32[]{:S(2)}) async-start(s8[11534336]{0:T(1024)(128)(4,1)} %bitcast.10), calls=%async_computation.6 | async-start | bytes 8388608
  14.7 7.9 %copy-start.2 = (bf16[4,512]{1,0:T(4,128)(2,1)S(1)}, bf16[4,512]{1,0:T(4,128)(2,1)}, u32[]{:S(2)}) copy-start(bf16[4,512]{1,0:T(4,128)(2,1)} %refs_6_.3) | copy-start | bytes 12292
  14.7 11.7 %slice-start.1 = ((s8[11534336]{0:T(1024)(128)(4,1)}), s8[4194304]{0:T(1024)(128)(4,1)S(1)}, s32[]{:S(2)}) async-start(s8[11534336]{0:T(1024)(128)(4,1)} %bitcast.6), calls=%async_computation.1 | async-start | bytes 8388608
  14.7 11.7 %slice-start.2 = ((s8[11534336]{0:T(1024)(128)(4,1)}), s8[3145728]{0:T(1024)(128)(4,1)S(1)}, s32[]{:S(2)}) async-start(s8[11534336]{0:T(1024)(128)(4,1)} %bitcast.6), calls=%async_computation.2 | async-start | bytes 6291456
  14.8 11.7 %slice-start.4 = ((s8[11534336]{0:T(1024)(128)(4,1)}), s8[4194304]{0:T(1024)(128)(4,1)S(1)}, s32[]{:S(2)}) async-start(s8[11534336]{0:T(1024)(128)(4,1)} %bitcast.8), calls=%async_computation.4 | async-start | bytes 8388608
  14.8 11.7 %slice-start.5 = ((s8[11534336]{0:T(1024)(128)(4,1)}), s8[3145728]{0:T(1024)(128)(4,1)S(1)}, s32[]{:S(2)}) async-start(s8[11534336]{0:T(1024)(128)(4,1)} %bitcast.8), calls=%async_computation.5 | async-start | bytes 6291456
  14.8 11.7 %slice-start.7 = ((s8[11534336]{0:T(1024)(128)(4,1)}), s8[4194304]{0:T(1024)(128)(4,1)S(1)}, s32[]{:S(2)}) async-start(s8[11534336]{0:T(1024)(128)(4,1)} %bitcast.10), calls=%async_computation.7 | async-start | bytes 8388608
  14.8 11.7 %slice-start.8 = ((s8[11534336]{0:T(1024)(128)(4,1)}), s8[3145728]{0:T(1024)(128)(4,1)S(1)}, s32[]{:S(2)}) async-start(s8[11534336]{0:T(1024)(128)(4,1)} %bitcast.10), calls=%async_computation.8 | async-start | bytes 6291456
  15.5 1.2 %collective-permute-start.4 = (f32[8,128]{1,0:T(8,128)S(1)}, f32[8,128]{1,0:T(8,128)S(1)}, u32[]{:S(2)}, u32[]{:S(2)}) collective-permute-start(f32[8,128]{1,0:T(8,128)S(1)} %get-tuple-element.38.own), channel_id=1, source_target_pairs={{0,1},{1,0},{2,3},{3,2},{4,5},{5,4},{6,7},{7,6},{8,9},{9,8},{10,11... | collective-permute-start | bytes 12296 | tf_op jit(solution)/shard_map/ppermute | solution.py:273
  16.7 9.7 %copy-start.1 = (f32[4096]{0:T(1024)S(1)}, f32[4096]{0:T(1024)}, u32[]{:S(2)}) copy-start(f32[4096]{0:T(1024)} %param.24) | copy-start | bytes 49156
  16.7 3.9 %collective-permute-start.7 = (bf16[16,128]{1,0:T(8,128)(2,1)S(1)}, bf16[16,128]{1,0:T(8,128)(2,1)S(1)}, u32[]{:S(2)}, u32[]{:S(2)}) collective-permute-start(bf16[16,128]{1,0:T(8,128)(2,1)S(1)} %shard_map.152.refs_0_), channel_id=1, source_target_pairs={{0,5},{1,4},{2,7},{3,6},{4,1},{5,0},{6,3},{7,2},{8,13},{9,12},{10,... | collective-permute-start | bytes 12296 | tf_op jit(solution)/shard_map/ppermute | solution.py:331
  17.7 4.8 %collective-permute-start.6 = (bf16[16,128]{1,0:T(8,128)(2,1)S(1)}, bf16[16,128]{1,0:T(8,128)(2,1)S(1)}, u32[]{:S(2)}, u32[]{:S(2)}) collective-permute-start(bf16[16,128]{1,0:T(8,128)(2,1)S(1)} %shard_map.152.refs_0_), channel_id=1, source_target_pairs={{0,7},{1,6},{2,5},{3,4},{4,3},{5,2},{6,1},{7,0},{8,15},{9,14},{10,... | collective-permute-start | bytes 12296 | tf_op jit(solution)/shard_map/ppermute | solution.py:331
  18.8 3.8 %collective-permute-start.5 = (bf16[16,128]{1,0:T(8,128)(2,1)S(1)}, bf16[16,128]{1,0:T(8,128)(2,1)S(1)}, u32[]{:S(2)}, u32[]{:S(2)}) collective-permute-start(bf16[16,128]{1,0:T(8,128)(2,1)S(1)} %shard_map.152.refs_0_), channel_id=1, source_target_pairs={{0,3},{1,2},{2,1},{3,0},{4,7},{5,6},{6,5},{7,4},{8,11},{9,10},{10,... | collective-permute-start | bytes 12296 | tf_op jit(solution)/shard_map/ppermute | solution.py:331
  23.2 4.2 %collective-permute-start.9 = (bf16[2,4,512]{2,1,0:T(4,128)(2,1)S(1)}, bf16[2,4,512]{2,1,0:T(4,128)(2,1)S(1)}, u32[]{:S(2)}, u32[]{:S(2)}) collective-permute-start(bf16[2,4,512]{2,1,0:T(4,128)(2,1)S(1)} %get-tuple-element.40.block), channel_id=1, source_target_pairs={{0,5},{1,4},{2,7},{3,6},{4,1},{5,0},{6,3},{7,2},{8,13},{9,12},{10,... | collective-permute-start | bytes 24584 | tf_op jit(solution)/shard_map/ppermute | solution.py:331
  24.0 4.9 %collective-permute-start.11 = (bf16[2,4,512]{2,1,0:T(4,128)(2,1)S(1)}, bf16[2,4,512]{2,1,0:T(4,128)(2,1)S(1)}, u32[]{:S(2)}, u32[]{:S(2)}) collective-permute-start(bf16[2,4,512]{2,1,0:T(4,128)(2,1)S(1)} %get-tuple-element.40.block), channel_id=1, source_target_pairs={{0,7},{1,6},{2,5},{3,4},{4,3},{5,2},{6,1},{7,0},{8,15},{9,14},{10,... | collective-permute-start | bytes 24584 | tf_op jit(solution)/shard_map/ppermute | solution.py:331
  25.7 3.2 %collective-permute-start.10 = (bf16[2,4,512]{2,1,0:T(4,128)(2,1)S(1)}, bf16[2,4,512]{2,1,0:T(4,128)(2,1)S(1)}, u32[]{:S(2)}, u32[]{:S(2)}) collective-permute-start(bf16[2,4,512]{2,1,0:T(4,128)(2,1)S(1)} %get-tuple-element.40.block), channel_id=1, source_target_pairs={{0,3},{1,2},{2,1},{3,0},{4,7},{5,6},{6,5},{7,4},{8,11},{9,10},{10,... | collective-permute-start | bytes 24584 | tf_op jit(solution)/shard_map/ppermute | solution.py:331
  31.3 1.2 %collective-permute-start.12 = (bf16[4,4,512]{2,1,0:T(4,128)(2,1)S(1)}, bf16[4,4,512]{2,1,0:T(4,128)(2,1)S(1)}, u32[]{:S(2)}, u32[]{:S(2)}) collective-permute-start(bf16[4,4,512]{2,1,0:T(4,128)(2,1)S(1)} %get-tuple-element.49), channel_id=1, source_target_pairs={{0,1},{1,0},{2,3},{3,2},{4,5},{5,4},{6,7},{7,6},{8,9},{9,8},{10,11... | collective-permute-start | bytes 49160 | tf_op jit(solution)/shard_map/ppermute | solution.py:273
  32.5 4.0 %collective-permute-start.13 = (bf16[4,512]{1,0:T(4,128)(2,1)S(1)}, bf16[4,512]{1,0:T(4,128)(2,1)S(1)}, u32[]{:S(2)}, u32[]{:S(2)}) collective-permute-start(bf16[4,512]{1,0:T(4,128)(2,1)S(1)} %get-tuple-element.52), channel_id=1, source_target_pairs={{0,5},{1,4},{2,7},{3,6},{4,1},{5,0},{6,3},{7,2},{8,13},{9,12},{10,... | collective-permute-start | bytes 12296 | tf_op jit(solution)/shard_map/ppermute | solution.py:331
  33.6 4.8 %collective-permute-start.14 = (bf16[4,512]{1,0:T(4,128)(2,1)S(1)}, bf16[4,512]{1,0:T(4,128)(2,1)S(1)}, u32[]{:S(2)}, u32[]{:S(2)}) collective-permute-start(bf16[4,512]{1,0:T(4,128)(2,1)S(1)} %get-tuple-element.53), channel_id=1, source_target_pairs={{0,7},{1,6},{2,5},{3,4},{4,3},{5,2},{6,1},{7,0},{8,15},{9,14},{10,... | collective-permute-start | bytes 12296 | tf_op jit(solution)/shard_map/ppermute | solution.py:331
  35.3 3.1 %collective-permute-start.15 = (bf16[4,512]{1,0:T(4,128)(2,1)S(1)}, bf16[4,512]{1,0:T(4,128)(2,1)S(1)}, u32[]{:S(2)}, u32[]{:S(2)}) collective-permute-start(bf16[4,512]{1,0:T(4,128)(2,1)S(1)} %get-tuple-element.54), channel_id=1, source_target_pairs={{0,3},{1,2},{2,1},{3,0},{4,7},{5,6},{6,5},{7,4},{8,11},{9,10},{10,... | collective-permute-start | bytes 12296 | tf_op jit(solution)/shard_map/ppermute | solution.py:331

commit v7 on v6

--- a/solution.py
+++ b/solution.py
@@ -102,7 +102,7 @@
 
 def recur_body(model_width, arrived, *refs):
     kept, *received = refs[: arrived + 1]
-    rec_state, lower_bound, head_gain, new_state, gated = refs[arrived + 1 :]
+    rec_state, lower_bound, head_gain, gates, gated = refs[arrived + 1 :]
     heads = rec_state.shape[0]
     row = 4 * heads
     total = kept[:row]
@@ -120,23 +120,30 @@
     forget = bound + (1.0 - bound) / (1.0 + jnp.exp(-forget_pre))
     key_in = 1.0 - forget
     query_act = silu(query_pre)
-    forget_t = forget.T
-    key_t = key_in.T
-    query_t = query_act.T
-    rows = []
-    for h in range(heads):
-        fresh = (
+    gates[0], gates[1], gates[2] = forget, key_in, value_in
+    read_t = (query_act * forget).T
+    rows = [
+        jnp.sum(read_t[:, h : h + 1] * rec_state[h], axis=0, keepdims=True)
+        for h in range(heads)
+    ]
+    fresh = jnp.sum(query_act * key_in, axis=1, keepdims=True) * value_in
+    head_out = jnp.concatenate(rows, axis=0) + fresh
+    head_out = head_out * lax.rsqrt(
+        jnp.mean(head_out * head_out, axis=1, keepdims=True) + epsilon
+    )
+    rounded = (head_out * head_gain[...] * silu(gate_pre)).astype(jnp.bfloat16)
+    gated[...] = rounded.astype(jnp.float32)
+
+
+def state_body(gates, rec_state, new_state):
+    forget_t = gates[0].T
+    key_t = gates[1].T
+    value_in = gates[2]
+    for h in range(rec_state.shape[0]):
+        new_state[h] = (
             forget_t[:, h : h + 1] * rec_state[h]
             + key_t[:, h : h + 1] * value_in[h : h + 1, :]
         )
-        new_state[h] = fresh
-        rows.append(jnp.sum(query_t[:, h : h + 1] * fresh, axis=0, keepdims=True))
-    head_out = jnp.concatenate(rows, axis=0)
-    head_out = head_out * lax.rsqrt(
-        jnp.mean(head_out * head_out, axis=1, keepdims=True) + epsilon
-    )
-    rounded = (head_out * head_gain[...] * silu(gate_pre)).astype(jnp.bfloat16)
-    gated[...] = rounded.astype(jnp.float32)
 
 
 def pair_body(own, other, out):
@@ -313,15 +320,16 @@
         lax.ppermute(block, "kv", [(i, i ^ j) for i in range(kv_count)])
         for j, block in zip(others, sent)
     ]
-    new_state, gated = call(
+    state = resident(rec_state[0])
+    gates, gated = call(
         lambda *refs: recur_body(model_width, len(received), *refs),
         (
-            pltpu.VMEM(rec_state.shape[1:], jnp.float32),
+            shape((3, heads, HEAD_DIM), jnp.float32),
             shape((heads, HEAD_DIM), jnp.float32),
         ),
         kept,
         *received,
-        resident(rec_state[0]),
+        state,
         lower_bound.reshape(heads, HEAD_DIM),
         head_gain.reshape(heads, HEAD_DIM),
         cost=LONG,
@@ -330,6 +338,10 @@
     def crossed(block, j):
         return lax.ppermute(block, GROUP, [(i, i ^ (2 * j + 1)) for i in range(group_count)])
 
+    new_state = call(
+        state_body, pltpu.VMEM(rec_state.shape[1:], jnp.float32), gates, state
+    )
+
     def gather(block):
         blocks = {j: crossed(block, j) for j in range(1, kv_count)}
         return [blocks[j] for j in reversed(others)]
@@ -337,6 +349,7 @@
     pair = call(
         pair_body, shape((2 * heads, HEAD_DIM), jnp.bfloat16), gated, swapped(gated)
     )
+    *arrived, new_state = lax.optimization_barrier((*gather(pair), new_state))
     pair, mixed = call(
         heads_body,
         (
@@ -344,7 +357,7 @@
             shape((row_count, own_width), jnp.bfloat16),
         ),
         pair,
-        *gather(pair),
+        *arrived,
         resident(w_heads_out),
         resident(w_other),
         tokens,

time: 39.2 us -> 38.9 us (level)
  waiting for transfers between devices: 11.3 us -> 10.9 us
    ppermute x9, waiting for transfers between devices: 6.24 us -> 5.8 us  [crossed(): lax.ppermute(block, GROUP, [(i, i ^ 2 * j + 1) for i in range(group_count)])]
    pallas_call x11 -> x12, Pallas kernels: 11.3 us -> 11.5 us  [call(): pl.pallas_call(body, out_shape=outs, in_specs=[VMEM] * len(args) + [HBM]...]
  transfers between devices with their start and end apart: 16 -> 16, of which waited for: 8 -> 8; matrix products, arithmetic and copies ran while one was open for 0% -> 0% of each run, Pallas kernels for 18% -> 19%
where the time goes in v7:
time: 38.9 us; the launch traced here: 38.7 us
  starting transfers between devices  15.5 us (40%)
  Pallas kernels  11.5 us (30%)
  waiting for transfers between devices  10.9 us (28%)
  between operations  0.79 us (2%)
    pallas_call x12, Pallas kernels, call(): pl.pallas_call(body, out_shape=outs, in_specs=[VMEM] * len(args) + [HBM]...  11.5 us
    ppermute x9, starting transfers between devices, crossed(): lax.ppermute(block, GROUP, [(i, i ^ 2 * j + 1) for i in range(group_count)])  9.36 us
    ppermute x9, waiting for transfers between devices, crossed(): lax.ppermute(block, GROUP, [(i, i ^ 2 * j + 1) for i in range(group_count)])  5.8 us
    ppermute x3, starting transfers between devices, local(): lax.ppermute(block, 'kv', [(i, i ^ j) for i in range(kv_count)])  5.25 us
    ppermute x3, waiting for transfers between devices, local(): lax.ppermute(block, 'kv', [(i, i ^ j) for i in range(kv_count)])  3.91 us
    ppermute x4, waiting for transfers between devices, swapped(): return lax.ppermute(block, 'tp', [(0, 1), (1, 0)])  1.21 us
    ppermute x4, starting transfers between devices, swapped(): return lax.ppermute(block, 'tp', [(0, 1), (1, 0)])  0.87 us
  transfers between devices with their start and end apart: 16, of which 8 were waited for; matrix products, arithmetic and copies ran while one was open for 0% of the time, Pallas kernels for 19%

profile of v7, /device:TPU:0, one launch (start us, length us, event | category | flops | bytes accessed | tf_op | source)
XLA Modules:
  0.0 38.7 jit_solution(18184038939911164683)
XLA Ops:
  0.6 0.6 %collective-permute-start = (bf16[4,512]{1,0:T(4,128)(2,1)}, bf16[4,512]{1,0:T(4,128)(2,1)S(1)}, u32[]{:S(2)}, u32[]{:S(2)}) collective-permute-start(bf16[4,512]{1,0:T(4,128)(2,1)} %refs_6_.3), channel_id=1, source_target_pairs={{0,1},{1,0},{2,3},{3,2},{4,5},{5,4},{6,7},{7,6},{8,9},{9,8},{10,11... | collective-permute-start | bytes 12296 | tf_op jit(solution)/shard_map/ppermute | solution.py:280
  1.2 3.6 %shard_map.149 = (f32[4,4,1024]{2,1,0:T(4,128)S(1)}, f32[4,128]{1,0:T(4,128)S(1)}, f32[1,512]{1,0:T(1,128)S(1)}, bf16[4,512,1024]{2,1,0:T(8,128)(2,1)S(1)}) custom-call(bf16[4,512]{1,0:T(4,128)(2,1)} %refs_6_.3, f32[1,4096]{1,0:T(1,128)} %bitcast.13, bf16[1024,1024]{1,0:T(8,128)(2,1)} %w_query.1, bf16[1024,1024]{1,0:T(8,128)(2,1)} %w_forget.1, ...), custom_call_target="tpu_custom_call" | custom-call | flops 10000000 | bytes 10000 | tf_op jit(solution)/shard_map/pallas_call | solution.py:29
  4.8 0.7 %shard_map.150 = (f32[40,128]{1,0:T(8,128)S(1)}, bf16[48,128]{1,0:T(8,128)(2,1)S(1)}, bf16[48,128]{1,0:T(8,128)(2,1)S(1)}, bf16[48,128]{1,0:T(8,128)(2,1)S(1)}) custom-call(bf16[4,512]{1,0:T(4,128)(2,1)S(1)} %collective-permute-done.other.refs_7_, f32[4,4,1024]{2,1,0:T(4,128)S(1)} %get-tuple-element.33.own, f32[4,128]{1,0:T(4,128)S(1)} %get-tuple-element.34.own_squares, ...), custom_call_target="tpu_custom_call" | custom-call | flops 99999997952 | bytes 10000 | tf_op jit(solution)/shard_map/pallas_call | solution.py:29
  5.5 3.7 %collective-permute-start.1 = (bf16[48,128]{1,0:T(8,128)(2,1)S(1)}, bf16[48,128]{1,0:T(8,128)(2,1)S(1)}, u32[]{:S(2)}, u32[]{:S(2)}) collective-permute-start(bf16[48,128]{1,0:T(8,128)(2,1)S(1)} %get-tuple-element.39), channel_id=1, source_target_pairs={{0,4},{2,6},{4,0},{6,2},{1,5},{3,7},{5,1},{7,3},{8,12},{10,14},{12... | collective-permute-start | bytes 36872 | tf_op jit(solution)/shard_map/ppermute | solution.py:320
  9.2 1.3 %collective-permute-start.2 = (bf16[48,128]{1,0:T(8,128)(2,1)S(1)}, bf16[48,128]{1,0:T(8,128)(2,1)S(1)}, u32[]{:S(2)}, u32[]{:S(2)}) collective-permute-start(bf16[48,128]{1,0:T(8,128)(2,1)S(1)} %get-tuple-element.40), channel_id=1, source_target_pairs={{0,6},{2,4},{4,2},{6,0},{1,7},{3,5},{5,3},{7,1},{8,14},{10,12},{12... | collective-permute-start | bytes 36872 | tf_op jit(solution)/shard_map/ppermute | solution.py:320
  10.5 0.2 collective-permute-start.3
  10.8 0.1 collective-permute-done.1.refs_1_
  10.9 3.8 %collective-permute-done.2.refs_2_ = bf16[48,128]{1,0:T(8,128)(2,1)S(1)} collective-permute-done((bf16[48,128]{1,0:T(8,128)(2,1)S(1)}, bf16[48,128]{1,0:T(8,128)(2,1)S(1)}, u32[]{:S(2)}, u32[]{:S(2)}) %collective-permute-start.2) | collective-permute-done | bytes 12320 | tf_op jit(solution)/shard_map/ppermute | solution.py:320
  14.7 0.5 %shard_map.151 = (f32[3,8,128]{2,1,0:T(8,128)S(1)}, f32[8,128]{1,0:T(8,128)S(1)}) custom-call(f32[40,128]{1,0:T(8,128)S(1)} %get-tuple-element.38.refs_0_, bf16[48,128]{1,0:T(8,128)(2,1)S(1)} %collective-permute-done.1.refs_1_, bf16[48,128]{1,0:T(8,128)(2,1)S(1)} %collective-permute-done.2.refs_2_, bf16[48,128]{1,0:T(8,128)(2,1)S(1)} %collective-permute-done.3.refs_3_, ...), custom_call_target="tpu_custom_call" | custom-call | flops 99999997952 | bytes 10000 | tf_op jit(solution)/shard_map/pallas_call | solution.py:29
  15.2 1.2 %collective-permute-done.4.other = f32[8,128]{1,0:T(8,128)S(1)} collective-permute-done((f32[8,128]{1,0:T(8,128)S(1)}, f32[8,128]{1,0:T(8,128)S(1)}, u32[]{:S(2)}, u32[]{:S(2)}) %collective-permute-start.4) | collective-permute-done | bytes 4128 | tf_op jit(solution)/shard_map/ppermute | solution.py:280
  16.4 1.1 %collective-permute-start.7 = (bf16[16,128]{1,0:T(8,128)(2,1)S(1)}, bf16[16,128]{1,0:T(8,128)(2,1)S(1)}, u32[]{:S(2)}, u32[]{:S(2)}) collective-permute-start(bf16[16,128]{1,0:T(8,128)(2,1)S(1)} %shard_map.152.refs_0_), channel_id=1, source_target_pairs={{0,5},{1,4},{2,7},{3,6},{4,1},{5,0},{6,3},{7,2},{8,13},{9,12},{10,... | collective-permute-start | bytes 12296 | tf_op jit(solution)/shard_map/ppermute | solution.py:339
  17.5 1.3 %collective-permute-start.6 = (bf16[16,128]{1,0:T(8,128)(2,1)S(1)}, bf16[16,128]{1,0:T(8,128)(2,1)S(1)}, u32[]{:S(2)}, u32[]{:S(2)}) collective-permute-start(bf16[16,128]{1,0:T(8,128)(2,1)S(1)} %shard_map.152.refs_0_), channel_id=1, source_target_pairs={{0,7},{1,6},{2,5},{3,4},{4,3},{5,2},{6,1},{7,0},{8,15},{9,14},{10,... | collective-permute-start | bytes 12296 | tf_op jit(solution)/shard_map/ppermute | solution.py:339
  18.8 0.6 %collective-permute-start.5 = (bf16[16,128]{1,0:T(8,128)(2,1)S(1)}, bf16[16,128]{1,0:T(8,128)(2,1)S(1)}, u32[]{:S(2)}, u32[]{:S(2)}) collective-permute-start(bf16[16,128]{1,0:T(8,128)(2,1)S(1)} %shard_map.152.refs_0_), channel_id=1, source_target_pairs={{0,3},{1,2},{2,1},{3,0},{4,7},{5,6},{6,5},{7,4},{8,11},{9,10},{10,... | collective-permute-start | bytes 12296 | tf_op jit(solution)/shard_map/ppermute | solution.py:339
  19.4 0.5 %shard_map.153.new_state = f32[8,128,128]{2,1,0:T(8,128)S(1)} custom-call(f32[3,8,128]{2,1,0:T(8,128)S(1)} %get-tuple-element.43.gates, f32[8,128,128]{2,1,0:T(8,128)S(1)} %bitcast.7), custom_call_target="tpu_custom_call" | custom-call | flops 10000000 | bytes 10000 | tf_op jit(solution)/shard_map/pallas_call | solution.py:29
  19.9 0.4 %collective-permute-done.7.refs_3_ = bf16[16,128]{1,0:T(8,128)(2,1)S(1)} collective-permute-done((bf16[16,128]{1,0:T(8,128)(2,1)S(1)}, bf16[16,128]{1,0:T(8,128)(2,1)S(1)}, u32[]{:S(2)}, u32[]{:S(2)}) %collective-permute-start.7) | collective-permute-done | bytes 4128 | tf_op jit(solution)/shard_map/ppermute | solution.py:339
  20.4 2.0 %collective-permute-done.6.refs_2_ = bf16[16,128]{1,0:T(8,128)(2,1)S(1)} collective-permute-done((bf16[16,128]{1,0:T(8,128)(2,1)S(1)}, bf16[16,128]{1,0:T(8,128)(2,1)S(1)}, u32[]{:S(2)}, u32[]{:S(2)}) %collective-permute-start.6) | collective-permute-done | bytes 4128 | tf_op jit(solution)/shard_map/ppermute | solution.py:339
  22.3 0.7 %shard_map.154 = (bf16[2,4,512]{2,1,0:T(4,128)(2,1)S(1)}, bf16[4,512]{1,0:T(4,128)(2,1)S(1)}) custom-call(bf16[16,128]{1,0:T(8,128)(2,1)S(1)} %shard_map.152.refs_0_, bf16[16,128]{1,0:T(8,128)(2,1)S(1)} %collective-permute-done.5.refs_1_, bf16[16,128]{1,0:T(8,128)(2,1)S(1)} %collective-permute-done.6.refs_2_, ...), custom_call_target="tpu_custom_call" | custom-call | flops 10000000 | bytes 10000 | tf_op jit(solution)/shard_map/pallas_call | solution.py:29
  23.0 0.7 %collective-permute-start.9 = (bf16[2,4,512]{2,1,0:T(4,128)(2,1)S(1)}, bf16[2,4,512]{2,1,0:T(4,128)(2,1)S(1)}, u32[]{:S(2)}, u32[]{:S(2)}) collective-permute-start(bf16[2,4,512]{2,1,0:T(4,128)(2,1)S(1)} %get-tuple-element.48.block), channel_id=1, source_target_pairs={{0,5},{1,4},{2,7},{3,6},{4,1},{5,0},{6,3},{7,2},{8,13},{9,12},{10,... | collective-permute-start | bytes 24584 | tf_op jit(solution)/shard_map/ppermute | solution.py:339
  23.7 1.8 %collective-permute-start.11 = (bf16[2,4,512]{2,1,0:T(4,128)(2,1)S(1)}, bf16[2,4,512]{2,1,0:T(4,128)(2,1)S(1)}, u32[]{:S(2)}, u32[]{:S(2)}) collective-permute-start(bf16[2,4,512]{2,1,0:T(4,128)(2,1)S(1)} %get-tuple-element.48.block), channel_id=1, source_target_pairs={{0,7},{1,6},{2,5},{3,4},{4,3},{5,2},{6,1},{7,0},{8,15},{9,14},{10,... | collective-permute-start | bytes 24584 | tf_op jit(solution)/shard_map/ppermute | solution.py:339
  25.4 0.8 %collective-permute-start.10 = (bf16[2,4,512]{2,1,0:T(4,128)(2,1)S(1)}, bf16[2,4,512]{2,1,0:T(4,128)(2,1)S(1)}, u32[]{:S(2)}, u32[]{:S(2)}) collective-permute-start(bf16[2,4,512]{2,1,0:T(4,128)(2,1)S(1)} %get-tuple-element.48.block), channel_id=1, source_target_pairs={{0,3},{1,2},{2,1},{3,0},{4,7},{5,6},{6,5},{7,4},{8,11},{9,10},{10,... | collective-permute-start | bytes 24584 | tf_op jit(solution)/shard_map/ppermute | solution.py:339
  26.2 0.9 %shard_map.155 = (f32[4,1408]{1,0:T(4,128)S(1)}, f32[4,1408]{1,0:T(4,128)S(1)}, f32[4,128]{1,0:T(4,128)S(1)}, f32[8,128,128]{2,1,0:T(8,128)}) custom-call(bf16[2,4,512]{2,1,0:T(4,128)(2,1)S(1)} %get-tuple-element.48.block, f32[1,4096]{1,0:T(1,128)S(1)} %bitcast.8, bf16[4096,1408]{1,0:T(8,128)(2,1)S(1)} %copy-done.1, bf16[4096,1408]{1,0:T(8,128)(2,1)S(1)} %copy-done.2, ...), custom_call_target="tpu_custom_call" | custom-call | flops 10000000 | bytes 10000 | tf_op jit(solution)/shard_map/pallas_call | solution.py:29
  27.1 0.9 %shard_map.156 = (f32[4,1408]{1,0:T(4,128)S(1)}, f32[4,1408]{1,0:T(4,128)S(1)}, f32[4,128]{1,0:T(4,128)S(1)}) custom-call(f32[4,1408]{1,0:T(4,128)S(1)} %get-tuple-element.50.refs_0_, f32[4,1408]{1,0:T(4,128)S(1)} %get-tuple-element.51.refs_1_, f32[4,128]{1,0:T(4,128)S(1)} %get-tuple-element.52.refs_2_, ...), custom_call_target="tpu_custom_call" | custom-call | flops 10000000 | bytes 10000 | tf_op jit(solution)/shard_map/pallas_call | solution.py:29
  28.0 0.6 %collective-permute-done.11.refs_4_ = bf16[2,4,512]{2,1,0:T(4,128)(2,1)S(1)} collective-permute-done((bf16[2,4,512]{2,1,0:T(4,128)(2,1)S(1)}, bf16[2,4,512]{2,1,0:T(4,128)(2,1)S(1)}, u32[]{:S(2)}, u32[]{:S(2)}) %collective-permute-start.11) | collective-permute-done | bytes 8224 | tf_op jit(solution)/shard_map/ppermute | solution.py:339
  28.6 2.4 %shard_map.157 = (bf16[4,1408]{1,0:T(4,128)(2,1)S(1)}, bf16[4,4,512]{2,1,0:T(4,128)(2,1)S(1)}) custom-call(f32[4,1408]{1,0:T(4,128)S(1)} %get-tuple-element.53.refs_0_, f32[4,1408]{1,0:T(4,128)S(1)} %get-tuple-element.54.refs_1_, f32[4,128]{1,0:T(4,128)S(1)} %get-tuple-element.55.refs_2_, bf16[2,4,512]{2,1,0:T(4,128)(2,1)S(1)} %collective-permute-done.10.refs_3_, ...), custom_call_target="tpu_custom_call" | custom-call | flops 10000000 | bytes 10000 | tf_op jit(solution)/shard_map/pallas_call | solution.py:29
  31.0 0.3 collective-permute-start.12
  31.3 0.9 %shard_map.158.sums = f32[4,4,512]{2,1,0:T(4,128)S(1)} custom-call(bf16[4,1408]{1,0:T(4,128)(2,1)S(1)} %get-tuple-element.56.hidden, bf16[1408,4096]{1,0:T(8,128)(2,1)S(1)} %copy-done), custom_call_target="tpu_custom_call" | custom-call | flops 10000000 | bytes 10000 | tf_op jit(solution)/shard_map/pallas_call | solution.py:29
  32.2 1.1 %collective-permute-start.13 = (bf16[4,512]{1,0:T(4,128)(2,1)S(1)}, bf16[4,512]{1,0:T(4,128)(2,1)S(1)}, u32[]{:S(2)}, u32[]{:S(2)}) collective-permute-start(bf16[4,512]{1,0:T(4,128)(2,1)S(1)} %get-tuple-element.60), channel_id=1, source_target_pairs={{0,5},{1,4},{2,7},{3,6},{4,1},{5,0},{6,3},{7,2},{8,13},{9,12},{10,... | collective-permute-start | bytes 12296 | tf_op jit(solution)/shard_map/ppermute | solution.py:339
  33.3 1.8 %collective-permute-start.14 = (bf16[4,512]{1,0:T(4,128)(2,1)S(1)}, bf16[4,512]{1,0:T(4,128)(2,1)S(1)}, u32[]{:S(2)}, u32[]{:S(2)}) collective-permute-start(bf16[4,512]{1,0:T(4,128)(2,1)S(1)} %get-tuple-element.61), channel_id=1, source_target_pairs={{0,7},{1,6},{2,5},{3,4},{4,3},{5,2},{6,1},{7,0},{8,15},{9,14},{10,... | collective-permute-start | bytes 12296 | tf_op jit(solution)/shard_map/ppermute | solution.py:339
  35.1 0.3 collective-permute-start.15
  35.3 0.8 %collective-permute-done.13.refs_0_ = bf16[4,512]{1,0:T(4,128)(2,1)S(1)} collective-permute-done((bf16[4,512]{1,0:T(4,128)(2,1)S(1)}, bf16[4,512]{1,0:T(4,128)(2,1)S(1)}, u32[]{:S(2)}, u32[]{:S(2)}) %collective-permute-start.13) | collective-permute-done | bytes 4128 | tf_op jit(solution)/shard_map/ppermute | solution.py:339
  36.2 1.9 %collective-permute-done.14.refs_1_ = bf16[4,512]{1,0:T(4,128)(2,1)S(1)} collective-permute-done((bf16[4,512]{1,0:T(4,128)(2,1)S(1)}, bf16[4,512]{1,0:T(4,128)(2,1)S(1)}, u32[]{:S(2)}, u32[]{:S(2)}) %collective-permute-start.14) | collective-permute-done | bytes 4128 | tf_op jit(solution)/shard_map/ppermute | solution.py:339
  38.1 0.6 %shard_map.160 = bf16[4,512]{1,0:T(4,128)(2,1)} custom-call(f32[4,512]{1,0:T(4,128)S(1)} %get-tuple-element.59.base, bf16[4,512]{1,0:T(4,128)(2,1)S(1)} %collective-permute-done.13.refs_0_, bf16[4,512]{1,0:T(4,128)(2,1)S(1)} %collective-permute-done.14.refs_1_, bf16[4,512]{1,0:T(4,128)(2,1)S(1)} %collective-permute-done.15.refs_2_), custom_call_target="tpu_custom_call" | custom-call | flops 10000000 | bytes 10000 | tf_op jit(solution)/shard_map/pallas_call | solution.py:29
  (30 shorter events, 0.2 us)
Async XLA Ops:
  0.6 4.1 %collective-permute-start = (bf16[4,512]{1,0:T(4,128)(2,1)}, bf16[4,512]{1,0:T(4,128)(2,1)S(1)}, u32[]{:S(2)}, u32[]{:S(2)}) collective-permute-start(bf16[4,512]{1,0:T(4,128)(2,1)} %refs_6_.3), channel_id=1, source_target_pairs={{0,1},{1,0},{2,3},{3,2},{4,5},{5,4},{6,7},{7,6},{8,9},{9,8},{10,11... | collective-permute-start | bytes 12296 | tf_op jit(solution)/shard_map/ppermute | solution.py:280
  4.8 6.0 %copy-start.3 = (bf16[2048,512]{1,0:T(8,128)(2,1)S(1)}, bf16[2048,512]{1,0:T(8,128)(2,1)}, u32[]{:S(2)}) copy-start(bf16[2048,512]{1,0:T(8,128)(2,1)} %refs_4_.1) | copy-start | bytes 6291460
  4.8 9.9 %copy-start.4 = (f32[1,8,128,128]{3,2,1,0:T(8,128)S(1)}, f32[1,8,128,128]{3,2,1,0:T(8,128)}, u32[]{:S(2)}) copy-start(f32[1,8,128,128]{3,2,1,0:T(8,128)} %param.15) | copy-start | bytes 1572868
  4.8 9.9 %copy-start.7 = (f32[1024]{0:T(1024)S(1)}, f32[1024]{0:T(1024)}, u32[]{:S(2)}) copy-start(f32[1024]{0:T(1024)} %param.21) | copy-start | bytes 12292
  4.8 9.9 %copy-start.8 = (f32[1024]{0:T(1024)S(1)}, f32[1024]{0:T(1024)}, u32[]{:S(2)}) copy-start(f32[1024]{0:T(1024)} %param.22) | copy-start | bytes 12292
  5.5 5.3 %collective-permute-start.1 = (bf16[48,128]{1,0:T(8,128)(2,1)S(1)}, bf16[48,128]{1,0:T(8,128)(2,1)S(1)}, u32[]{:S(2)}, u32[]{:S(2)}) collective-permute-start(bf16[48,128]{1,0:T(8,128)(2,1)S(1)} %get-tuple-element.39), channel_id=1, source_target_pairs={{0,4},{2,6},{4,0},{6,2},{1,5},{3,7},{5,1},{7,3},{8,12},{10,14},{12... | collective-permute-start | bytes 36872 | tf_op jit(solution)/shard_map/ppermute | solution.py:320
  9.2 5.5 %collective-permute-start.2 = (bf16[48,128]{1,0:T(8,128)(2,1)S(1)}, bf16[48,128]{1,0:T(8,128)(2,1)S(1)}, u32[]{:S(2)}, u32[]{:S(2)}) collective-permute-start(bf16[48,128]{1,0:T(8,128)(2,1)S(1)} %get-tuple-element.40), channel_id=1, source_target_pairs={{0,6},{2,4},{4,2},{6,0},{1,7},{3,5},{5,3},{7,1},{8,14},{10,12},{12... | collective-permute-start | bytes 36872 | tf_op jit(solution)/shard_map/ppermute | solution.py:320
  10.5 4.1 %collective-permute-start.3 = (bf16[48,128]{1,0:T(8,128)(2,1)S(1)}, bf16[48,128]{1,0:T(8,128)(2,1)S(1)}, u32[]{:S(2)}, u32[]{:S(2)}) collective-permute-start(bf16[48,128]{1,0:T(8,128)(2,1)S(1)} %get-tuple-element.41), channel_id=1, source_target_pairs={{0,2},{2,0},{4,6},{6,4},{1,3},{3,1},{5,7},{7,5},{8,10},{10,8},{12,... | collective-permute-start | bytes 36872 | tf_op jit(solution)/shard_map/ppermute | solution.py:320
  10.8 11.6 %collective-permute-start.8 = (bf16[2048,512]{1,0:T(8,128)(2,1)S(1)}, bf16[2048,512]{1,0:T(8,128)(2,1)S(1)}, u32[]{:S(2)}, u32[]{:S(2)}) collective-permute-start(bf16[2048,512]{1,0:T(8,128)(2,1)S(1)} %copy-done.3), channel_id=1, source_target_pairs={{0,1},{1,0},{2,3},{3,2},{4,5},{5,4},{6,7},{7,6},{8,9},{9,8},{10,11... | collective-permute-start | bytes 6291464 | tf_op jit(solution)/shard_map/ppermute | solution.py:280
  14.7 7.6 %copy-start.6 = (bf16[4,512]{1,0:T(4,128)(2,1)S(1)}, bf16[4,512]{1,0:T(4,128)(2,1)}, u32[]{:S(2)}) copy-start(bf16[4,512]{1,0:T(4,128)(2,1)} %refs_6_.3) | copy-start | bytes 12292
  14.7 11.5 %copy-start = (bf16[1408,4096]{1,0:T(8,128)(2,1)S(1)}, bf16[1408,4096]{1,0:T(8,128)(2,1)}, u32[]{:S(2)}) copy-start(bf16[1408,4096]{1,0:T(8,128)(2,1)} %w_down.3) | copy-start | bytes 34603012
  14.7 11.5 %copy-start.1 = (bf16[4096,1408]{1,0:T(8,128)(2,1)S(1)}, bf16[4096,1408]{1,0:T(8,128)(2,1)}, u32[]{:S(2)}) copy-start(bf16[4096,1408]{1,0:T(8,128)(2,1)} %refs_6_.5) | copy-start | bytes 34603012
  14.7 11.5 %copy-start.2 = (bf16[4096,1408]{1,0:T(8,128)(2,1)S(1)}, bf16[4096,1408]{1,0:T(8,128)(2,1)}, u32[]{:S(2)}) copy-start(bf16[4096,1408]{1,0:T(8,128)(2,1)} %refs_7_.3) | copy-start | bytes 34603012
  15.2 1.2 %collective-permute-start.4 = (f32[8,128]{1,0:T(8,128)S(1)}, f32[8,128]{1,0:T(8,128)S(1)}, u32[]{:S(2)}, u32[]{:S(2)}) collective-permute-start(f32[8,128]{1,0:T(8,128)S(1)} %get-tuple-element.42.own), channel_id=1, source_target_pairs={{0,1},{1,0},{2,3},{3,2},{4,5},{5,4},{6,7},{7,6},{8,9},{9,8},{10,11... | collective-permute-start | bytes 12296 | tf_op jit(solution)/shard_map/ppermute | solution.py:280
  16.4 3.9 %collective-permute-start.7 = (bf16[16,128]{1,0:T(8,128)(2,1)S(1)}, bf16[16,128]{1,0:T(8,128)(2,1)S(1)}, u32[]{:S(2)}, u32[]{:S(2)}) collective-permute-start(bf16[16,128]{1,0:T(8,128)(2,1)S(1)} %shard_map.152.refs_0_), channel_id=1, source_target_pairs={{0,5},{1,4},{2,7},{3,6},{4,1},{5,0},{6,3},{7,2},{8,13},{9,12},{10,... | collective-permute-start | bytes 12296 | tf_op jit(solution)/shard_map/ppermute | solution.py:339
  17.5 4.8 %collective-permute-start.6 = (bf16[16,128]{1,0:T(8,128)(2,1)S(1)}, bf16[16,128]{1,0:T(8,128)(2,1)S(1)}, u32[]{:S(2)}, u32[]{:S(2)}) collective-permute-start(bf16[16,128]{1,0:T(8,128)(2,1)S(1)} %shard_map.152.refs_0_), channel_id=1, source_target_pairs={{0,7},{1,6},{2,5},{3,4},{4,3},{5,2},{6,1},{7,0},{8,15},{9,14},{10,... | collective-permute-start | bytes 12296 | tf_op jit(solution)/shard_map/ppermute | solution.py:339
  18.8 3.5 %collective-permute-start.5 = (bf16[16,128]{1,0:T(8,128)(2,1)S(1)}, bf16[16,128]{1,0:T(8,128)(2,1)S(1)}, u32[]{:S(2)}, u32[]{:S(2)}) collective-permute-start(bf16[16,128]{1,0:T(8,128)(2,1)S(1)} %shard_map.152.refs_0_), channel_id=1, source_target_pairs={{0,3},{1,2},{2,1},{3,0},{4,7},{5,6},{6,5},{7,4},{8,11},{9,10},{10,... | collective-permute-start | bytes 12296 | tf_op jit(solution)/shard_map/ppermute | solution.py:339
  19.9 6.3 %copy-start.5 = (f32[4096]{0:T(1024)S(1)}, f32[4096]{0:T(1024)}, u32[]{:S(2)}) copy-start(f32[4096]{0:T(1024)} %param.24) | copy-start | bytes 49156
  23.0 4.1 %collective-permute-start.9 = (bf16[2,4,512]{2,1,0:T(4,128)(2,1)S(1)}, bf16[2,4,512]{2,1,0:T(4,128)(2,1)S(1)}, u32[]{:S(2)}, u32[]{:S(2)}) collective-permute-start(bf16[2,4,512]{2,1,0:T(4,128)(2,1)S(1)} %get-tuple-element.48.block), channel_id=1, source_target_pairs={{0,5},{1,4},{2,7},{3,6},{4,1},{5,0},{6,3},{7,2},{8,13},{9,12},{10,... | collective-permute-start | bytes 24584 | tf_op jit(solution)/shard_map/ppermute | solution.py:339
  23.7 4.9 %collective-permute-start.11 = (bf16[2,4,512]{2,1,0:T(4,128)(2,1)S(1)}, bf16[2,4,512]{2,1,0:T(4,128)(2,1)S(1)}, u32[]{:S(2)}, u32[]{:S(2)}) collective-permute-start(bf16[2,4,512]{2,1,0:T(4,128)(2,1)S(1)} %get-tuple-element.48.block), channel_id=1, source_target_pairs={{0,7},{1,6},{2,5},{3,4},{4,3},{5,2},{6,1},{7,0},{8,15},{9,14},{10,... | collective-permute-start | bytes 24584 | tf_op jit(solution)/shard_map/ppermute | solution.py:339
  25.4 3.2 %collective-permute-start.10 = (bf16[2,4,512]{2,1,0:T(4,128)(2,1)S(1)}, bf16[2,4,512]{2,1,0:T(4,128)(2,1)S(1)}, u32[]{:S(2)}, u32[]{:S(2)}) collective-permute-start(bf16[2,4,512]{2,1,0:T(4,128)(2,1)S(1)} %get-tuple-element.48.block), channel_id=1, source_target_pairs={{0,3},{1,2},{2,1},{3,0},{4,7},{5,6},{6,5},{7,4},{8,11},{9,10},{10,... | collective-permute-start | bytes 24584 | tf_op jit(solution)/shard_map/ppermute | solution.py:339
  31.0 1.2 %collective-permute-start.12 = (bf16[4,4,512]{2,1,0:T(4,128)(2,1)S(1)}, bf16[4,4,512]{2,1,0:T(4,128)(2,1)S(1)}, u32[]{:S(2)}, u32[]{:S(2)}) collective-permute-start(bf16[4,4,512]{2,1,0:T(4,128)(2,1)S(1)} %get-tuple-element.57), channel_id=1, source_target_pairs={{0,1},{1,0},{2,3},{3,2},{4,5},{5,4},{6,7},{7,6},{8,9},{9,8},{10,11... | collective-permute-start | bytes 49160 | tf_op jit(solution)/shard_map/ppermute | solution.py:280
  32.2 4.0 %collective-permute-start.13 = (bf16[4,512]{1,0:T(4,128)(2,1)S(1)}, bf16[4,512]{1,0:T(4,128)(2,1)S(1)}, u32[]{:S(2)}, u32[]{:S(2)}) collective-permute-start(bf16[4,512]{1,0:T(4,128)(2,1)S(1)} %get-tuple-element.60), channel_id=1, source_target_pairs={{0,5},{1,4},{2,7},{3,6},{4,1},{5,0},{6,3},{7,2},{8,13},{9,12},{10,... | collective-permute-start | bytes 12296 | tf_op jit(solution)/shard_map/ppermute | solution.py:339
  33.3 4.8 %collective-permute-start.14 = (bf16[4,512]{1,0:T(4,128)(2,1)S(1)}, bf16[4,512]{1,0:T(4,128)(2,1)S(1)}, u32[]{:S(2)}, u32[]{:S(2)}) collective-permute-start(bf16[4,512]{1,0:T(4,128)(2,1)S(1)} %get-tuple-element.61), channel_id=1, source_target_pairs={{0,7},{1,6},{2,5},{3,4},{4,3},{5,2},{6,1},{7,0},{8,15},{9,14},{10,... | collective-permute-start | bytes 12296 | tf_op jit(solution)/shard_map/ppermute | solution.py:339
  35.1 3.1 %collective-permute-start.15 = (bf16[4,512]{1,0:T(4,128)(2,1)S(1)}, bf16[4,512]{1,0:T(4,128)(2,1)S(1)}, u32[]{:S(2)}, u32[]{:S(2)}) collective-permute-start(bf16[4,512]{1,0:T(4,128)(2,1)S(1)} %get-tuple-element.62), channel_id=1, source_target_pairs={{0,3},{1,2},{2,1},{3,0},{4,7},{5,6},{6,5},{7,4},{8,11},{9,10},{10,... | collective-permute-start | bytes 12296 | tf_op jit(solution)/shard_map/ppermute | solution.py:339

commit v8 on v7

--- a/solution.py
+++ b/solution.py
@@ -62,8 +62,8 @@
         *[(w.at[pl.ds(theirs, half), :], rest.at[i]) for i, w in enumerate(weights)],
     ]
     copies = [pltpu.make_async_copy(src, dst, sems.at[i]) for i, (src, dst) in enumerate(moves)]
-    for copy in copies:
-        copy.start()
+    for i, copy in enumerate(copies):
+        copy.start(priority=i % 2)
     copies[0].wait()
     copies[1].wait()
     cols = held_tokens[...].astype(jnp.float32)
@@ -239,7 +239,7 @@
 
 def chip_sum_body(sums, passed, mixed, base, *sent):
     base[...] = mixed[...].astype(jnp.float32) + sums[0] + passed[0].astype(jnp.float32)
-    for j, out in zip(chip_order(sums.shape[0]), sent):
+    for j, out in zip(reversed(range(1, sums.shape[0])), sent):
         out[...] = (sums[j] + passed[j].astype(jnp.float32)).astype(jnp.bfloat16)
 
 
@@ -427,7 +427,7 @@
         result_body,
         shape(mixed.shape, jnp.bfloat16),
         base,
-        *[crossed(block, j) for j, block in zip(others, sent)],
+        *[crossed(block, j) for j, block in zip(reversed(range(1, kv_count)), sent)],
     )
     return (result, new_state[None])
 

time: 38.9 us -> 38.8 us (level)
  waiting for transfers between devices: 10.9 us -> 9.84 us
  starting transfers between devices: 15.5 us -> 16.4 us
    ppermute x9, waiting for transfers between devices: 5.8 us -> 4.72 us  [crossed(): lax.ppermute(block, GROUP, [(i, i ^ 2 * j + 1) for i in range(group_count)])]
    ppermute x9, starting transfers between devices: 9.36 us -> 10.3 us  [crossed(): lax.ppermute(block, GROUP, [(i, i ^ 2 * j + 1) for i in range(group_count)])]
where the time goes in v8:
time: 38.8 us; the launch traced here: 38.6 us
  starting transfers between devices  16.4 us (42%)
  Pallas kernels  11.5 us (30%)
  waiting for transfers between devices  9.84 us (25%)
  between operations  0.79 us (2%)
    pallas_call x12, Pallas kernels, call(): pl.pallas_call(body, out_shape=outs, in_specs=[VMEM] * len(args) + [HBM]...  11.5 us
    ppermute x9, starting transfers between devices, crossed(): lax.ppermute(block, GROUP, [(i, i ^ 2 * j + 1) for i in range(group_count)])  10.3 us
    ppermute x3, starting transfers between devices, local(): lax.ppermute(block, 'kv', [(i, i ^ j) for i in range(kv_count)])  5.24 us
    ppermute x9, waiting for transfers between devices, crossed(): lax.ppermute(block, GROUP, [(i, i ^ 2 * j + 1) for i in range(group_count)])  4.72 us
    ppermute x3, waiting for transfers between devices, local(): lax.ppermute(block, 'kv', [(i, i ^ j) for i in range(kv_count)])  3.91 us
    ppermute x4, waiting for transfers between devices, swapped(): return lax.ppermute(block, 'tp', [(0, 1), (1, 0)])  1.21 us
    ppermute x4, starting transfers between devices, swapped(): return lax.ppermute(block, 'tp', [(0, 1), (1, 0)])  0.87 us
  transfers between devices with their start and end apart: 16, of which 8 were waited for; matrix products, arithmetic and copies ran while one was open for 0% of the time, Pallas kernels for 19%

profile of v8, /device:TPU:0, one launch (start us, length us, event | category | flops | bytes accessed | tf_op | source)
XLA Modules:
  0.0 38.6 jit_solution(7323641374052580249)
XLA Ops:
  0.6 0.6 %collective-permute-start = (bf16[4,512]{1,0:T(4,128)(2,1)}, bf16[4,512]{1,0:T(4,128)(2,1)S(1)}, u32[]{:S(2)}, u32[]{:S(2)}) collective-permute-start(bf16[4,512]{1,0:T(4,128)(2,1)} %refs_6_.3), channel_id=1, source_target_pairs={{0,1},{1,0},{2,3},{3,2},{4,5},{5,4},{6,7},{7,6},{8,9},{9,8},{10,11... | collective-permute-start | bytes 12296 | tf_op jit(solution)/shard_map/ppermute | solution.py:280
  1.2 3.6 %shard_map.149 = (f32[4,4,1024]{2,1,0:T(4,128)S(1)}, f32[4,128]{1,0:T(4,128)S(1)}, f32[1,512]{1,0:T(1,128)S(1)}, bf16[4,512,1024]{2,1,0:T(8,128)(2,1)S(1)}) custom-call(bf16[4,512]{1,0:T(4,128)(2,1)} %refs_6_.3, f32[1,4096]{1,0:T(1,128)} %bitcast.13, bf16[1024,1024]{1,0:T(8,128)(2,1)} %w_query.1, bf16[1024,1024]{1,0:T(8,128)(2,1)} %w_forget.1, ...), custom_call_target="tpu_custom_call" | custom-call | flops 10000000 | bytes 10000 | tf_op jit(solution)/shard_map/pallas_call | solution.py:29
  4.8 0.7 %shard_map.150 = (f32[40,128]{1,0:T(8,128)S(1)}, bf16[48,128]{1,0:T(8,128)(2,1)S(1)}, bf16[48,128]{1,0:T(8,128)(2,1)S(1)}, bf16[48,128]{1,0:T(8,128)(2,1)S(1)}) custom-call(bf16[4,512]{1,0:T(4,128)(2,1)S(1)} %collective-permute-done.other.refs_7_, f32[4,4,1024]{2,1,0:T(4,128)S(1)} %get-tuple-element.33.own, f32[4,128]{1,0:T(4,128)S(1)} %get-tuple-element.34.own_squares, ...), custom_call_target="tpu_custom_call" | custom-call | flops 99999997952 | bytes 10000 | tf_op jit(solution)/shard_map/pallas_call | solution.py:29
  5.5 3.7 %collective-permute-start.1 = (bf16[48,128]{1,0:T(8,128)(2,1)S(1)}, bf16[48,128]{1,0:T(8,128)(2,1)S(1)}, u32[]{:S(2)}, u32[]{:S(2)}) collective-permute-start(bf16[48,128]{1,0:T(8,128)(2,1)S(1)} %get-tuple-element.39), channel_id=1, source_target_pairs={{0,4},{2,6},{4,0},{6,2},{1,5},{3,7},{5,1},{7,3},{8,12},{10,14},{12... | collective-permute-start | bytes 36872 | tf_op jit(solution)/shard_map/ppermute | solution.py:320
  9.2 1.3 %collective-permute-start.2 = (bf16[48,128]{1,0:T(8,128)(2,1)S(1)}, bf16[48,128]{1,0:T(8,128)(2,1)S(1)}, u32[]{:S(2)}, u32[]{:S(2)}) collective-permute-start(bf16[48,128]{1,0:T(8,128)(2,1)S(1)} %get-tuple-element.40), channel_id=1, source_target_pairs={{0,6},{2,4},{4,2},{6,0},{1,7},{3,5},{5,3},{7,1},{8,14},{10,12},{12... | collective-permute-start | bytes 36872 | tf_op jit(solution)/shard_map/ppermute | solution.py:320
  10.5 0.2 collective-permute-start.3
  10.8 0.1 collective-permute-done.1.refs_1_
  10.9 3.8 %collective-permute-done.2.refs_2_ = bf16[48,128]{1,0:T(8,128)(2,1)S(1)} collective-permute-done((bf16[48,128]{1,0:T(8,128)(2,1)S(1)}, bf16[48,128]{1,0:T(8,128)(2,1)S(1)}, u32[]{:S(2)}, u32[]{:S(2)}) %collective-permute-start.2) | collective-permute-done | bytes 12320 | tf_op jit(solution)/shard_map/ppermute | solution.py:320
  14.7 0.5 %shard_map.151 = (f32[3,8,128]{2,1,0:T(8,128)S(1)}, f32[8,128]{1,0:T(8,128)S(1)}) custom-call(f32[40,128]{1,0:T(8,128)S(1)} %get-tuple-element.38.refs_0_, bf16[48,128]{1,0:T(8,128)(2,1)S(1)} %collective-permute-done.1.refs_1_, bf16[48,128]{1,0:T(8,128)(2,1)S(1)} %collective-permute-done.2.refs_2_, bf16[48,128]{1,0:T(8,128)(2,1)S(1)} %collective-permute-done.3.refs_3_, ...), custom_call_target="tpu_custom_call" | custom-call | flops 99999997952 | bytes 10000 | tf_op jit(solution)/shard_map/pallas_call | solution.py:29
  15.2 1.2 %collective-permute-done.4.other = f32[8,128]{1,0:T(8,128)S(1)} collective-permute-done((f32[8,128]{1,0:T(8,128)S(1)}, f32[8,128]{1,0:T(8,128)S(1)}, u32[]{:S(2)}, u32[]{:S(2)}) %collective-permute-start.4) | collective-permute-done | bytes 4128 | tf_op jit(solution)/shard_map/ppermute | solution.py:280
  16.4 1.1 %collective-permute-start.7 = (bf16[16,128]{1,0:T(8,128)(2,1)S(1)}, bf16[16,128]{1,0:T(8,128)(2,1)S(1)}, u32[]{:S(2)}, u32[]{:S(2)}) collective-permute-start(bf16[16,128]{1,0:T(8,128)(2,1)S(1)} %shard_map.152.refs_0_), channel_id=1, source_target_pairs={{0,5},{1,4},{2,7},{3,6},{4,1},{5,0},{6,3},{7,2},{8,13},{9,12},{10,... | collective-permute-start | bytes 12296 | tf_op jit(solution)/shard_map/ppermute | solution.py:339
  17.5 1.3 %collective-permute-start.6 = (bf16[16,128]{1,0:T(8,128)(2,1)S(1)}, bf16[16,128]{1,0:T(8,128)(2,1)S(1)}, u32[]{:S(2)}, u32[]{:S(2)}) collective-permute-start(bf16[16,128]{1,0:T(8,128)(2,1)S(1)} %shard_map.152.refs_0_), channel_id=1, source_target_pairs={{0,7},{1,6},{2,5},{3,4},{4,3},{5,2},{6,1},{7,0},{8,15},{9,14},{10,... | collective-permute-start | bytes 12296 | tf_op jit(solution)/shard_map/ppermute | solution.py:339
  18.8 0.6 %collective-permute-start.5 = (bf16[16,128]{1,0:T(8,128)(2,1)S(1)}, bf16[16,128]{1,0:T(8,128)(2,1)S(1)}, u32[]{:S(2)}, u32[]{:S(2)}) collective-permute-start(bf16[16,128]{1,0:T(8,128)(2,1)S(1)} %shard_map.152.refs_0_), channel_id=1, source_target_pairs={{0,3},{1,2},{2,1},{3,0},{4,7},{5,6},{6,5},{7,4},{8,11},{9,10},{10,... | collective-permute-start | bytes 12296 | tf_op jit(solution)/shard_map/ppermute | solution.py:339
  19.4 0.5 %shard_map.153.new_state = f32[8,128,128]{2,1,0:T(8,128)S(1)} custom-call(f32[3,8,128]{2,1,0:T(8,128)S(1)} %get-tuple-element.43.gates, f32[8,128,128]{2,1,0:T(8,128)S(1)} %bitcast.7), custom_call_target="tpu_custom_call" | custom-call | flops 10000000 | bytes 10000 | tf_op jit(solution)/shard_map/pallas_call | solution.py:29
  19.9 0.4 %collective-permute-done.7.refs_3_ = bf16[16,128]{1,0:T(8,128)(2,1)S(1)} collective-permute-done((bf16[16,128]{1,0:T(8,128)(2,1)S(1)}, bf16[16,128]{1,0:T(8,128)(2,1)S(1)}, u32[]{:S(2)}, u32[]{:S(2)}) %collective-permute-start.7) | collective-permute-done | bytes 4128 | tf_op jit(solution)/shard_map/ppermute | solution.py:339
  20.4 2.0 %collective-permute-done.6.refs_2_ = bf16[16,128]{1,0:T(8,128)(2,1)S(1)} collective-permute-done((bf16[16,128]{1,0:T(8,128)(2,1)S(1)}, bf16[16,128]{1,0:T(8,128)(2,1)S(1)}, u32[]{:S(2)}, u32[]{:S(2)}) %collective-permute-start.6) | collective-permute-done | bytes 4128 | tf_op jit(solution)/shard_map/ppermute | solution.py:339
  22.3 0.7 %shard_map.154 = (bf16[2,4,512]{2,1,0:T(4,128)(2,1)S(1)}, bf16[4,512]{1,0:T(4,128)(2,1)S(1)}) custom-call(bf16[16,128]{1,0:T(8,128)(2,1)S(1)} %shard_map.152.refs_0_, bf16[16,128]{1,0:T(8,128)(2,1)S(1)} %collective-permute-done.5.refs_1_, bf16[16,128]{1,0:T(8,128)(2,1)S(1)} %collective-permute-done.6.refs_2_, ...), custom_call_target="tpu_custom_call" | custom-call | flops 10000000 | bytes 10000 | tf_op jit(solution)/shard_map/pallas_call | solution.py:29
  23.0 0.7 %collective-permute-start.9 = (bf16[2,4,512]{2,1,0:T(4,128)(2,1)S(1)}, bf16[2,4,512]{2,1,0:T(4,128)(2,1)S(1)}, u32[]{:S(2)}, u32[]{:S(2)}) collective-permute-start(bf16[2,4,512]{2,1,0:T(4,128)(2,1)S(1)} %get-tuple-element.48.block), channel_id=1, source_target_pairs={{0,5},{1,4},{2,7},{3,6},{4,1},{5,0},{6,3},{7,2},{8,13},{9,12},{10,... | collective-permute-start | bytes 24584 | tf_op jit(solution)/shard_map/ppermute | solution.py:339
  23.7 1.8 %collective-permute-start.11 = (bf16[2,4,512]{2,1,0:T(4,128)(2,1)S(1)}, bf16[2,4,512]{2,1,0:T(4,128)(2,1)S(1)}, u32[]{:S(2)}, u32[]{:S(2)}) collective-permute-start(bf16[2,4,512]{2,1,0:T(4,128)(2,1)S(1)} %get-tuple-element.48.block), channel_id=1, source_target_pairs={{0,7},{1,6},{2,5},{3,4},{4,3},{5,2},{6,1},{7,0},{8,15},{9,14},{10,... | collective-permute-start | bytes 24584 | tf_op jit(solution)/shard_map/ppermute | solution.py:339
  25.4 0.8 %collective-permute-start.10 = (bf16[2,4,512]{2,1,0:T(4,128)(2,1)S(1)}, bf16[2,4,512]{2,1,0:T(4,128)(2,1)S(1)}, u32[]{:S(2)}, u32[]{:S(2)}) collective-permute-start(bf16[2,4,512]{2,1,0:T(4,128)(2,1)S(1)} %get-tuple-element.48.block), channel_id=1, source_target_pairs={{0,3},{1,2},{2,1},{3,0},{4,7},{5,6},{6,5},{7,4},{8,11},{9,10},{10,... | collective-permute-start | bytes 24584 | tf_op jit(solution)/shard_map/ppermute | solution.py:339
  26.2 0.9 %shard_map.155 = (f32[4,1408]{1,0:T(4,128)S(1)}, f32[4,1408]{1,0:T(4,128)S(1)}, f32[4,128]{1,0:T(4,128)S(1)}, f32[8,128,128]{2,1,0:T(8,128)}) custom-call(bf16[2,4,512]{2,1,0:T(4,128)(2,1)S(1)} %get-tuple-element.48.block, f32[1,4096]{1,0:T(1,128)S(1)} %bitcast.8, bf16[4096,1408]{1,0:T(8,128)(2,1)S(1)} %copy-done.1, bf16[4096,1408]{1,0:T(8,128)(2,1)S(1)} %copy-done.2, ...), custom_call_target="tpu_custom_call" | custom-call | flops 10000000 | bytes 10000 | tf_op jit(solution)/shard_map/pallas_call | solution.py:29
  27.1 0.9 %shard_map.156 = (f32[4,1408]{1,0:T(4,128)S(1)}, f32[4,1408]{1,0:T(4,128)S(1)}, f32[4,128]{1,0:T(4,128)S(1)}) custom-call(f32[4,1408]{1,0:T(4,128)S(1)} %get-tuple-element.50.refs_0_, f32[4,1408]{1,0:T(4,128)S(1)} %get-tuple-element.51.refs_1_, f32[4,128]{1,0:T(4,128)S(1)} %get-tuple-element.52.refs_2_, ...), custom_call_target="tpu_custom_call" | custom-call | flops 10000000 | bytes 10000 | tf_op jit(solution)/shard_map/pallas_call | solution.py:29
  28.0 0.6 %collective-permute-done.11.refs_4_ = bf16[2,4,512]{2,1,0:T(4,128)(2,1)S(1)} collective-permute-done((bf16[2,4,512]{2,1,0:T(4,128)(2,1)S(1)}, bf16[2,4,512]{2,1,0:T(4,128)(2,1)S(1)}, u32[]{:S(2)}, u32[]{:S(2)}) %collective-permute-start.11) | collective-permute-done | bytes 8224 | tf_op jit(solution)/shard_map/ppermute | solution.py:339
  28.6 2.4 %shard_map.157 = (bf16[4,1408]{1,0:T(4,128)(2,1)S(1)}, bf16[4,4,512]{2,1,0:T(4,128)(2,1)S(1)}) custom-call(f32[4,1408]{1,0:T(4,128)S(1)} %get-tuple-element.53.refs_0_, f32[4,1408]{1,0:T(4,128)S(1)} %get-tuple-element.54.refs_1_, f32[4,128]{1,0:T(4,128)S(1)} %get-tuple-element.55.refs_2_, bf16[2,4,512]{2,1,0:T(4,128)(2,1)S(1)} %collective-permute-done.10.refs_3_, ...), custom_call_target="tpu_custom_call" | custom-call | flops 10000000 | bytes 10000 | tf_op jit(solution)/shard_map/pallas_call | solution.py:29
  31.0 0.3 collective-permute-start.12
  31.3 0.9 %shard_map.158.sums = f32[4,4,512]{2,1,0:T(4,128)S(1)} custom-call(bf16[4,1408]{1,0:T(4,128)(2,1)S(1)} %get-tuple-element.56.hidden, bf16[1408,4096]{1,0:T(8,128)(2,1)S(1)} %copy-done), custom_call_target="tpu_custom_call" | custom-call | flops 10000000 | bytes 10000 | tf_op jit(solution)/shard_map/pallas_call | solution.py:29
  32.2 1.9 %collective-permute-start.13 = (bf16[4,512]{1,0:T(4,128)(2,1)S(1)}, bf16[4,512]{1,0:T(4,128)(2,1)S(1)}, u32[]{:S(2)}, u32[]{:S(2)}) collective-permute-start(bf16[4,512]{1,0:T(4,128)(2,1)S(1)} %get-tuple-element.60), channel_id=1, source_target_pairs={{0,7},{1,6},{2,5},{3,4},{4,3},{5,2},{6,1},{7,0},{8,15},{9,14},{10,... | collective-permute-start | bytes 12296 | tf_op jit(solution)/shard_map/ppermute | solution.py:339
  34.0 0.1 collective-permute-start.14
  34.2 2.1 %collective-permute-start.15 = (bf16[4,512]{1,0:T(4,128)(2,1)S(1)}, bf16[4,512]{1,0:T(4,128)(2,1)S(1)}, u32[]{:S(2)}, u32[]{:S(2)}) collective-permute-start(bf16[4,512]{1,0:T(4,128)(2,1)S(1)} %get-tuple-element.62), channel_id=1, source_target_pairs={{0,3},{1,2},{2,1},{3,0},{4,7},{5,6},{6,5},{7,4},{8,11},{9,10},{10,... | collective-permute-start | bytes 12296 | tf_op jit(solution)/shard_map/ppermute | solution.py:339
  36.2 0.8 %collective-permute-done.13.refs_0_ = bf16[4,512]{1,0:T(4,128)(2,1)S(1)} collective-permute-done((bf16[4,512]{1,0:T(4,128)(2,1)S(1)}, bf16[4,512]{1,0:T(4,128)(2,1)S(1)}, u32[]{:S(2)}, u32[]{:S(2)}) %collective-permute-start.13) | collective-permute-done | bytes 4128 | tf_op jit(solution)/shard_map/ppermute | solution.py:339
  37.1 0.9 %collective-permute-done.14.refs_1_ = bf16[4,512]{1,0:T(4,128)(2,1)S(1)} collective-permute-done((bf16[4,512]{1,0:T(4,128)(2,1)S(1)}, bf16[4,512]{1,0:T(4,128)(2,1)S(1)}, u32[]{:S(2)}, u32[]{:S(2)}) %collective-permute-start.14) | collective-permute-done | bytes 4128 | tf_op jit(solution)/shard_map/ppermute | solution.py:339
  38.0 0.6 %shard_map.160 = bf16[4,512]{1,0:T(4,128)(2,1)} custom-call(f32[4,512]{1,0:T(4,128)S(1)} %get-tuple-element.59.base, bf16[4,512]{1,0:T(4,128)(2,1)S(1)} %collective-permute-done.13.refs_0_, bf16[4,512]{1,0:T(4,128)(2,1)S(1)} %collective-permute-done.14.refs_1_, bf16[4,512]{1,0:T(4,128)(2,1)S(1)} %collective-permute-done.15.refs_2_), custom_call_target="tpu_custom_call" | custom-call | flops 10000000 | bytes 10000 | tf_op jit(solution)/shard_map/pallas_call | solution.py:29
  (30 shorter events, 0.1 us)
Async XLA Ops:
  0.6 4.1 %collective-permute-start = (bf16[4,512]{1,0:T(4,128)(2,1)}, bf16[4,512]{1,0:T(4,128)(2,1)S(1)}, u32[]{:S(2)}, u32[]{:S(2)}) collective-permute-start(bf16[4,512]{1,0:T(4,128)(2,1)} %refs_6_.3), channel_id=1, source_target_pairs={{0,1},{1,0},{2,3},{3,2},{4,5},{5,4},{6,7},{7,6},{8,9},{9,8},{10,11... | collective-permute-start | bytes 12296 | tf_op jit(solution)/shard_map/ppermute | solution.py:280
  4.8 6.0 %copy-start.3 = (bf16[2048,512]{1,0:T(8,128)(2,1)S(1)}, bf16[2048,512]{1,0:T(8,128)(2,1)}, u32[]{:S(2)}) copy-start(bf16[2048,512]{1,0:T(8,128)(2,1)} %refs_4_.1) | copy-start | bytes 6291460
  4.8 9.9 %copy-start.4 = (f32[1,8,128,128]{3,2,1,0:T(8,128)S(1)}, f32[1,8,128,128]{3,2,1,0:T(8,128)}, u32[]{:S(2)}) copy-start(f32[1,8,128,128]{3,2,1,0:T(8,128)} %param.15) | copy-start | bytes 1572868
  4.8 9.9 %copy-start.7 = (f32[1024]{0:T(1024)S(1)}, f32[1024]{0:T(1024)}, u32[]{:S(2)}) copy-start(f32[1024]{0:T(1024)} %param.21) | copy-start | bytes 12292
  4.8 9.9 %copy-start.8 = (f32[1024]{0:T(1024)S(1)}, f32[1024]{0:T(1024)}, u32[]{:S(2)}) copy-start(f32[1024]{0:T(1024)} %param.22) | copy-start | bytes 12292
  5.5 5.3 %collective-permute-start.1 = (bf16[48,128]{1,0:T(8,128)(2,1)S(1)}, bf16[48,128]{1,0:T(8,128)(2,1)S(1)}, u32[]{:S(2)}, u32[]{:S(2)}) collective-permute-start(bf16[48,128]{1,0:T(8,128)(2,1)S(1)} %get-tuple-element.39), channel_id=1, source_target_pairs={{0,4},{2,6},{4,0},{6,2},{1,5},{3,7},{5,1},{7,3},{8,12},{10,14},{12... | collective-permute-start | bytes 36872 | tf_op jit(solution)/shard_map/ppermute | solution.py:320
  9.2 5.5 %collective-permute-start.2 = (bf16[48,128]{1,0:T(8,128)(2,1)S(1)}, bf16[48,128]{1,0:T(8,128)(2,1)S(1)}, u32[]{:S(2)}, u32[]{:S(2)}) collective-permute-start(bf16[48,128]{1,0:T(8,128)(2,1)S(1)} %get-tuple-element.40), channel_id=1, source_target_pairs={{0,6},{2,4},{4,2},{6,0},{1,7},{3,5},{5,3},{7,1},{8,14},{10,12},{12... | collective-permute-start | bytes 36872 | tf_op jit(solution)/shard_map/ppermute | solution.py:320
  10.5 4.1 %collective-permute-start.3 = (bf16[48,128]{1,0:T(8,128)(2,1)S(1)}, bf16[48,128]{1,0:T(8,128)(2,1)S(1)}, u32[]{:S(2)}, u32[]{:S(2)}) collective-permute-start(bf16[48,128]{1,0:T(8,128)(2,1)S(1)} %get-tuple-element.41), channel_id=1, source_target_pairs={{0,2},{2,0},{4,6},{6,4},{1,3},{3,1},{5,7},{7,5},{8,10},{10,8},{12,... | collective-permute-start | bytes 36872 | tf_op jit(solution)/shard_map/ppermute | solution.py:320
  10.8 11.6 %collective-permute-start.8 = (bf16[2048,512]{1,0:T(8,128)(2,1)S(1)}, bf16[2048,512]{1,0:T(8,128)(2,1)S(1)}, u32[]{:S(2)}, u32[]{:S(2)}) collective-permute-start(bf16[2048,512]{1,0:T(8,128)(2,1)S(1)} %copy-done.3), channel_id=1, source_target_pairs={{0,1},{1,0},{2,3},{3,2},{4,5},{5,4},{6,7},{7,6},{8,9},{9,8},{10,11... | collective-permute-start | bytes 6291464 | tf_op jit(solution)/shard_map/ppermute | solution.py:280
  14.7 7.6 %copy-start.6 = (bf16[4,512]{1,0:T(4,128)(2,1)S(1)}, bf16[4,512]{1,0:T(4,128)(2,1)}, u32[]{:S(2)}) copy-start(bf16[4,512]{1,0:T(4,128)(2,1)} %refs_6_.3) | copy-start | bytes 12292
  14.7 11.5 %copy-start = (bf16[1408,4096]{1,0:T(8,128)(2,1)S(1)}, bf16[1408,4096]{1,0:T(8,128)(2,1)}, u32[]{:S(2)}) copy-start(bf16[1408,4096]{1,0:T(8,128)(2,1)} %w_down.3) | copy-start | bytes 34603012
  14.7 11.5 %copy-start.1 = (bf16[4096,1408]{1,0:T(8,128)(2,1)S(1)}, bf16[4096,1408]{1,0:T(8,128)(2,1)}, u32[]{:S(2)}) copy-start(bf16[4096,1408]{1,0:T(8,128)(2,1)} %refs_6_.5) | copy-start | bytes 34603012
  14.7 11.5 %copy-start.2 = (bf16[4096,1408]{1,0:T(8,128)(2,1)S(1)}, bf16[4096,1408]{1,0:T(8,128)(2,1)}, u32[]{:S(2)}) copy-start(bf16[4096,1408]{1,0:T(8,128)(2,1)} %refs_7_.3) | copy-start | bytes 34603012
  15.2 1.2 %collective-permute-start.4 = (f32[8,128]{1,0:T(8,128)S(1)}, f32[8,128]{1,0:T(8,128)S(1)}, u32[]{:S(2)}, u32[]{:S(2)}) collective-permute-start(f32[8,128]{1,0:T(8,128)S(1)} %get-tuple-element.42.own), channel_id=1, source_target_pairs={{0,1},{1,0},{2,3},{3,2},{4,5},{5,4},{6,7},{7,6},{8,9},{9,8},{10,11... | collective-permute-start | bytes 12296 | tf_op jit(solution)/shard_map/ppermute | solution.py:280
  16.4 3.9 %collective-permute-start.7 = (bf16[16,128]{1,0:T(8,128)(2,1)S(1)}, bf16[16,128]{1,0:T(8,128)(2,1)S(1)}, u32[]{:S(2)}, u32[]{:S(2)}) collective-permute-start(bf16[16,128]{1,0:T(8,128)(2,1)S(1)} %shard_map.152.refs_0_), channel_id=1, source_target_pairs={{0,5},{1,4},{2,7},{3,6},{4,1},{5,0},{6,3},{7,2},{8,13},{9,12},{10,... | collective-permute-start | bytes 12296 | tf_op jit(solution)/shard_map/ppermute | solution.py:339
  17.5 4.8 %collective-permute-start.6 = (bf16[16,128]{1,0:T(8,128)(2,1)S(1)}, bf16[16,128]{1,0:T(8,128)(2,1)S(1)}, u32[]{:S(2)}, u32[]{:S(2)}) collective-permute-start(bf16[16,128]{1,0:T(8,128)(2,1)S(1)} %shard_map.152.refs_0_), channel_id=1, source_target_pairs={{0,7},{1,6},{2,5},{3,4},{4,3},{5,2},{6,1},{7,0},{8,15},{9,14},{10,... | collective-permute-start | bytes 12296 | tf_op jit(solution)/shard_map/ppermute | solution.py:339
  18.8 3.5 %collective-permute-start.5 = (bf16[16,128]{1,0:T(8,128)(2,1)S(1)}, bf16[16,128]{1,0:T(8,128)(2,1)S(1)}, u32[]{:S(2)}, u32[]{:S(2)}) collective-permute-start(bf16[16,128]{1,0:T(8,128)(2,1)S(1)} %shard_map.152.refs_0_), channel_id=1, source_target_pairs={{0,3},{1,2},{2,1},{3,0},{4,7},{5,6},{6,5},{7,4},{8,11},{9,10},{10,... | collective-permute-start | bytes 12296 | tf_op jit(solution)/shard_map/ppermute | solution.py:339
  19.9 6.3 %copy-start.5 = (f32[4096]{0:T(1024)S(1)}, f32[4096]{0:T(1024)}, u32[]{:S(2)}) copy-start(f32[4096]{0:T(1024)} %param.24) | copy-start | bytes 49156
  23.0 4.1 %collective-permute-start.9 = (bf16[2,4,512]{2,1,0:T(4,128)(2,1)S(1)}, bf16[2,4,512]{2,1,0:T(4,128)(2,1)S(1)}, u32[]{:S(2)}, u32[]{:S(2)}) collective-permute-start(bf16[2,4,512]{2,1,0:T(4,128)(2,1)S(1)} %get-tuple-element.48.block), channel_id=1, source_target_pairs={{0,5},{1,4},{2,7},{3,6},{4,1},{5,0},{6,3},{7,2},{8,13},{9,12},{10,... | collective-permute-start | bytes 24584 | tf_op jit(solution)/shard_map/ppermute | solution.py:339
  23.7 4.9 %collective-permute-start.11 = (bf16[2,4,512]{2,1,0:T(4,128)(2,1)S(1)}, bf16[2,4,512]{2,1,0:T(4,128)(2,1)S(1)}, u32[]{:S(2)}, u32[]{:S(2)}) collective-permute-start(bf16[2,4,512]{2,1,0:T(4,128)(2,1)S(1)} %get-tuple-element.48.block), channel_id=1, source_target_pairs={{0,7},{1,6},{2,5},{3,4},{4,3},{5,2},{6,1},{7,0},{8,15},{9,14},{10,... | collective-permute-start | bytes 24584 | tf_op jit(solution)/shard_map/ppermute | solution.py:339
  25.4 3.2 %collective-permute-start.10 = (bf16[2,4,512]{2,1,0:T(4,128)(2,1)S(1)}, bf16[2,4,512]{2,1,0:T(4,128)(2,1)S(1)}, u32[]{:S(2)}, u32[]{:S(2)}) collective-permute-start(bf16[2,4,512]{2,1,0:T(4,128)(2,1)S(1)} %get-tuple-element.48.block), channel_id=1, source_target_pairs={{0,3},{1,2},{2,1},{3,0},{4,7},{5,6},{6,5},{7,4},{8,11},{9,10},{10,... | collective-permute-start | bytes 24584 | tf_op jit(solution)/shard_map/ppermute | solution.py:339
  31.0 1.2 %collective-permute-start.12 = (bf16[4,4,512]{2,1,0:T(4,128)(2,1)S(1)}, bf16[4,4,512]{2,1,0:T(4,128)(2,1)S(1)}, u32[]{:S(2)}, u32[]{:S(2)}) collective-permute-start(bf16[4,4,512]{2,1,0:T(4,128)(2,1)S(1)} %get-tuple-element.57), channel_id=1, source_target_pairs={{0,1},{1,0},{2,3},{3,2},{4,5},{5,4},{6,7},{7,6},{8,9},{9,8},{10,11... | collective-permute-start | bytes 49160 | tf_op jit(solution)/shard_map/ppermute | solution.py:280
  32.2 4.9 %collective-permute-start.13 = (bf16[4,512]{1,0:T(4,128)(2,1)S(1)}, bf16[4,512]{1,0:T(4,128)(2,1)S(1)}, u32[]{:S(2)}, u32[]{:S(2)}) collective-permute-start(bf16[4,512]{1,0:T(4,128)(2,1)S(1)} %get-tuple-element.60), channel_id=1, source_target_pairs={{0,7},{1,6},{2,5},{3,4},{4,3},{5,2},{6,1},{7,0},{8,15},{9,14},{10,... | collective-permute-start | bytes 12296 | tf_op jit(solution)/shard_map/ppermute | solution.py:339
  34.0 3.9 %collective-permute-start.14 = (bf16[4,512]{1,0:T(4,128)(2,1)S(1)}, bf16[4,512]{1,0:T(4,128)(2,1)S(1)}, u32[]{:S(2)}, u32[]{:S(2)}) collective-permute-start(bf16[4,512]{1,0:T(4,128)(2,1)S(1)} %get-tuple-element.61), channel_id=1, source_target_pairs={{0,5},{1,4},{2,7},{3,6},{4,1},{5,0},{6,3},{7,2},{8,13},{9,12},{10,... | collective-permute-start | bytes 12296 | tf_op jit(solution)/shard_map/ppermute | solution.py:339
  34.2 3.8 %collective-permute-start.15 = (bf16[4,512]{1,0:T(4,128)(2,1)S(1)}, bf16[4,512]{1,0:T(4,128)(2,1)S(1)}, u32[]{:S(2)}, u32[]{:S(2)}) collective-permute-start(bf16[4,512]{1,0:T(4,128)(2,1)S(1)} %get-tuple-element.62), channel_id=1, source_target_pairs={{0,3},{1,2},{2,1},{3,0},{4,7},{5,6},{6,5},{7,4},{8,11},{9,10},{10,... | collective-permute-start | bytes 12296 | tf_op jit(solution)/shard_map/ppermute | solution.py:339
